TPU v7x, 32 devices: a whole 2x2x4 slice. The times are simulated.
32 devices in a mesh: kv: 8 (over z, x), tp: 4 (over y, core).
Axes of the slice: x: 2, y: 2, z: 4, core: 2. Of those that a mesh axis runs over, the one named last changes fastest.
Arguments:
- inputs: bfloat16 [4, 2048, 2048], P(None, 'kv'), may hold values from -40 to 40
- query_weight: bfloat16 [2048, 2048], P(None, 'tp'), may hold values from -0.125 to 0.125
- key_weight: bfloat16 [2048, 1024], P(None, 'tp'), may hold values from -0.125 to 0.125
- value_weight: bfloat16 [2048, 1024], P(None, 'tp'), may hold values from -0.125 to 0.125
- out_weight: bfloat16 [2048, 2048], P('tp'), may hold values from -1 to 1
- chosen: int32 [4, 32, 32], P(None, 'kv'), may hold values from 0 to 31, as said below
- lengths: int32 [4], replicated, may hold values from 1 to 2048, 3072 in all
Outputs:
- mixed: bfloat16 [4, 2048, 2048], P(None, 'kv', 'tp')
Inputs may be any that keep to these rules, and one draw needn't show every extreme that they name: chosen[b, q, 0] = q; every entry names a block of the same sequence at or before q; entries may repeat. Over the query blocks of positions k * 256 to (k+1) * 256 - 1 of all sequences, the named blocks that lie in another span of 256 positions number at most 3 distinct blocks for each other span, and 3 is reached.
All inputs are finite; a program needn't handle non-finite values.
Results may differ from a plain program's by a relative error of at most 0.014.
The roundings to bfloat16 on the way count: a program that leaves them out, or rounds other values in their place, can miss the bound.
Values may be sent and summed in bfloat16 or wider, within the bound.
No kernel may reach another device: no remote copies, remote signals or barrier semaphores. Data moves between devices by JAX's collectives and lax.ppermute only.
A program may use at most 128 MiB of HBM per device.

v0:
```python
import jax
import jax.numpy as jnp
from jax import lax
from jax.sharding import PartitionSpec as P

HD = 128
KB = 64
TOPK = 32
CAP = 3


def unique_slots(chosen_rows):
    order = jnp.arange(TOPK, dtype=jnp.int32)
    repeated = jnp.any(
        (chosen_rows[..., :, None] == chosen_rows[..., None, :])
        & (order[:, None] > order[None, :]),
        axis=-1,
    )
    return jnp.repeat(jnp.logical_not(repeated), KB, axis=-1)


def attend(queries, key_sets, value_sets, key_pos, unique_key, query_pos, live_length, scaling):
    scores = (
        jnp.einsum("nqkgd,npkd->nkgqp", queries, key_sets, preferred_element_type=jnp.float32)
        * scaling
    )
    allowed = (
        (key_pos[:, None, :] <= query_pos[:, :, None])
        & (key_pos[:, None, :] < live_length)
        & unique_key[:, None, :]
    )
    allowed = allowed | (key_pos[:, None, :] == query_pos[:, :, None])
    scores = jnp.where(allowed[:, None, None], scores, -jnp.inf)
    highest = jnp.max(scores, axis=-1, keepdims=True)
    raised = jnp.exp(scores - highest)
    weights = (raised / jnp.sum(raised, axis=-1, keepdims=True)).astype(jnp.bfloat16)
    combined = jnp.einsum(
        "nkgqp,npkd->nqkgd", weights, value_sets, preferred_element_type=jnp.float32
    )
    living = (query_pos < live_length)[:, :, None, None, None]
    return jnp.where(living, combined, 0.0).astype(jnp.bfloat16)


def shards(inputs, query_weight, key_weight, value_weight, out_weight, chosen, lengths):
    batch_size, positions, model_width = inputs.shape
    kv_local = key_weight.shape[1] // HD
    heads_local = query_weight.shape[1] // HD
    per_group = heads_local // kv_local
    per_dev = positions // KB
    owned = batch_size * per_dev
    device = lax.axis_index("kv")
    devices = lax.axis_size("kv")
    flat_rows = inputs.reshape(batch_size * positions, model_width)
    queries = jnp.dot(flat_rows, query_weight, preferred_element_type=jnp.float32).astype(
        jnp.bfloat16
    )
    queries = queries.reshape(batch_size, per_dev, KB, kv_local, per_group, HD)
    key_rows = jnp.dot(flat_rows, key_weight, preferred_element_type=jnp.float32).astype(
        jnp.bfloat16
    )
    key_rows = key_rows.reshape(owned, KB, kv_local * HD)
    value_rows = jnp.dot(flat_rows, value_weight, preferred_element_type=jnp.float32).astype(
        jnp.bfloat16
    )
    value_rows = value_rows.reshape(owned, KB, kv_local * HD)
    seq_base = jnp.arange(batch_size, dtype=jnp.int32)[:, None, None]
    owners = chosen // per_dev
    local_block = seq_base * per_dev + chosen % per_dev
    one_hot = (owners * owned + local_block).reshape(-1)[:, None] == jnp.arange(
        devices * owned, dtype=jnp.int32
    )[None, :]
    needed = jnp.any(one_hot, axis=0).reshape(devices, owned) & (
        jnp.arange(devices, dtype=jnp.int32)[:, None] != device
    )
    slots = jnp.cumsum(needed.astype(jnp.int32), axis=1) - 1
    matches = needed[:, :, None] & (
        slots[:, :, None] == jnp.arange(CAP, dtype=jnp.int32)[None, None, :]
    )
    requests = jnp.sum(
        jnp.where(matches, jnp.arange(owned, dtype=jnp.int32)[None, :, None], 0), axis=1
    )
    asked = lax.all_to_all(requests, "kv", split_axis=0, concat_axis=0, tiled=True)
    got_keys, got_values = (
        lax.all_to_all(key_rows[asked], "kv", split_axis=0, concat_axis=0, tiled=True),
        lax.all_to_all(value_rows[asked], "kv", split_axis=0, concat_axis=0, tiled=True),
    )
    key_table = jnp.concatenate(
        [key_rows, got_keys.reshape(devices * CAP, KB, kv_local * HD)], axis=0
    )
    value_table = jnp.concatenate(
        [value_rows, got_values.reshape(devices * CAP, KB, kv_local * HD)], axis=0
    )
    slot_of = jnp.sum(jnp.where(one_hot, slots.reshape(-1)[None, :], 0), axis=1).reshape(
        chosen.shape
    )
    table_rows = jnp.where(owners == device, local_block, owned + owners * CAP + slot_of)
    offsets = jnp.arange(KB, dtype=jnp.int32)
    query_pos = (device * per_dev + jnp.arange(per_dev, dtype=jnp.int32))[:, None] * KB + offsets[
        None, :
    ]
    key_pos = (chosen[..., None] * KB + offsets).reshape(batch_size, per_dev, TOPK * KB)
    unique_key = unique_slots(chosen)
    scaling = HD ** (-0.5)

    def one_seq(seq_inputs):
        seq_queries, seq_rows, seq_key_pos, seq_unique, live_length = seq_inputs
        key_sets = key_table[seq_rows].reshape(per_dev, TOPK * KB, kv_local, HD)
        value_sets = value_table[seq_rows].reshape(per_dev, TOPK * KB, kv_local, HD)
        return attend(
            seq_queries,
            key_sets,
            value_sets,
            seq_key_pos,
            seq_unique,
            query_pos,
            live_length,
            scaling,
        )

    attended = lax.map(one_seq, (queries, table_rows, key_pos, unique_key, lengths))
    attended = attended.reshape(batch_size * positions, heads_local * HD)
    partial_value = jnp.dot(attended, out_weight, preferred_element_type=jnp.float32).astype(
        jnp.bfloat16
    )
    partial_value = (
        lax.optimization_barrier(partial_value)
        .astype(jnp.float32)
        .reshape(batch_size, positions, model_width)
    )
    return lax.psum_scatter(
        partial_value.astype(jnp.bfloat16), "tp", scatter_dimension=2, tiled=True
    )


def solution(mesh):
    placed = (
        P(None, "kv", None),
        P(None, "tp"),
        P(None, "tp"),
        P(None, "tp"),
        P("tp", None),
        P(None, "kv", None),
        P(),
    )
    return jax.shard_map(
        shards, mesh=mesh, in_specs=placed, out_specs=P(None, "kv", "tp"), check_vma=False
    )
```

profile of v0, /device:TPU:0, one launch (start us, length us, event | category | flops | bytes accessed | tf_op | source)
XLA Modules:
  0.0 305.6 jit_solution(2691484994486179288)
XLA Ops:
  8.9 7.3 %all-to-all-start = ((s32[8,1,3]{2,1,0:T(1,128)}), s32[8,1,3]{2,1,0:T(1,128)S(1)}, u32[]{:S(2)}, u32[]{:S(2)}) async-start(s32[8,1,3]{2,1,0:T(1,128)} %copy.26), calls=%async_computation | async-start | bytes 8192 | tf_op jit(solution)/shard_map/all_to_all | solution.py:82
  16.2 3.7 %convolution_convert_fusion.3 = bf16[1024,256]{1,0:T(8,128)(2,1)S(1)} fusion(bf16[1024,2048]{1,0:T(8,128)(2,1)} %bitcast.80, bf16[2048,256]{1,0:T(8,128)(2,1)} %param.12), kind=kOutput, calls=%fused_computation.38 | convolution fusion | flops 1074003968 | bytes 5767168 | tf_op jit(solution)/shard_map/dot_general | solution.py:62
  24.4 4.2 %all-to-all-start.1 = ((bf16[8,3,64,256]{3,2,1,0:T(8,128)(2,1)}), bf16[8,3,64,256]{3,2,1,0:T(8,128)(2,1)}, u32[]{:S(2)}, u32[]{:S(2)}) async-start(bf16[8,3,64,256]{3,2,1,0:T(8,128)(2,1)} %bitcast.4), calls=%async_computation.1 | async-start | bytes 1572864 | tf_op jit(solution)/shard_map/all_to_all | solution.py:85
  28.6 3.7 %convolution_convert_fusion.2 = bf16[1024,256]{1,0:T(8,128)(2,1)S(1)} fusion(bf16[1024,2048]{1,0:T(8,128)(2,1)} %bitcast.81, bf16[2048,256]{1,0:T(8,128)(2,1)} %param.11), kind=kOutput, calls=%fused_computation.37 | convolution fusion | flops 1074003968 | bytes 5767168 | tf_op jit(solution)/shard_map/dot_general | solution.py:58
  33.8 13.8 %all-to-all-done.1 = bf16[8,3,64,256]{3,2,1,0:T(8,128)(2,1)} async-done(((bf16[8,3,64,256]{3,2,1,0:T(8,128)(2,1)}), bf16[8,3,64,256]{3,2,1,0:T(8,128)(2,1)}, u32[]{:S(2)}, u32[]{:S(2)}) %all-to-all-start.1) | async-done | bytes 786464 | tf_op jit(solution)/shard_map/all_to_all | solution.py:85
  47.7 4.2 %all-to-all-start.2 = ((bf16[8,3,64,256]{3,2,1,0:T(8,128)(2,1)}), bf16[8,3,64,256]{3,2,1,0:T(8,128)(2,1)}, u32[]{:S(2)}, u32[]{:S(2)}) async-start(bf16[8,3,64,256]{3,2,1,0:T(8,128)(2,1)} %bitcast.78), calls=%async_computation.2 | async-start | bytes 1572864 | tf_op jit(solution)/shard_map/all_to_all | solution.py:84
  52.1 6.2 %convolution_convert_fusion.1 = bf16[1024,512]{1,0:T(8,128)(2,1)} fusion(bf16[1024,2048]{1,0:T(8,128)(2,1)} %bitcast.82, bf16[2048,512]{1,0:T(8,128)(2,1)} %param.10), kind=kOutput, calls=%fused_computation.34 | convolution fusion | flops 2148007936 | bytes 7340032 | tf_op jit(solution)/shard_map/dot_general | solution.py:54
  64.8 6.6 %all-to-all-done.2 = bf16[8,3,64,256]{3,2,1,0:T(8,128)(2,1)} async-done(((bf16[8,3,64,256]{3,2,1,0:T(8,128)(2,1)}), bf16[8,3,64,256]{3,2,1,0:T(8,128)(2,1)}, u32[]{:S(2)}, u32[]{:S(2)}) %all-to-all-start.2) | async-done | bytes 786464 | tf_op jit(solution)/shard_map/all_to_all | solution.py:84
  73.8 175.5 %while.11 = (s32[]{:T(128)}, bf16[4,4,64,2,2,128]{5,4,3,2,1,0:T(2,128)(2,1)}, s32[4]{0:T(128)}, s32[4,4,32]{2,1,0:T(4,128)S(1)}, bf16[40,64,256]{2,1,0:T(8,128)(...) while((s32[]{:T(128)}, ...), condition=%wide.region_8.9_spmd.clone, body=%wide.region_5.8_spmd.clone.sunk | while | flops 1093415040 | bytes 80374576 | solution.py:120
  78.2 4.1 %gather_fusion = bf16[128,64,256]{2,1,0:T(8,128)(2,1)} fusion(bf16[40,64,256]{2,1,0:T(8,128)(2,1)} %get-tuple-element.247, s32[1024]{0:T(1024)S(1)} %pad_clamp_fusion.3), kind=kCustom, calls=%fused_computation.1.clone.clone.1 | custom fusion | bytes 8389120 | tf_op jit(solution)/shard_map/while/body/eval_jaxpr/gather | solution.py:107
  82.3 6.9 %reshape.252 = bf16[4,2048,2,128]{3,2,1,0:T(2,128)(2,1)} reshape(bf16[128,64,256]{2,1,0:T(8,128)(2,1)} %gather_fusion) | data formatting | bytes 8388608 | tf_op jit(solution)/shard_map/while/body/eval_jaxpr/reshape | solution.py:107
  90.3 3.5 %fusion.43 = f32[4,2,2048,64,2]{2,3,4,1,0:T(8,128)S(1)} fusion(bf16[4,2048,2,128,1]{3,2,1,0,4:T(2,128)(2,1)} %bitcast.71, bf16[1,4,64,2,2,128]{5,4,3,2,1,0:T(2,128)(2,1)S(1)} %constant_dynamic-slice_fusion.2), kind=kOutput, calls=%fused_computation.10.clone.1 | convolution fusion | flops 536870912 | bytes 12845056 | tf_op jit(solution)/shard_map/while/body/eval_jaxpr/nqkgd,npkd->nkgqp/dot_general | solution.py:24
  93.9 5.9 %fusion.44 = (f32[4,2,2,64]{3,2,1,0:T(2,128)}, f32[4,2,2,64,2048]{4,3,2,1,0:T(8,128)}) fusion(f32[4,2,2048,64,2]{2,3,4,1,0:T(8,128)S(1)} %fusion.43, pred[4,64,2048]{2,1,0:T(8,128)(4,1)S(1)} %copy-done.1), kind=kOutput, calls=%fused_computation.68.clone.1 | output fusion | flops 12584959 | bytes 17305600 | tf_op jit(solution)/shard_map/while/body/eval_jaxpr/sub | solution.py:35
  103.9 6.9 %reshape.253 = bf16[4,2048,2,128]{3,2,1,0:T(2,128)(2,1)} reshape(bf16[128,64,256]{2,1,0:T(8,128)(2,1)} %gather_fusion.1) | data formatting | bytes 8388608 | tf_op jit(solution)/shard_map/while/body/eval_jaxpr/reshape | solution.py:108
  110.8 5.9 %fusion.45 = bf16[1,4,64,2,2,128]{5,2,4,3,1,0:T(8,128)(2,1)S(1)} fusion(f32[4,2,2,64,2048]{4,3,2,1,0:T(8,128)} %get-tuple-element.216, f32[4,2,2,64]{3,2,1,0:T(2,128)} %get-tuple-element.217, bf16[4,2048,2,128,1]{3,2,1,0,4:T(2,128)(2,1)} %bitcast.72, pred[4,64]{1,0:T(4,128)(4,1)S(1)} %broadcast_compare_fusion.6), kind=kOutput, calls=%fused_computation.20.clone.1 | convolution fusion | flops 541327360 | bytes 12849408 | tf_op jit(solution)/shard_map/while/body/eval_jaxpr/nkgqp,npkd->nqkgd/dot_general | solution.py:37
  122.1 4.1 %gather_fusion = bf16[128,64,256]{2,1,0:T(8,128)(2,1)} fusion(bf16[40,64,256]{2,1,0:T(8,128)(2,1)} %get-tuple-element.247, s32[1024]{0:T(1024)S(1)} %pad_clamp_fusion.3), kind=kCustom, calls=%fused_computation.1.clone.clone.1 | custom fusion | bytes 8389120 | tf_op jit(solution)/shard_map/while/body/eval_jaxpr/gather | solution.py:107
  126.2 6.9 %reshape.252 = bf16[4,2048,2,128]{3,2,1,0:T(2,128)(2,1)} reshape(bf16[128,64,256]{2,1,0:T(8,128)(2,1)} %gather_fusion) | data formatting | bytes 8388608 | tf_op jit(solution)/shard_map/while/body/eval_jaxpr/reshape | solution.py:107
  137.7 5.9 %fusion.44 = (f32[4,2,2,64]{3,2,1,0:T(2,128)}, f32[4,2,2,64,2048]{4,3,2,1,0:T(8,128)}) fusion(f32[4,2,2048,64,2]{2,3,4,1,0:T(8,128)S(1)} %fusion.43, pred[4,64,2048]{2,1,0:T(8,128)(4,1)S(1)} %copy-done.1), kind=kOutput, calls=%fused_computation.68.clone.1 | output fusion | flops 12584959 | bytes 17305600 | tf_op jit(solution)/shard_map/while/body/eval_jaxpr/sub | solution.py:35
  147.8 6.9 %reshape.253 = bf16[4,2048,2,128]{3,2,1,0:T(2,128)(2,1)} reshape(bf16[128,64,256]{2,1,0:T(8,128)(2,1)} %gather_fusion.1) | data formatting | bytes 8388608 | tf_op jit(solution)/shard_map/while/body/eval_jaxpr/reshape | solution.py:108
  154.7 5.9 %fusion.45 = bf16[1,4,64,2,2,128]{5,2,4,3,1,0:T(8,128)(2,1)S(1)} fusion(f32[4,2,2,64,2048]{4,3,2,1,0:T(8,128)} %get-tuple-element.216, f32[4,2,2,64]{3,2,1,0:T(2,128)} %get-tuple-element.217, bf16[4,2048,2,128,1]{3,2,1,0,4:T(2,128)(2,1)} %bitcast.72, pred[4,64]{1,0:T(4,128)(4,1)S(1)} %broadcast_compare_fusion.6), kind=kOutput, calls=%fused_computation.20.clone.1 | convolution fusion | flops 541327360 | bytes 12849408 | tf_op jit(solution)/shard_map/while/body/eval_jaxpr/nkgqp,npkd->nqkgd/dot_general | solution.py:37
  166.0 4.1 %gather_fusion = bf16[128,64,256]{2,1,0:T(8,128)(2,1)} fusion(bf16[40,64,256]{2,1,0:T(8,128)(2,1)} %get-tuple-element.247, s32[1024]{0:T(1024)S(1)} %pad_clamp_fusion.3), kind=kCustom, calls=%fused_computation.1.clone.clone.1 | custom fusion | bytes 8389120 | tf_op jit(solution)/shard_map/while/body/eval_jaxpr/gather | solution.py:107
  170.0 6.9 %reshape.252 = bf16[4,2048,2,128]{3,2,1,0:T(2,128)(2,1)} reshape(bf16[128,64,256]{2,1,0:T(8,128)(2,1)} %gather_fusion) | data formatting | bytes 8388608 | tf_op jit(solution)/shard_map/while/body/eval_jaxpr/reshape | solution.py:107
  181.6 5.9 %fusion.44 = (f32[4,2,2,64]{3,2,1,0:T(2,128)}, f32[4,2,2,64,2048]{4,3,2,1,0:T(8,128)}) fusion(f32[4,2,2048,64,2]{2,3,4,1,0:T(8,128)S(1)} %fusion.43, pred[4,64,2048]{2,1,0:T(8,128)(4,1)S(1)} %copy-done.1), kind=kOutput, calls=%fused_computation.68.clone.1 | output fusion | flops 12584959 | bytes 17305600 | tf_op jit(solution)/shard_map/while/body/eval_jaxpr/sub | solution.py:35
  191.7 6.9 %reshape.253 = bf16[4,2048,2,128]{3,2,1,0:T(2,128)(2,1)} reshape(bf16[128,64,256]{2,1,0:T(8,128)(2,1)} %gather_fusion.1) | data formatting | bytes 8388608 | tf_op jit(solution)/shard_map/while/body/eval_jaxpr/reshape | solution.py:108
  198.6 5.9 %fusion.45 = bf16[1,4,64,2,2,128]{5,2,4,3,1,0:T(8,128)(2,1)S(1)} fusion(f32[4,2,2,64,2048]{4,3,2,1,0:T(8,128)} %get-tuple-element.216, f32[4,2,2,64]{3,2,1,0:T(2,128)} %get-tuple-element.217, bf16[4,2048,2,128,1]{3,2,1,0,4:T(2,128)(2,1)} %bitcast.72, pred[4,64]{1,0:T(4,128)(4,1)S(1)} %broadcast_compare_fusion.6), kind=kOutput, calls=%fused_computation.20.clone.1 | convolution fusion | flops 541327360 | bytes 12849408 | tf_op jit(solution)/shard_map/while/body/eval_jaxpr/nkgqp,npkd->nqkgd/dot_general | solution.py:37
  209.9 4.1 %gather_fusion = bf16[128,64,256]{2,1,0:T(8,128)(2,1)} fusion(bf16[40,64,256]{2,1,0:T(8,128)(2,1)} %get-tuple-element.247, s32[1024]{0:T(1024)S(1)} %pad_clamp_fusion.3), kind=kCustom, calls=%fused_computation.1.clone.clone.1 | custom fusion | bytes 8389120 | tf_op jit(solution)/shard_map/while/body/eval_jaxpr/gather | solution.py:107
  213.9 6.9 %reshape.252 = bf16[4,2048,2,128]{3,2,1,0:T(2,128)(2,1)} reshape(bf16[128,64,256]{2,1,0:T(8,128)(2,1)} %gather_fusion) | data formatting | bytes 8388608 | tf_op jit(solution)/shard_map/while/body/eval_jaxpr/reshape | solution.py:107
  225.5 5.9 %fusion.44 = (f32[4,2,2,64]{3,2,1,0:T(2,128)}, f32[4,2,2,64,2048]{4,3,2,1,0:T(8,128)}) fusion(f32[4,2,2048,64,2]{2,3,4,1,0:T(8,128)S(1)} %fusion.43, pred[4,64,2048]{2,1,0:T(8,128)(4,1)S(1)} %copy-done.1), kind=kOutput, calls=%fused_computation.68.clone.1 | output fusion | flops 12584959 | bytes 17305600 | tf_op jit(solution)/shard_map/while/body/eval_jaxpr/sub | solution.py:35
  235.5 6.9 %reshape.253 = bf16[4,2048,2,128]{3,2,1,0:T(2,128)(2,1)} reshape(bf16[128,64,256]{2,1,0:T(8,128)(2,1)} %gather_fusion.1) | data formatting | bytes 8388608 | tf_op jit(solution)/shard_map/while/body/eval_jaxpr/reshape | solution.py:108
  242.5 5.9 %fusion.45 = bf16[1,4,64,2,2,128]{5,2,4,3,1,0:T(8,128)(2,1)S(1)} fusion(f32[4,2,2,64,2048]{4,3,2,1,0:T(8,128)} %get-tuple-element.216, f32[4,2,2,64]{3,2,1,0:T(2,128)} %get-tuple-element.217, bf16[4,2048,2,128,1]{3,2,1,0,4:T(2,128)(2,1)} %bitcast.72, pred[4,64]{1,0:T(4,128)(4,1)S(1)} %broadcast_compare_fusion.6), kind=kOutput, calls=%fused_computation.20.clone.1 | convolution fusion | flops 541327360 | bytes 12849408 | tf_op jit(solution)/shard_map/while/body/eval_jaxpr/nkgqp,npkd->nqkgd/dot_general | solution.py:37
  250.9 4.3 %convolution_convert_fusion = bf16[1024,2048]{1,0:T(8,128)(2,1)} fusion(bf16[1024,512]{1,0:T(8,128)(2,1)S(1)} %reshape.192, bf16[512,2048]{1,0:T(8,128)(2,1)S(1)} %copy-done), kind=kOutput, calls=%fused_computation.33 | convolution fusion | flops 2149580800 | bytes 7340032 | tf_op jit(solution)/shard_map/dot_general | solution.py:122
  255.2 43.6 %reduce-scatter.2.cloned.1.call-done = bf16[4,256,512]{2,1,0:T(8,128)(2,1)} async-done(((bf16[4,256,2048]{2,1,0:T(8,128)(2,1)}), bf16[4,256,512]{2,1,0:T(8,128)(2,1)}) %reduce-scatter.2.cloned.1.call-update) | async-done | bytes 1048592 | tf_op jit(solution)/shard_map/reduce_scatter | solution.py:130
  (118 shorter events, 71.9 us)
Async XLA Ops:
  6.5 244.3 %copy-start = (bf16[512,2048]{1,0:T(8,128)(2,1)S(1)}, bf16[512,2048]{1,0:T(8,128)(2,1)}, u32[]{:S(2)}) copy-start(bf16[512,2048]{1,0:T(8,128)(2,1)} %param.13) | copy-start | bytes 6291460
  8.9 13.7 %all-to-all-start = ((s32[8,1,3]{2,1,0:T(1,128)}), s32[8,1,3]{2,1,0:T(1,128)S(1)}, u32[]{:S(2)}, u32[]{:S(2)}) async-start(s32[8,1,3]{2,1,0:T(1,128)} %copy.26), calls=%async_computation | async-start | bytes 8192 | tf_op jit(solution)/shard_map/all_to_all | solution.py:82
  19.9 12.4 %copy-start.2 = (bf16[1024,256]{1,0:T(8,128)(2,1)}, bf16[1024,256]{1,0:T(8,128)(2,1)S(1)}, u32[]{:S(2)}) copy-start(bf16[1024,256]{1,0:T(8,128)(2,1)S(1)} %convolution_convert_fusion.3) | copy-start | bytes 1572868
  24.4 23.3 %all-to-all-start.1 = ((bf16[8,3,64,256]{3,2,1,0:T(8,128)(2,1)}), bf16[8,3,64,256]{3,2,1,0:T(8,128)(2,1)}, u32[]{:S(2)}, u32[]{:S(2)}) async-start(bf16[8,3,64,256]{3,2,1,0:T(8,128)(2,1)} %bitcast.4), calls=%async_computation.1 | async-start | bytes 1572864 | tf_op jit(solution)/shard_map/all_to_all | solution.py:85
  32.3 26.0 %copy-start.3 = (bf16[1024,256]{1,0:T(8,128)(2,1)}, bf16[1024,256]{1,0:T(8,128)(2,1)S(1)}, u32[]{:S(2)}) copy-start(bf16[1024,256]{1,0:T(8,128)(2,1)S(1)} %convolution_convert_fusion.2) | copy-start | bytes 1572868
  47.7 23.7 %all-to-all-start.2 = ((bf16[8,3,64,256]{3,2,1,0:T(8,128)(2,1)}), bf16[8,3,64,256]{3,2,1,0:T(8,128)(2,1)}, u32[]{:S(2)}, u32[]{:S(2)}) async-start(bf16[8,3,64,256]{3,2,1,0:T(8,128)(2,1)} %bitcast.78), calls=%async_computation.2 | async-start | bytes 1572864 | tf_op jit(solution)/shard_map/all_to_all | solution.py:84
  51.9 9.4 %copy-start.4 = (s32[4,4,32]{2,1,0:T(4,128)S(1)}, s32[4,4,32]{2,1,0:T(4,128)}, u32[]{:S(2)}) copy-start(s32[4,4,32]{2,1,0:T(4,128)} %param.14) | copy-start | bytes 6148
  51.9 246.8 %reduce-scatter.2.cloned.1.call-start = ((), (), s32[]{:S(2)}) async-start(), calls=%async_computation.4 | async-start | bytes 5242880 | tf_op jit(solution)/shard_map/reduce_scatter | solution.py:130
  63.3 10.5 %copy-start.5 = (s32[4]{0:T(128)S(1)}, s32[4]{0:T(128)}, u32[]{:S(2)}) copy-start(s32[4]{0:T(128)} %add_multiply_fusion) | copy-start | bytes 52
  90.3 3.5 %copy-start.1 = (pred[4,64,2048]{2,1,0:T(8,128)(4,1)S(1)}, pred[4,64,2048]{2,1,0:T(8,128)(4,1)}, u32[]{:S(2)}) copy-start(pred[4,64,2048]{2,1,0:T(8,128)(4,1)} %compare_or_fusion.2) | copy-start | bytes 1572868 | tf_op jit(solution)/shard_map/while
  110.8 6.9 %copy-start.6 = (s32[4]{0:T(128)S(1)}, s32[4]{0:T(128)}, u32[]{:S(2)}) copy-start(s32[4]{0:T(128)} %get-tuple-element.268) | copy-start | bytes 52 | tf_op jit(solution)/shard_map/while
  134.2 3.5 %copy-start.1 = (pred[4,64,2048]{2,1,0:T(8,128)(4,1)S(1)}, pred[4,64,2048]{2,1,0:T(8,128)(4,1)}, u32[]{:S(2)}) copy-start(pred[4,64,2048]{2,1,0:T(8,128)(4,1)} %compare_or_fusion.2) | copy-start | bytes 1572868 | tf_op jit(solution)/shard_map/while
  154.7 6.9 %copy-start.6 = (s32[4]{0:T(128)S(1)}, s32[4]{0:T(128)}, u32[]{:S(2)}) copy-start(s32[4]{0:T(128)} %get-tuple-element.268) | copy-start | bytes 52 | tf_op jit(solution)/shard_map/while
  178.1 3.5 %copy-start.1 = (pred[4,64,2048]{2,1,0:T(8,128)(4,1)S(1)}, pred[4,64,2048]{2,1,0:T(8,128)(4,1)}, u32[]{:S(2)}) copy-start(pred[4,64,2048]{2,1,0:T(8,128)(4,1)} %compare_or_fusion.2) | copy-start | bytes 1572868 | tf_op jit(solution)/shard_map/while
  198.6 6.9 %copy-start.6 = (s32[4]{0:T(128)S(1)}, s32[4]{0:T(128)}, u32[]{:S(2)}) copy-start(s32[4]{0:T(128)} %get-tuple-element.268) | copy-start | bytes 52 | tf_op jit(solution)/shard_map/while
  222.0 3.5 %copy-start.1 = (pred[4,64,2048]{2,1,0:T(8,128)(4,1)S(1)}, pred[4,64,2048]{2,1,0:T(8,128)(4,1)}, u32[]{:S(2)}) copy-start(pred[4,64,2048]{2,1,0:T(8,128)(4,1)} %compare_or_fusion.2) | copy-start | bytes 1572868 | tf_op jit(solution)/shard_map/while
  242.5 6.9 %copy-start.6 = (s32[4]{0:T(128)S(1)}, s32[4]{0:T(128)}, u32[]{:S(2)}) copy-start(s32[4]{0:T(128)} %get-tuple-element.268) | copy-start | bytes 52 | tf_op jit(solution)/shard_map/while
Sparse Core Ops, SparseCore 0:
  255.3 43.3 reduce-scatter.1
where the time goes:
time: 308 us; the launch traced here: 306 us
  local copies, waits for them, and re-layouts  109 us (35%)
  waiting for transfers between devices  66.7 us (22%)
  matrix products  55.6 us (18%)
  other arithmetic  45 us (15%)
  starting transfers between devices  15.9 us (5%)
  between operations  13.5 us (4%)
    reduce_scatter x1, waiting for transfers between devices, shards(): lax.psum_scatter(partial_value.astype(jnp.bfloat16), 'tp', scatter_dimens...  43.6 us
    reshape x4, local copies, waits for them, and re-layouts, one_seq(): value_sets = value_table[seq_rows].reshape(per_dev, TOPK * KB, kv_local, HD)  27.7 us
    reshape x4, local copies, waits for them, and re-layouts, one_seq(): key_sets = key_table[seq_rows].reshape(per_dev, TOPK * KB, kv_local, HD)  27.7 us
    dot_general x4, matrix products, attend(): jnp.einsum('nkgqp,npkd->nqkgd', weights, value_sets, preferred_element_ty...  23.6 us
    sub x4, other arithmetic, attend(): raised = jnp.exp(scores - highest)  23.5 us
    gather x4, local copies, waits for them, and re-layouts, one_seq(): key_sets = key_table[seq_rows].reshape(per_dev, TOPK * KB, kv_local, HD)  16.2 us
    dot_general x4, matrix products, attend(): jnp.einsum('nqkgd,npkd->nkgqp', queries, key_sets, preferred_element_type...  14 us
    all_to_all x1, waiting for transfers between devices, shards(): lax.all_to_all(value_rows[asked], 'kv', split_axis=0, concat_axis=0, tile...  13.8 us
  transfers between devices with their start and end apart: 4, of which 4 were waited for; matrix products, arithmetic and copies ran while one was open for 7% of the time, Pallas kernels for 0%

commit v1 on v0

v1 whole, which is shorter than its diff:
```python
import math

import jax
import jax.numpy as jnp
from jax import lax
from jax.experimental import pallas as pl
from jax.experimental.pallas import tpu as pltpu
from jax.sharding import PartitionSpec as P

HD = 128
KB = 64
CORES = 2
SCALE = HD ** (-0.5) * math.log2(math.e)


ANY = pl.BlockSpec(memory_space=pl.ANY)
SMEM = pl.BlockSpec(memory_space=pltpu.SMEM)
VMEM = pl.BlockSpec(memory_space=pltpu.VMEM)


def nth_longest(len_ref, tier):
    batch = len_ref.shape[0]
    found = jnp.int32(0)
    for b in range(batch):
        rank = jnp.int32(0)
        for other in range(batch):
            if other < b:
                rank += (len_ref[other] >= len_ref[b]).astype(jnp.int32)
            elif other > b:
                rank += (len_ref[other] > len_ref[b]).astype(jnp.int32)
        found = jnp.where(rank == tier, b, found)
    return found


def cost(flops, moved):
    return pl.CostEstimate(flops=int(flops), bytes_accessed=int(moved), transcendentals=0)


def first_kv(lengths, rows, wk, wv):
    _, span, width = rows.shape
    kv_width = wk.shape[1]
    tiles = 4
    depth = width // tiles

    def body(len_ref, x_ref, k_ref, v_ref, out_ref, x, k, v, acc, sem):
        seq = nth_longest(len_ref, 0)
        alive = lax.axis_index("kv") * span < len_ref[seq]

        @pl.when(alive)
        def _():
            def copies(t):
                part = pl.ds(pl.multiple_of(t * depth, depth), depth)
                return (
                    pltpu.make_async_copy(k_ref.at[part], k.at[t], sem.at[3 * t]),
                    pltpu.make_async_copy(v_ref.at[part], v.at[t], sem.at[3 * t + 1]),
                    pltpu.make_async_copy(x_ref.at[seq, :, part], x.at[t], sem.at[3 * t + 2]),
                )

            for t in range(tiles):
                for copy in copies(t):
                    copy.start()
            acc[...] = jnp.zeros_like(acc)

            @pl.loop(0, tiles)
            def _(t):
                for copy in copies(t):
                    copy.wait()
                acc[:, :kv_width] += jnp.dot(x[t], k[t], preferred_element_type=jnp.float32)
                acc[:, kv_width:] += jnp.dot(x[t], v[t], preferred_element_type=jnp.float32)

            out_ref[...] = acc[...].astype(out_ref.dtype)

    return pl.pallas_call(
        body,
        in_specs=[SMEM, ANY, ANY, ANY],
        out_specs=VMEM,
        out_shape=jax.ShapeDtypeStruct((span, 2 * kv_width), jnp.bfloat16),
        scratch_shapes=[
            pltpu.VMEM((tiles, span, depth), jnp.bfloat16),
            pltpu.VMEM((tiles, depth, kv_width), jnp.bfloat16),
            pltpu.VMEM((tiles, depth, kv_width), jnp.bfloat16),
            pltpu.VMEM((span, 2 * kv_width), jnp.float32),
            pltpu.SemaphoreType.DMA((3 * tiles,)),
        ],
        cost_estimate=cost(4 * span * width * kv_width, 3 << 20),
        name="first_kv",
    )(lengths, rows, wk, wv)


def other_qkv(lengths, rows, wq, wk, wv, after):
    batch, span, width = rows.shape
    kv_width = wk.shape[1]
    q_width = wq.shape[1]

    def body(len_ref, x_ref, q_ref, k_ref, v_ref, _, *rest):
        q_outs, kv_outs = rest[:batch], rest[batch : 2 * batch - 1]
        x, wqs, wks, wvs, q, kv, sem, out_sem = rest[2 * batch - 1 :]
        here = lax.axis_index("kv")
        seqs = [nth_longest(len_ref, tier) for tier in range(batch)]
        alive = [here * span < len_ref[seq] for seq in seqs]
        weights = [
            pltpu.make_async_copy(ref, buf, sem.at[batch + i])
            for i, (ref, buf) in enumerate(((q_ref, wqs), (k_ref, wks), (v_ref, wvs)))
        ]
        inbound = [
            pltpu.make_async_copy(x_ref.at[seqs[tier]], x.at[tier], sem.at[tier])
            for tier in range(batch)
        ]
        q_out = [
            pltpu.make_async_copy(q.at[tier], q_outs[tier], out_sem.at[tier])
            for tier in range(batch)
        ]
        kv_out = [
            pltpu.make_async_copy(kv.at[tier], kv_outs[tier - 1], out_sem.at[batch + tier])
            for tier in range(1, batch)
        ]
        tiers = [*range(1, batch), 0]

        @pl.when(alive[0])
        def _():
            for copy in weights:
                copy.start()
            for tier in tiers:

                @pl.when(alive[tier])
                def _():
                    inbound[tier].start()

            for copy in weights:
                copy.wait()

        @pl.loop(0, batch)
        def _(step):
            tier = lax.rem(step + 1, batch)

            @pl.when(here * span < len_ref[nth_longest(len_ref, tier)])
            def _():
                pltpu.make_async_copy(x_ref.at[0], x.at[tier], sem.at[tier]).wait()
                q[tier] = jnp.dot(
                    x[tier], wqs[...], preferred_element_type=jnp.float32
                ).astype(q.dtype)
                kv[tier, :, :kv_width] = jnp.dot(
                    x[tier], wks[...], preferred_element_type=jnp.float32
                ).astype(kv.dtype)
                kv[tier, :, kv_width:] = jnp.dot(
                    x[tier], wvs[...], preferred_element_type=jnp.float32
                ).astype(kv.dtype)
                for t in range(batch):

                    @pl.when(tier == t)
                    def _():
                        q_out[t].start()
                        if t > 0:
                            kv_out[t - 1].start()

        for tier in tiers:

            @pl.when(alive[tier])
            def _():
                if tier > 0:
                    kv_out[tier - 1].wait()
                q_out[tier].wait()

    outs = pl.pallas_call(
        body,
        in_specs=[SMEM, ANY, ANY, ANY, ANY, ANY],
        out_specs=[ANY] * (2 * batch - 1),
        out_shape=[jax.ShapeDtypeStruct((span, q_width), jnp.bfloat16)] * batch
        + [jax.ShapeDtypeStruct((span, 2 * kv_width), jnp.bfloat16)] * (batch - 1),
        scratch_shapes=[
            pltpu.VMEM((batch, span, width), jnp.bfloat16),
            pltpu.VMEM((width, q_width), jnp.bfloat16),
            pltpu.VMEM((width, kv_width), jnp.bfloat16),
            pltpu.VMEM((width, kv_width), jnp.bfloat16),
            pltpu.VMEM((batch, span, q_width), jnp.bfloat16),
            pltpu.VMEM((batch, span, 2 * kv_width), jnp.bfloat16),
            pltpu.SemaphoreType.DMA((batch + 3,)),
            pltpu.SemaphoreType.DMA((2 * batch,)),
        ],
        cost_estimate=cost(2 * batch * span * width * (q_width + 2 * kv_width), 8 << 20),
        name="other_qkv",
    )(lengths, rows, wq, wk, wv, after)
    return outs[:batch], outs[batch:]


def attend(tiers, columns, lengths, chosen, queries, own_kv, slabs, wo, parts, after=()):
    group = len(tiers)
    span, q_width = queries[0].shape
    blocks = span // KB
    kv_width = own_kv[0].shape[-1] // 2
    kv_heads = kv_width // HD
    per = q_width // kv_width
    width = wo.shape[1]
    piece = width // (parts * CORES)
    names = chosen.shape[2]
    spread = jnp.repeat(jnp.swapaxes(chosen, 1, 2), KB, axis=2)
    devices = lax.axis_size("kv")
    most = max(len(part) for part in slabs)
    room = (most + 1) * blocks
    arrays = [array for part in slabs for array, _, _ in part]

    def body(len_ref, pick_ref, names_ref, *rest):
        q_hbm, kv_hbm = rest[:group], rest[group : 2 * group]
        rest = rest[2 * group :]
        slab_refs = rest[: len(arrays)]
        w_hbm = rest[len(arrays)]
        rest = rest[len(arrays) + 1 + len(after) :]
        keep_hbm, give_hbm, q_ref, w_ref, packed, top, low, acc, att, mask, out = rest[:11]
        marks, listed, count, q_sem, kv_sem, w_sem, slot_sem, out_sem = rest[11:]
        here = lax.axis_index("kv")
        member = lax.axis_index("tp")
        y, core = lax.div(member, CORES), lax.rem(member, CORES)
        row, column = lax.div(here, columns), lax.rem(here, columns)
        load_w = pltpu.make_async_copy(w_hbm, w_ref, w_sem)
        any_alive = here * span < len_ref[nth_longest(len_ref, min(tiers))]

        @pl.when(any_alive)
        def _():
            load_w.start()

        def stores(g, side, far):
            return pltpu.make_async_copy(
                out.at[g, side, far],
                (give_hbm, keep_hbm)[side].at[far, g],
                out_sem.at[g, side, far],
            )

        def one(g, tier):
            seq = nth_longest(len_ref, tier)
            length = len_ref[seq]

            @pl.when(here * span < length)
            def _():
                for i in range(group):

                    @pl.when(g == i)
                    def _():
                        pltpu.make_async_copy(q_hbm[i], q_ref, q_sem).start()
                        pltpu.make_async_copy(
                            kv_hbm[i], packed.at[pl.ds(0, span)], kv_sem
                        ).start()

                for c in range(blocks):
                    listed[c] = here * blocks + c
                count[0] = blocks
                if arrays:

                    @pl.when(here > 0)
                    def _():
                        @pl.loop(0, devices * blocks, unroll=8)
                        def _(b):
                            marks[b] = 0

                        @pl.loop(0, names, unroll=4)
                        def _(t):
                            for i in range(blocks):
                                marks[pick_ref[seq, i, t]] = 1

                    at = 0
                    for i in range(group):
                        for _, back, turned in slabs[i]:
                            ref = slab_refs[at]
                            at += 1
                            source = (row - back) * columns + lax.rem(
                                column - turned + columns, columns
                            )

                            @pl.when((g == i) & (row >= back) & (source < here))
                            def _():
                                @pl.loop(0, blocks)
                                def _(c):
                                    @pl.when(marks[source * blocks + c] > 0)
                                    def _():
                                        slot = count[0]
                                        listed[slot] = source * blocks + c
                                        count[0] = slot + 1
                                        pltpu.make_async_copy(
                                            ref.at[pl.ds(pl.multiple_of(c * KB, KB), KB)],
                                            packed.at[pl.ds(pl.multiple_of(slot * KB, KB), KB)],
                                            slot_sem.at[slot],
                                        ).start()

                picked = names_ref[seq]
                own_id = here * blocks + lax.broadcasted_iota(jnp.int32, (1, span), 1) // KB
                times = jnp.sum((picked == own_id).astype(jnp.float32), axis=0, keepdims=True)
                extra = jnp.log2(times) * (1.0 / SCALE)
                top[...] = jnp.full_like(top, -jnp.inf)
                low[...] = jnp.zeros_like(low)
                acc[...] = jnp.zeros_like(acc)
                pltpu.make_async_copy(q_hbm[0], q_ref, q_sem).wait()
                pltpu.make_async_copy(kv_hbm[0], packed.at[pl.ds(0, span)], kv_sem).wait()
                found = count[0]
                chunks = lax.div(found + blocks - 1, blocks)

                @pl.loop(0, chunks)
                def _(chunk):
                    @pl.when(chunk == 1)
                    def _():
                        @pl.loop(found, chunks * blocks)
                        def _(slot):
                            listed[slot] = -1
                            packed[pl.ds(pl.multiple_of(slot * KB, KB), KB), :] = jnp.zeros(
                                (KB, 2 * kv_width), packed.dtype
                            )

                        @pl.loop(blocks, found)
                        def _(slot):
                            pltpu.make_async_copy(
                                kv_hbm[0].at[pl.ds(0, KB)],
                                packed.at[pl.ds(pl.multiple_of(slot * KB, KB), KB)],
                                slot_sem.at[slot],
                            ).wait()

                    query = lax.broadcasted_iota(jnp.int32, (KB, span), 1)
                    for c in range(blocks):
                        named = picked == listed[chunk * blocks + c]
                        named = jnp.max(jnp.where(named, 0.0, -jnp.inf), axis=0, keepdims=True)
                        key = c * KB + lax.broadcasted_iota(jnp.int32, (KB, span), 0)
                        key = jnp.where(chunk == 0, key, -1)
                        part = jnp.where(key == query, extra, named)
                        mask[c] = jnp.where(key <= query, part, -jnp.inf)
                    at = pl.ds(pl.multiple_of(chunk * span, span), span)
                    for head in range(kv_heads):
                        base = head * per * HD
                        rows = jnp.concatenate(
                            [q_ref[:, base + k * HD : base + (k + 1) * HD] for k in range(per)],
                            axis=0,
                        )
                        s = lax.dot_general(
                            packed[at, head * HD : (head + 1) * HD],
                            rows,
                            (((1,), (1,)), ((), ())),
                            preferred_element_type=jnp.float32,
                        )
                        bias = mask[...].reshape(span, span)
                        s = s + jnp.concatenate([bias] * per, axis=1)
                        old = top[head]
                        high = jnp.maximum(old, jnp.max(s, axis=0, keepdims=True))
                        e = jnp.exp2((s - high) * SCALE)
                        fade = jnp.exp2((old - high) * SCALE)
                        top[head] = high
                        low[head] = low[head] * fade + jnp.sum(e, axis=0, keepdims=True)
                        acc[head] = acc[head] * fade + lax.dot_general(
                            packed[at, kv_width + head * HD : kv_width + (head + 1) * HD],
                            e.astype(jnp.bfloat16),
                            (((0,), (0,)), ((), ())),
                            preferred_element_type=jnp.float32,
                        )

                living = here * span + lax.broadcasted_iota(jnp.int32, (span, 1), 0) < length
                for head in range(kv_heads):
                    done = acc[head] * (1.0 / low[head])
                    for k in range(per):
                        col = (head * per + k) * HD
                        att[:, col : col + HD] = jnp.where(
                            living, done[:, k * span : (k + 1) * span].T, 0.0
                        ).astype(att.dtype)

                @pl.when((g == 0) | (here * span >= len_ref[nth_longest(len_ref, tier + 1)]))
                def _():
                    load_w.wait()

                for side in range(CORES):
                    mine = (CORES - 1 - core, core)[side]

                    @pl.loop(0, parts)
                    def _(step):
                        far = parts - 1 - step
                        first = (lax.rem(y + far, parts) * CORES + mine) * piece
                        out[g, side, far] = jnp.dot(
                            att[...],
                            w_ref[:, pl.ds(pl.multiple_of(first, piece), piece)],
                            preferred_element_type=jnp.float32,
                        ).astype(out.dtype)
                        stores(g, side, far).start()

        if group == 1:
            one(0, tiers[0])
        else:

            @pl.loop(0, group)
            def _(g):
                one(g, tiers[0] - g)

        for g in range(group):

            @pl.when(here * span < len_ref[nth_longest(len_ref, tiers[g])])
            def _():
                for side in range(CORES):
                    for far in range(parts):
                        stores(g, side, far).wait()

    result = jax.ShapeDtypeStruct((parts, group, span, piece), jnp.bfloat16)
    return pl.pallas_call(
        body,
        in_specs=[SMEM, SMEM, VMEM, *[ANY] * (2 * group + len(arrays) + 1 + len(after))],
        out_specs=[ANY, ANY],
        out_shape=[result, result],
        scratch_shapes=[
            pltpu.VMEM((span, q_width), jnp.bfloat16),
            pltpu.VMEM(wo.shape, jnp.bfloat16),
            pltpu.VMEM((room * KB, 2 * kv_width), jnp.bfloat16),
            pltpu.VMEM((kv_heads, 1, per * span), jnp.float32),
            pltpu.VMEM((kv_heads, 1, per * span), jnp.float32),
            pltpu.VMEM((kv_heads, HD, per * span), jnp.float32),
            pltpu.VMEM((span, q_width), jnp.bfloat16),
            pltpu.VMEM((blocks, KB, span), jnp.float32),
            pltpu.VMEM((group, CORES, parts, span, piece), jnp.bfloat16),
            pltpu.SMEM((devices * blocks,), jnp.int32),
            pltpu.SMEM((room,), jnp.int32),
            pltpu.SMEM((1,), jnp.int32),
            pltpu.SemaphoreType.DMA,
            pltpu.SemaphoreType.DMA,
            pltpu.SemaphoreType.DMA,
            pltpu.SemaphoreType.DMA((room,)),
            pltpu.SemaphoreType.DMA((group, CORES, parts)),
        ],
        cost_estimate=cost(group * 4 * span * q_width * width, group * (3 << 20)),
    )(lengths, chosen, spread, *queries, *own_kv, *arrays, wo, *after)


def finish(lengths, batch, groups):
    _, _, span, piece = groups[0][1].shape

    def body(len_ref, *refs):
        out_ref = refs[-1]
        at = 0
        for tiers, _, _, coming in groups:
            mine = refs[at : at + 2 + len(coming)]
            at += 2 + len(coming)
            for g, tier in enumerate(tiers):
                seq = nth_longest(len_ref, tier)
                alive = lax.axis_index("kv") * span < len_ref[seq]

                @pl.when(alive)
                def _():
                    total = mine[0][0, g].astype(jnp.float32) + mine[1][0, g].astype(jnp.float32)
                    for ref in mine[2:]:
                        total = total + ref[g].astype(jnp.float32)
                    out_ref[seq] = total.astype(out_ref.dtype)

                @pl.when(jnp.logical_not(alive))
                def _():
                    out_ref[seq] = jnp.zeros((span, piece), out_ref.dtype)

    specs, operands = [SMEM], [lengths]
    for tiers, keep, got, coming in groups:
        size = len(tiers)
        near = pl.BlockSpec((1, size, span, piece), lambda i: (0, 0, 0, 0))
        flat = pl.BlockSpec((size, span, piece), lambda i: (0, 0, 0))
        specs += [near, near] + [flat] * len(coming)
        operands += [keep, got, *coming]
    return pl.pallas_call(
        body,
        grid=(1,),
        in_specs=specs,
        out_specs=pl.BlockSpec((batch, span, piece), lambda i: (0, 0, 0)),
        out_shape=jax.ShapeDtypeStruct((batch, span, piece), jnp.bfloat16),
        cost_estimate=cost(batch * 4 * span * piece, batch * 8 * span * piece),
        name="finish",
    )(*operands)


def gather_spans(slab, reach, columns):
    rows = reach // columns
    arrived = []

    def turn(x, back):
        for d in range(1, columns):
            pairs = [
                (r * columns + c, r * columns + (c + d) % columns)
                for r in range(back, rows)
                for c in range(columns)
                if r > 0 or c + d < columns
            ]
            arrived.append((lax.ppermute(x, "kv", pairs), back, d))

    turn(slab, 0)
    passing = slab
    for back in range(1, rows):
        pairs = [
            (r * columns + c, (r + 1) * columns + c)
            for r in range(back - 1, rows - 1)
            for c in range(columns)
        ]
        passing = lax.ppermute(passing, "kv", pairs)
        arrived.append((passing, back, 0))
        turn(passing, back)
    return arrived


def layer(reaches, together, columns, inputs, wq, wk, wv, wo, chosen, lengths):
    batch, _, _ = inputs.shape
    members = lax.axis_size("tp")
    parts = members // CORES

    kv0 = first_kv(lengths, inputs, wk, wv)
    queries, kv_rest = other_qkv(lengths, inputs, wq, wk, wv, kv0)
    own = [kv0, *kv_rest]
    gathered = [
        gather_spans(own[tier], reaches[tier], columns) if reaches[tier] > 1 else []
        for tier in range(batch)
    ]

    groups = []
    for tiers in together:
        reach = max(max(reaches[tier] for tier in tiers), 1)
        keep, give = attend(
            tiers,
            columns,
            lengths,
            chosen,
            [queries[tier] for tier in tiers],
            [own[tier] for tier in tiers],
            [gathered[tier] for tier in tiers],
            wo,
            parts,
        )

        def swap(x, move):
            pairs = [
                (k * members + t, k * members + move(t))
                for k in range(reach)
                for t in range(members)
            ]
            return lax.ppermute(x, ("kv", "tp"), pairs)

        got = swap(give, lambda t: t ^ 1)
        coming = []
        for far in range(1, parts):
            both = keep[far].astype(jnp.float32) + got[far].astype(jnp.float32)
            coming.append(
                swap(
                    both.astype(jnp.bfloat16),
                    lambda t, far=far: ((t // CORES + far) % parts) * CORES + t % CORES,
                )
            )
        groups.append((tiers, keep, got, coming))
    return finish(lengths, batch, groups)


def tier_reaches(devices, batch, columns):
    reaches = []
    for tier in range(batch):
        reach = devices >> tier
        if reach > 1:
            reach = -(-reach // columns) * columns
        reaches.append(reach)
    return tuple(reaches)


def solution(mesh):
    placed = (
        P(None, "kv", None),
        P(None, "tp"),
        P(None, "tp"),
        P(None, "tp"),
        P("tp", None),
        P(None, "kv", None),
        P(),
    )
    devices = mesh.shape["kv"]
    columns = 1 << ((devices.bit_length() - 1) // 2)

    def shards(*args):
        batch, span = args[0].shape[0], args[0].shape[1]
        lengths = args[-1]
        common = tier_reaches(devices, batch, columns)
        backwards = range(batch - 1, -1, -1)
        together = (tuple(backwards[:2]), *((tier,) for tier in backwards[2:]))
        out = layer(common, together, columns, *args)
        reach = jnp.array(common, jnp.int32)
        longer = jnp.sum((lengths[None, :] > reach[:, None] * span).astype(jnp.int32), axis=1)
        fits = jnp.all(longer <= jnp.arange(batch, dtype=jnp.int32))
        return lax.cond(
            fits,
            lambda done, *a: done,
            lambda done, *a: layer((devices,) * batch, (tuple(backwards),), columns, *a),
            out,
            *args,
        )

    return jax.shard_map(
        shards, mesh=mesh, in_specs=placed, out_specs=P(None, "kv", "tp"), check_vma=False
    )
```

time: 308 us -> 95.7 us (0.31)
  local copies, waits for them, and re-layouts: 109 us -> 4.35 us
  matrix products: 55.6 us -> 0 us
  waiting for transfers between devices: 66.7 us -> 24.3 us
  other arithmetic: 45 us -> 4.04 us
  Pallas kernels: 0 us -> 34.9 us
  between operations: 13.5 us -> 1.06 us
  starting transfers between devices: 15.9 us -> 26.2 us
    reshape x13 -> x1, local copies, waits for them, and re-layouts: 60 us -> 0.87 us  [attend(): spread = jnp.repeat(jnp.swapaxes(chosen, 1, 2), KB, axis=2)]
    dot_general x12 -> x0, matrix products: 55.6 us -> none  [the longest x4 23.6 us: attend(): jnp.einsum('nkgqp,npkd->nqkgd', weights, value_sets, preferred_element_ty...]
    reduce_scatter x1 -> x0, waiting for transfers between devices: 43.6 us -> none  [shards(): lax.psum_scatter(partial_value.astype(jnp.bfloat16), 'tp', scatter_dimens...]
    pallas_call x0 -> x6, Pallas kernels: none -> 34.9 us  [the longest x3 20.8 us: attend(): pl.pallas_call(body, in_specs=[SMEM, SMEM, VMEM, *[ANY] * (2 * group + le...]
    gather x10 -> x0, local copies, waits for them, and re-layouts: 30.3 us -> none  [the longest x4 16.2 us: one_seq(): key_sets = key_table[seq_rows].reshape(per_dev, TOPK * KB, kv_local, HD)]
    ppermute x0 -> x17, starting transfers between devices: none -> 26.2 us  [the longest x6 12.4 us: swap(): return lax.ppermute(x, ('kv', 'tp'), pairs)]
    ppermute x0 -> x17, waiting for transfers between devices: none -> 24.3 us  [the longest x6 16.2 us: swap(): return lax.ppermute(x, ('kv', 'tp'), pairs)]
    sub x5 -> x0, other arithmetic: 23.6 us -> none  [the longest x4 23.5 us: attend(): raised = jnp.exp(scores - highest)]
  transfers between devices with their start and end apart: 4 -> 17, of which waited for: 4 -> 4; matrix products, arithmetic and copies ran while one was open for 7% -> 5% of each run, Pallas kernels for 0% -> 22%
where the time goes in v1:
time: 95.7 us; the launch traced here: 95.1 us
  Pallas kernels  34.9 us (36%)
  starting transfers between devices  26.2 us (27%)
  waiting for transfers between devices  24.3 us (25%)
  local copies, waits for them, and re-layouts  4.35 us (5%)
  other arithmetic  4.04 us (4%)
  between operations  1.06 us (1%)
    pallas_call x3, Pallas kernels, attend(): pl.pallas_call(body, in_specs=[SMEM, SMEM, VMEM, *[ANY] * (2 * group + le...  20.8 us
    ppermute x6, waiting for transfers between devices, swap(): return lax.ppermute(x, ('kv', 'tp'), pairs)  16.2 us
    ppermute x6, starting transfers between devices, swap(): return lax.ppermute(x, ('kv', 'tp'), pairs)  12.4 us
    ppermute x7, starting transfers between devices, turn(): arrived.append((lax.ppermute(x, 'kv', pairs), back, d))  9.79 us
    pallas_call x1, Pallas kernels, other_qkv(): pl.pallas_call(body, in_specs=[SMEM, ANY, ANY, ANY, ANY, ANY], out_specs=...  7.8 us
    ppermute x4, waiting for transfers between devices, gather_spans(): passing = lax.ppermute(passing, 'kv', pairs)  4.78 us
    pallas_call x1, Pallas kernels, first_kv(): pl.pallas_call(body, in_specs=[SMEM, ANY, ANY, ANY], out_specs=VMEM, out_...  3.99 us
    ppermute x4, starting transfers between devices, gather_spans(): passing = lax.ppermute(passing, 'kv', pairs)  3.97 us
  transfers between devices with their start and end apart: 17, of which 4 were waited for; matrix products, arithmetic and copies ran while one was open for 5% of the time, Pallas kernels for 22%

profile of v1, /device:TPU:0, one launch (start us, length us, event | category | flops | bytes accessed | tf_op | source)
XLA Modules:
  0.0 95.1 jit_solution(15192007507596902922)
XLA Ops:
  0.0 4.0 %first_kv.3._.rest_1_ = bf16[256,512]{1,0:T(8,128)(2,1)} custom-call(s32[4]{0:T(128)} %len_ref.11, bf16[4,256,2048]{2,1,0:T(8,128)(2,1)} %x_ref.3, bf16[2048,256]{1,0:T(8,128)(2,1)} %k_ref.3, bf16[2048,256]{1,0:T(8,128)(2,1)} %v_ref.3), custom_call_target="tpu_custom_call" | custom-call | flops 536870912 | bytes 3145728 | tf_op jit(solution)/shard_map/first_kv/pallas_call | solution.py:73
  4.1 7.8 %other_qkv.3 = (bf16[256,512]{1,0:T(8,128)(2,1)}, bf16[256,512]{1,0:T(8,128)(2,1)}, bf16[256,512]{1,0:T(8,128)(2,1)}, bf16[256,512]{1,0:T(8,128)(2,1)}, bf16[256...) custom-call(s32[4]{0:T(128)S(1)} %copy-done.15, bf16[4,256,2048]{2,1,0:T(8,128)(2,1)} %x_ref.3, ...), custom_call_target="tpu_custom_call" | custom-call | flops 4294967296 | bytes 8388608 | tf_op jit(solution)/shard_map/other_qkv/pallas_call | solution.py:164
  11.9 2.4 %collective-permute-start.30 = (bf16[256,512]{1,0:T(8,128)(2,1)}, bf16[256,512]{1,0:T(8,128)(2,1)S(1)}, u32[]{:S(2)}, u32[]{:S(2)}) collective-permute-start(bf16[256,512]{1,0:T(8,128)(2,1)} %get-tuple-element.55.rest_3_), channel_id=1, source_target_pairs={{0,4},{1,5},{2,6},{3,7}} | collective-permute-start | bytes 786440 | tf_op jit(solution)/shard_map/ppermute | solution.py:476
  14.3 1.3 %collective-permute-start.39 = (bf16[256,512]{1,0:T(8,128)(2,1)S(1)}, bf16[256,512]{1,0:T(8,128)(2,1)S(1)}, u32[]{:S(2)}, u32[]{:S(2)}) collective-permute-start(bf16[256,512]{1,0:T(8,128)(2,1)S(1)} %copy-done.7), channel_id=1, source_target_pairs={{0,8},{4,12},{8,16},{12,20},{16,24},{20,28},{1,9},{5,13},{9,17},{1... | collective-permute-start | bytes 786440 | tf_op jit(solution)/shard_map/ppermute | solution.py:486
  15.9 0.9 reshape.91.names_ref
  16.8 3.3 %collective-permute-done.30.rest_4_ = bf16[256,512]{1,0:T(8,128)(2,1)S(1)} collective-permute-done((bf16[256,512]{1,0:T(8,128)(2,1)}, bf16[256,512]{1,0:T(8,128)(2,1)S(1)}, u32[]{:S(2)}, u32[]{:S(2)}) %collective-permute-start.30) | collective-permute-done | bytes 262176 | tf_op jit(solution)/shard_map/ppermute | solution.py:476
  20.1 0.7 copy-done.37
  20.8 9.1 %shard_map.84 = (bf16[2,2,256,512]{3,2,1,0:T(8,128)(2,1)}, bf16[2,2,256,512]{3,2,1,0:T(8,128)(2,1)}) custom-call(s32[4]{0:T(128)S(1)} %copy-done.15, s32[4,4,32]{2,1,0:T(4,128)S(1)} %copy-done.14, s32[4,32,256]{2,1,0:T(8,128)} %reshape.91.names_ref, bf16[256,512]{1,0:T(8,128)(2,1)} %get-tuple-element.52.rest_0_, bf16[256,512]{1,0:T(8,128)(2,1)} %get-tuple-element.53.rest_1_, ...), custom_call_target="tpu_custom_call" | custom-call | flops 2147483648 | bytes 6291456 | tf_op jit(solution)/shard_map/pallas_call | solution.py:394
  29.9 1.9 %collective-permute-start.31 = (bf16[2,2,256,512]{3,2,1,0:T(8,128)(2,1)}, bf16[2,2,256,512]{3,2,1,0:T(8,128)(2,1)}, u32[]{:S(2)}, u32[]{:S(2)}) collective-permute-start(bf16[2,2,256,512]{3,2,1,0:T(8,128)(2,1)} %get-tuple-element.57), channel_id=1, source_target_pairs={{0,1},{1,0},{2,3},{3,2},{4,5},{5,4},{6,7},{7,6}} | collective-permute-start | bytes 3145736 | tf_op jit(solution)/shard_map/ppermute | solution.py:526
  31.8 1.3 %collective-permute-start.34 = (bf16[256,512]{1,0:T(8,128)(2,1)}, bf16[256,512]{1,0:T(8,128)(2,1)S(1)}, u32[]{:S(2)}, u32[]{:S(2)}) collective-permute-start(bf16[256,512]{1,0:T(8,128)(2,1)} %get-tuple-element.59.rest_1_), channel_id=1, source_target_pairs={{0,8},{4,12},{1,9},{5,13},{2,10},{6,14},{3,11},{7,15}} | collective-permute-start | bytes 786440 | tf_op jit(solution)/shard_map/ppermute | solution.py:486
  33.2 0.7 collective-permute-start.41
  33.9 1.3 %collective-permute-start.33 = (bf16[256,512]{1,0:T(8,128)(2,1)}, bf16[256,512]{1,0:T(8,128)(2,1)S(1)}, u32[]{:S(2)}, u32[]{:S(2)}) collective-permute-start(bf16[256,512]{1,0:T(8,128)(2,1)} %get-tuple-element.59.rest_1_), channel_id=1, source_target_pairs={{0,4},{8,12},{12,8},{1,5},{9,13},{13,9},{2,6},{10,14},{14,10},{3,7... | collective-permute-start | bytes 786440 | tf_op jit(solution)/shard_map/ppermute | solution.py:476
  35.2 4.8 %collective-permute-done.34.rest_3_ = bf16[256,512]{1,0:T(8,128)(2,1)S(1)} collective-permute-done((bf16[256,512]{1,0:T(8,128)(2,1)}, bf16[256,512]{1,0:T(8,128)(2,1)S(1)}, u32[]{:S(2)}, u32[]{:S(2)}) %collective-permute-start.34) | collective-permute-done | bytes 262176 | tf_op jit(solution)/shard_map/ppermute | solution.py:486
  41.3 1.3 %collective-permute-start.38 = (bf16[256,512]{1,0:T(8,128)(2,1)S(1)}, bf16[256,512]{1,0:T(8,128)(2,1)S(1)}, u32[]{:S(2)}, u32[]{:S(2)}) collective-permute-start(bf16[256,512]{1,0:T(8,128)(2,1)S(1)} %copy-done.7), channel_id=1, source_target_pairs={{0,4},{8,12},{12,8},{16,20},{20,16},{24,28},{28,24},{1,5},{9,13},{... | collective-permute-start | bytes 786440 | tf_op jit(solution)/shard_map/ppermute | solution.py:476
  42.7 1.4 %collective-permute-start.40 = (bf16[256,512]{1,0:T(8,128)(2,1)S(1)}, bf16[256,512]{1,0:T(8,128)(2,1)}, u32[]{:S(2)}, u32[]{:S(2)}) collective-permute-start(bf16[256,512]{1,0:T(8,128)(2,1)S(1)} %collective-permute-done.39.rest_3_), channel_id=1, source_target_pairs={{8,12},{12,8},{16,20},{20,16},{24,28},{28,24},{9,13},{13,9},{17,21... | collective-permute-start | bytes 786440 | tf_op jit(solution)/shard_map/ppermute | solution.py:476
  44.1 1.4 %collective-permute-start.42 = (bf16[256,512]{1,0:T(8,128)(2,1)S(1)}, bf16[256,512]{1,0:T(8,128)(2,1)}, u32[]{:S(2)}, u32[]{:S(2)}) collective-permute-start(bf16[256,512]{1,0:T(8,128)(2,1)S(1)} %collective-permute-done.41.rest_5_), channel_id=1, source_target_pairs={{16,20},{20,16},{24,28},{28,24},{17,21},{21,17},{25,29},{29,25},{1... | collective-permute-start | bytes 786440 | tf_op jit(solution)/shard_map/ppermute | solution.py:476
  45.4 1.4 %collective-permute-start.44 = (bf16[256,512]{1,0:T(8,128)(2,1)S(1)}, bf16[256,512]{1,0:T(8,128)(2,1)}, u32[]{:S(2)}, u32[]{:S(2)}) collective-permute-start(bf16[256,512]{1,0:T(8,128)(2,1)S(1)} %collective-permute-done.43.rest_7_), channel_id=1, source_target_pairs={{24,28},{28,24},{25,29},{29,25},{26,30},{30,26},{27,31},{31,27}} | collective-permute-start | bytes 786440 | tf_op jit(solution)/shard_map/ppermute | solution.py:476
  46.8 5.7 %shard_map.85 = (bf16[2,1,256,512]{3,2,1,0:T(8,128)(2,1)}, bf16[2,1,256,512]{3,2,1,0:T(8,128)(2,1)}) custom-call(s32[4]{0:T(128)S(1)} %copy-done.15, s32[4,4,32]{2,1,0:T(4,128)S(1)} %copy-done.14, s32[4,32,256]{2,1,0:T(8,128)} %reshape.91.names_ref, bf16[256,512]{1,0:T(8,128)(2,1)} %get-tuple-element.58.rest_0_, bf16[256,512]{1,0:T(8,128)(2,1)} %get-tuple-element.59.rest_1_, ...), custom_call_target="tpu_custom_call" | custom-call | flops 1073741824 | bytes 3145728 | tf_op jit(solution)/shard_map/pallas_call | solution.py:394
  52.5 1.9 %collective-permute-start.36 = (bf16[2,1,256,512]{3,2,1,0:T(8,128)(2,1)}, bf16[2,1,256,512]{3,2,1,0:T(8,128)(2,1)}, u32[]{:S(2)}, u32[]{:S(2)}) collective-permute-start(bf16[2,1,256,512]{3,2,1,0:T(8,128)(2,1)} %get-tuple-element.61), channel_id=1, source_target_pairs={{0,1},{1,0},{2,3},{3,2},{4,5},{5,4},{6,7},{7,6},{8,9},{9,8},{10,11... | collective-permute-start | bytes 1572872 | tf_op jit(solution)/shard_map/ppermute | solution.py:526
  54.6 6.0 %shard_map.86 = (bf16[2,1,256,512]{3,2,1,0:T(8,128)(2,1)}, bf16[2,1,256,512]{3,2,1,0:T(8,128)(2,1)}) custom-call(s32[4]{0:T(128)S(1)} %copy-done.15, s32[4,4,32]{2,1,0:T(4,128)S(1)} %copy-done.14, s32[4,32,256]{2,1,0:T(8,128)} %reshape.91.names_ref, bf16[256,512]{1,0:T(8,128)(2,1)} %get-tuple-element.62.rest_0_, bf16[256,512]{1,0:T(8,128)(2,1)} %first_kv.3._.rest_1_, ...), custom_call_target="tpu_custom_call" | custom-call | flops 1073741824 | bytes 3145728 | tf_op jit(solution)/shard_map/pallas_call | solution.py:394
  61.1 2.0 %fusion.1 = bf16[2,256,512]{2,1,0:T(8,128)(2,1)} fusion(bf16[2,2,256,512]{3,2,1,0:T(8,128)(2,1)} %collective-permute-done.31.refs_1_, bf16[2,2,256,512]{3,2,1,0:T(8,128)(2,1)S(1)} %copy-done.3), kind=kLoop, calls=%fused_computation.3 | loop fusion | flops 1048576 | bytes 1572864 | tf_op jit(solution)/shard_map/convert_element_type | solution.py:534
  63.1 4.1 %collective-permute-start.32 = (bf16[2,256,512]{2,1,0:T(8,128)(2,1)}, bf16[2,256,512]{2,1,0:T(8,128)(2,1)}, u32[]{:S(2)}, u32[]{:S(2)}) collective-permute-start(bf16[2,256,512]{2,1,0:T(8,128)(2,1)} %fusion.1), channel_id=1, source_target_pairs={{0,2},{1,3},{2,0},{3,1},{4,6},{5,7},{6,4},{7,5}} | collective-permute-start | bytes 1572872 | tf_op jit(solution)/shard_map/ppermute | solution.py:526
  67.2 1.1 %fusion.2 = bf16[1,256,512]{2,1,0:T(8,128)(2,1)S(1)} fusion(bf16[2,1,256,512]{3,2,1,0:T(8,128)(2,1)} %collective-permute-done.36.refs_4_, bf16[2,1,256,512]{3,2,1,0:T(8,128)(2,1)} %get-tuple-element.60.refs_3_), kind=kLoop, calls=%fused_computation.6 | loop fusion | flops 524288 | bytes 786432 | tf_op jit(solution)/shard_map/convert_element_type | solution.py:534
  68.3 1.9 %collective-permute-start.37 = (bf16[1,256,512]{2,1,0:T(8,128)(2,1)S(1)}, bf16[1,256,512]{2,1,0:T(8,128)(2,1)S(1)}, u32[]{:S(2)}, u32[]{:S(2)}) collective-permute-start(bf16[1,256,512]{2,1,0:T(8,128)(2,1)S(1)} %fusion.2), channel_id=1, source_target_pairs={{0,2},{1,3},{2,0},{3,1},{4,6},{5,7},{6,4},{7,5},{8,10},{9,11},{10,... | collective-permute-start | bytes 786440 | tf_op jit(solution)/shard_map/ppermute | solution.py:526
  70.3 0.7 copy-done.5
  71.1 2.0 %collective-permute-start.46 = (bf16[1,256,512]{2,1,0:T(8,128)(2,1)S(1)}, bf16[1,256,512]{2,1,0:T(8,128)(2,1)S(1)}, u32[]{:S(2)}, u32[]{:S(2)}) collective-permute-start(bf16[1,256,512]{2,1,0:T(8,128)(2,1)S(1)} %fusion.3), channel_id=1, source_target_pairs={{0,2},{1,3},{2,0},{3,1},{4,6},{5,7},{6,4},{7,5},{8,10},{9,11},{10,... | collective-permute-start | bytes 786440 | tf_op jit(solution)/shard_map/ppermute | solution.py:526
  73.3 0.7 compare_reduce_fusion
  74.6 11.2 %collective-permute-done.37.refs_5_ = bf16[1,256,512]{2,1,0:T(8,128)(2,1)S(1)} collective-permute-done((bf16[1,256,512]{2,1,0:T(8,128)(2,1)S(1)}, bf16[1,256,512]{2,1,0:T(8,128)(2,1)S(1)}, u32[]{:S(2)}, u32[]{:S(2)}) %collective-permute-start.37) | collective-permute-done | bytes 262176 | tf_op jit(solution)/shard_map/ppermute | solution.py:526
  85.8 5.0 %collective-permute-done.46.refs_8_ = bf16[1,256,512]{2,1,0:T(8,128)(2,1)S(1)} collective-permute-done((bf16[1,256,512]{2,1,0:T(8,128)(2,1)S(1)}, bf16[1,256,512]{2,1,0:T(8,128)(2,1)S(1)}, u32[]{:S(2)}, u32[]{:S(2)}) %collective-permute-start.46) | collective-permute-done | bytes 262176 | tf_op jit(solution)/shard_map/ppermute | solution.py:526
  90.8 0.7 copy-done.13
  91.5 2.3 %finish.3 = bf16[4,256,512]{2,1,0:T(8,128)(2,1)S(1)} custom-call(s32[4]{0:T(128)S(1)} %copy-done.15, bf16[2,2,256,512]{3,2,1,0:T(8,128)(2,1)} %get-tuple-element.56.refs_0_, bf16[2,2,256,512]{3,2,1,0:T(8,128)(2,1)} %collective-permute-done.31.refs_1_, bf16[2,256,512]{2,1,0:T(8,128)(2,1)} %collective-permute-done.32.refs_2_, ...), custom_call_target="tpu_custom_call" | custom-call | flops 2097152 | bytes 4194304 | tf_op jit(solution)/shard_map/finish/pallas_call | solution.py:453
  94.1 1.0 %copy-done.6 = bf16[4,256,512]{2,1,0:T(8,128)(2,1)} copy-done((bf16[4,256,512]{2,1,0:T(8,128)(2,1)}, bf16[4,256,512]{2,1,0:T(8,128)(2,1)S(1)}, u32[]{:S(2)}) %copy-start.6) | copy-done | bytes 1048600
  (57 shorter events, 2.8 us)
Async XLA Ops:
  0.0 4.0 %copy-start.15 = (s32[4]{0:T(128)S(1)}, s32[4]{0:T(128)}, u32[]{:S(2)}) copy-start(s32[4]{0:T(128)} %len_ref.11) | copy-start | bytes 52
  0.0 4.0 %copy-start.2 = (bf16[2048,256]{1,0:T(8,128)(2,1)S(1)}, bf16[2048,256]{1,0:T(8,128)(2,1)}, u32[]{:S(2)}) copy-start(bf16[2048,256]{1,0:T(8,128)(2,1)} %v_ref.3) | copy-start | bytes 3145732
  0.0 4.0 %copy-start.1 = (bf16[2048,256]{1,0:T(8,128)(2,1)S(1)}, bf16[2048,256]{1,0:T(8,128)(2,1)}, u32[]{:S(2)}) copy-start(bf16[2048,256]{1,0:T(8,128)(2,1)} %k_ref.3) | copy-start | bytes 3145732
  4.0 10.2 %copy-start.7 = (bf16[256,512]{1,0:T(8,128)(2,1)S(1)}, bf16[256,512]{1,0:T(8,128)(2,1)}, u32[]{:S(2)}) copy-start(bf16[256,512]{1,0:T(8,128)(2,1)} %first_kv.3._.rest_1_) | copy-start | bytes 786436
  4.0 11.6 %copy-start.14 = (s32[4,4,32]{2,1,0:T(4,128)S(1)}, s32[4,4,32]{2,1,0:T(4,128)}, u32[]{:S(2)}) copy-start(s32[4,4,32]{2,1,0:T(4,128)} %pick_ref.5) | copy-start | bytes 6148
  11.9 8.3 %collective-permute-start.30 = (bf16[256,512]{1,0:T(8,128)(2,1)}, bf16[256,512]{1,0:T(8,128)(2,1)S(1)}, u32[]{:S(2)}, u32[]{:S(2)}) collective-permute-start(bf16[256,512]{1,0:T(8,128)(2,1)} %get-tuple-element.55.rest_3_), channel_id=1, source_target_pairs={{0,4},{1,5},{2,6},{3,7}} | collective-permute-start | bytes 786440 | tf_op jit(solution)/shard_map/ppermute | solution.py:476
  14.3 18.9 %collective-permute-start.39 = (bf16[256,512]{1,0:T(8,128)(2,1)S(1)}, bf16[256,512]{1,0:T(8,128)(2,1)S(1)}, u32[]{:S(2)}, u32[]{:S(2)}) collective-permute-start(bf16[256,512]{1,0:T(8,128)(2,1)S(1)} %copy-done.7), channel_id=1, source_target_pairs={{0,8},{4,12},{8,16},{12,20},{16,24},{20,28},{1,9},{5,13},{9,17},{1... | collective-permute-start | bytes 786440 | tf_op jit(solution)/shard_map/ppermute | solution.py:486
  29.9 31.2 %collective-permute-start.31 = (bf16[2,2,256,512]{3,2,1,0:T(8,128)(2,1)}, bf16[2,2,256,512]{3,2,1,0:T(8,128)(2,1)}, u32[]{:S(2)}, u32[]{:S(2)}) collective-permute-start(bf16[2,2,256,512]{3,2,1,0:T(8,128)(2,1)} %get-tuple-element.57), channel_id=1, source_target_pairs={{0,1},{1,0},{2,3},{3,2},{4,5},{5,4},{6,7},{7,6}} | collective-permute-start | bytes 3145736 | tf_op jit(solution)/shard_map/ppermute | solution.py:526
  31.8 8.1 %collective-permute-start.34 = (bf16[256,512]{1,0:T(8,128)(2,1)}, bf16[256,512]{1,0:T(8,128)(2,1)S(1)}, u32[]{:S(2)}, u32[]{:S(2)}) collective-permute-start(bf16[256,512]{1,0:T(8,128)(2,1)} %get-tuple-element.59.rest_1_), channel_id=1, source_target_pairs={{0,8},{4,12},{1,9},{5,13},{2,10},{6,14},{3,11},{7,15}} | collective-permute-start | bytes 786440 | tf_op jit(solution)/shard_map/ppermute | solution.py:486
  33.2 21.4 %copy-start.8 = (bf16[256,512]{1,0:T(8,128)(2,1)}, bf16[256,512]{1,0:T(8,128)(2,1)S(1)}, u32[]{:S(2)}) copy-start(bf16[256,512]{1,0:T(8,128)(2,1)S(1)} %collective-permute-done.39.rest_3_) | copy-start | bytes 786436
  33.2 7.4 %collective-permute-start.41 = (bf16[256,512]{1,0:T(8,128)(2,1)S(1)}, bf16[256,512]{1,0:T(8,128)(2,1)S(1)}, u32[]{:S(2)}, u32[]{:S(2)}) collective-permute-start(bf16[256,512]{1,0:T(8,128)(2,1)S(1)} %collective-permute-done.39.rest_3_), channel_id=1, source_target_pairs={{8,16},{12,20},{16,24},{20,28},{9,17},{13,21},{17,25},{21,29},{10,... | collective-permute-start | bytes 786440 | tf_op jit(solution)/shard_map/ppermute | solution.py:486
  33.9 8.8 %collective-permute-start.33 = (bf16[256,512]{1,0:T(8,128)(2,1)}, bf16[256,512]{1,0:T(8,128)(2,1)S(1)}, u32[]{:S(2)}, u32[]{:S(2)}) collective-permute-start(bf16[256,512]{1,0:T(8,128)(2,1)} %get-tuple-element.59.rest_1_), channel_id=1, source_target_pairs={{0,4},{8,12},{12,8},{1,5},{9,13},{13,9},{2,6},{10,14},{14,10},{3,7... | collective-permute-start | bytes 786440 | tf_op jit(solution)/shard_map/ppermute | solution.py:476
  39.9 5.5 %copy-start.34 = (bf16[256,512]{1,0:T(8,128)(2,1)}, bf16[256,512]{1,0:T(8,128)(2,1)S(1)}, u32[]{:S(2)}) copy-start(bf16[256,512]{1,0:T(8,128)(2,1)S(1)} %collective-permute-done.34.rest_3_) | copy-start | bytes 786436
  39.9 4.1 %collective-permute-start.35 = (bf16[256,512]{1,0:T(8,128)(2,1)S(1)}, bf16[256,512]{1,0:T(8,128)(2,1)S(1)}, u32[]{:S(2)}, u32[]{:S(2)}) collective-permute-start(bf16[256,512]{1,0:T(8,128)(2,1)S(1)} %collective-permute-done.34.rest_3_), channel_id=1, source_target_pairs={{8,12},{12,8},{9,13},{13,9},{10,14},{14,10},{11,15},{15,11}} | collective-permute-start | bytes 786440 | tf_op jit(solution)/shard_map/ppermute | solution.py:476
  40.6 13.9 %copy-start.9 = (bf16[256,512]{1,0:T(8,128)(2,1)}, bf16[256,512]{1,0:T(8,128)(2,1)S(1)}, u32[]{:S(2)}) copy-start(bf16[256,512]{1,0:T(8,128)(2,1)S(1)} %collective-permute-done.41.rest_5_) | copy-start | bytes 786436
  40.6 4.8 %collective-permute-start.43 = (bf16[256,512]{1,0:T(8,128)(2,1)S(1)}, bf16[256,512]{1,0:T(8,128)(2,1)S(1)}, u32[]{:S(2)}, u32[]{:S(2)}) collective-permute-start(bf16[256,512]{1,0:T(8,128)(2,1)S(1)} %collective-permute-done.41.rest_5_), channel_id=1, source_target_pairs={{16,24},{20,28},{17,25},{21,29},{18,26},{22,30},{19,27},{23,31}} | collective-permute-start | bytes 786440 | tf_op jit(solution)/shard_map/ppermute | solution.py:486
  41.3 11.2 %collective-permute-start.38 = (bf16[256,512]{1,0:T(8,128)(2,1)S(1)}, bf16[256,512]{1,0:T(8,128)(2,1)S(1)}, u32[]{:S(2)}, u32[]{:S(2)}) collective-permute-start(bf16[256,512]{1,0:T(8,128)(2,1)S(1)} %copy-done.7), channel_id=1, source_target_pairs={{0,4},{8,12},{12,8},{16,20},{20,16},{24,28},{28,24},{1,5},{9,13},{... | collective-permute-start | bytes 786440 | tf_op jit(solution)/shard_map/ppermute | solution.py:476
  42.6 4.1 %copy-start.35 = (bf16[256,512]{1,0:T(8,128)(2,1)}, bf16[256,512]{1,0:T(8,128)(2,1)S(1)}, u32[]{:S(2)}) copy-start(bf16[256,512]{1,0:T(8,128)(2,1)S(1)} %collective-permute-done.33.rest_2_) | copy-start | bytes 786436
  42.7 11.8 %collective-permute-start.40 = (bf16[256,512]{1,0:T(8,128)(2,1)S(1)}, bf16[256,512]{1,0:T(8,128)(2,1)}, u32[]{:S(2)}, u32[]{:S(2)}) collective-permute-start(bf16[256,512]{1,0:T(8,128)(2,1)S(1)} %collective-permute-done.39.rest_3_), channel_id=1, source_target_pairs={{8,12},{12,8},{16,20},{20,16},{24,28},{28,24},{9,13},{13,9},{17,21... | collective-permute-start | bytes 786440 | tf_op jit(solution)/shard_map/ppermute | solution.py:476
  44.0 2.7 %copy-start.36 = (bf16[256,512]{1,0:T(8,128)(2,1)}, bf16[256,512]{1,0:T(8,128)(2,1)S(1)}, u32[]{:S(2)}) copy-start(bf16[256,512]{1,0:T(8,128)(2,1)S(1)} %collective-permute-done.35.rest_4_) | copy-start | bytes 786436
  44.1 10.4 %collective-permute-start.42 = (bf16[256,512]{1,0:T(8,128)(2,1)S(1)}, bf16[256,512]{1,0:T(8,128)(2,1)}, u32[]{:S(2)}, u32[]{:S(2)}) collective-permute-start(bf16[256,512]{1,0:T(8,128)(2,1)S(1)} %collective-permute-done.41.rest_5_), channel_id=1, source_target_pairs={{16,20},{20,16},{24,28},{28,24},{17,21},{21,17},{25,29},{29,25},{1... | collective-permute-start | bytes 786440 | tf_op jit(solution)/shard_map/ppermute | solution.py:476
  45.4 9.1 %copy-start.10 = (bf16[256,512]{1,0:T(8,128)(2,1)}, bf16[256,512]{1,0:T(8,128)(2,1)S(1)}, u32[]{:S(2)}) copy-start(bf16[256,512]{1,0:T(8,128)(2,1)S(1)} %collective-permute-done.43.rest_7_) | copy-start | bytes 786436
  45.4 9.1 %collective-permute-start.44 = (bf16[256,512]{1,0:T(8,128)(2,1)S(1)}, bf16[256,512]{1,0:T(8,128)(2,1)}, u32[]{:S(2)}, u32[]{:S(2)}) collective-permute-start(bf16[256,512]{1,0:T(8,128)(2,1)S(1)} %collective-permute-done.43.rest_7_), channel_id=1, source_target_pairs={{24,28},{28,24},{25,29},{29,25},{26,30},{30,26},{27,31},{31,27}} | collective-permute-start | bytes 786440 | tf_op jit(solution)/shard_map/ppermute | solution.py:476
  52.5 14.7 %collective-permute-start.36 = (bf16[2,1,256,512]{3,2,1,0:T(8,128)(2,1)}, bf16[2,1,256,512]{3,2,1,0:T(8,128)(2,1)}, u32[]{:S(2)}, u32[]{:S(2)}) collective-permute-start(bf16[2,1,256,512]{3,2,1,0:T(8,128)(2,1)} %get-tuple-element.61), channel_id=1, source_target_pairs={{0,1},{1,0},{2,3},{3,2},{4,5},{5,4},{6,7},{7,6},{8,9},{9,8},{10,11... | collective-permute-start | bytes 1572872 | tf_op jit(solution)/shard_map/ppermute | solution.py:526
  54.5 6.6 %copy-start.3 = (bf16[2,2,256,512]{3,2,1,0:T(8,128)(2,1)S(1)}, bf16[2,2,256,512]{3,2,1,0:T(8,128)(2,1)}, u32[]{:S(2)}) copy-start(bf16[2,2,256,512]{3,2,1,0:T(8,128)(2,1)} %get-tuple-element.56.refs_0_) | copy-start | bytes 3145732
  60.6 9.7 %copy-start.4 = (bf16[2,1,256,512]{3,2,1,0:T(8,128)(2,1)S(1)}, bf16[2,1,256,512]{3,2,1,0:T(8,128)(2,1)}, u32[]{:S(2)}) copy-start(bf16[2,1,256,512]{3,2,1,0:T(8,128)(2,1)} %get-tuple-element.63.refs_6_) | copy-start | bytes 1572868
  60.6 12.5 %copy-start.38 = (s32[4]{0:T(128)S(1)}, s32[4]{0:T(128)}, u32[]{:S(2)}) copy-start(s32[4]{0:T(128)} %constant.10) | copy-start | bytes 52
  60.6 9.7 %collective-permute-start.45 = (bf16[2,1,256,512]{3,2,1,0:T(8,128)(2,1)}, bf16[2,1,256,512]{3,2,1,0:T(8,128)(2,1)S(1)}, u32[]{:S(2)}, u32[]{:S(2)}) collective-permute-start(bf16[2,1,256,512]{3,2,1,0:T(8,128)(2,1)} %get-tuple-element.64), channel_id=1, source_target_pairs={{0,1},{1,0},{2,3},{3,2},{4,5},{5,4},{6,7},{7,6},{8,9},{9,8},{10,11... | collective-permute-start | bytes 1572872 | tf_op jit(solution)/shard_map/ppermute | solution.py:526
  63.1 28.4 %collective-permute-start.32 = (bf16[2,256,512]{2,1,0:T(8,128)(2,1)}, bf16[2,256,512]{2,1,0:T(8,128)(2,1)}, u32[]{:S(2)}, u32[]{:S(2)}) collective-permute-start(bf16[2,256,512]{2,1,0:T(8,128)(2,1)} %fusion.1), channel_id=1, source_target_pairs={{0,2},{1,3},{2,0},{3,1},{4,6},{5,7},{6,4},{7,5}} | collective-permute-start | bytes 1572872 | tf_op jit(solution)/shard_map/ppermute | solution.py:526
  68.3 17.5 %collective-permute-start.37 = (bf16[1,256,512]{2,1,0:T(8,128)(2,1)S(1)}, bf16[1,256,512]{2,1,0:T(8,128)(2,1)S(1)}, u32[]{:S(2)}, u32[]{:S(2)}) collective-permute-start(bf16[1,256,512]{2,1,0:T(8,128)(2,1)S(1)} %fusion.2), channel_id=1, source_target_pairs={{0,2},{1,3},{2,0},{3,1},{4,6},{5,7},{6,4},{7,5},{8,10},{9,11},{10,... | collective-permute-start | bytes 786440 | tf_op jit(solution)/shard_map/ppermute | solution.py:526
  71.1 19.7 %collective-permute-start.46 = (bf16[1,256,512]{2,1,0:T(8,128)(2,1)S(1)}, bf16[1,256,512]{2,1,0:T(8,128)(2,1)S(1)}, u32[]{:S(2)}, u32[]{:S(2)}) collective-permute-start(bf16[1,256,512]{2,1,0:T(8,128)(2,1)S(1)} %fusion.3), channel_id=1, source_target_pairs={{0,2},{1,3},{2,0},{3,1},{4,6},{5,7},{6,4},{7,5},{8,10},{9,11},{10,... | collective-permute-start | bytes 786440 | tf_op jit(solution)/shard_map/ppermute | solution.py:526
  85.8 5.7 %copy-start.12 = (bf16[1,256,512]{2,1,0:T(8,128)(2,1)}, bf16[1,256,512]{2,1,0:T(8,128)(2,1)S(1)}, u32[]{:S(2)}) copy-start(bf16[1,256,512]{2,1,0:T(8,128)(2,1)S(1)} %collective-permute-done.37.refs_5_) | copy-start | bytes 786436
  (5 other events, 5.2 us)

commit v2 on v1

--- a/solution.py
+++ b/solution.py
@@ -10,6 +10,7 @@
 HD = 128
 KB = 64
 CORES = 2
+ROOM = 24 << 20
 SCALE = HD ** (-0.5) * math.log2(math.e)
 
 
@@ -36,154 +37,118 @@
     return pl.CostEstimate(flops=int(flops), bytes_accessed=int(moved), transcendentals=0)
 
 
-def first_kv(lengths, rows, wk, wv):
-    _, span, width = rows.shape
-    kv_width = wk.shape[1]
-    tiles = 4
-    depth = width // tiles
-
-    def body(len_ref, x_ref, k_ref, v_ref, out_ref, x, k, v, acc, sem):
-        seq = nth_longest(len_ref, 0)
-        alive = lax.axis_index("kv") * span < len_ref[seq]
-
-        @pl.when(alive)
-        def _():
-            def copies(t):
-                part = pl.ds(pl.multiple_of(t * depth, depth), depth)
-                return (
-                    pltpu.make_async_copy(k_ref.at[part], k.at[t], sem.at[3 * t]),
-                    pltpu.make_async_copy(v_ref.at[part], v.at[t], sem.at[3 * t + 1]),
-                    pltpu.make_async_copy(x_ref.at[seq, :, part], x.at[t], sem.at[3 * t + 2]),
-                )
-
-            for t in range(tiles):
-                for copy in copies(t):
-                    copy.start()
-            acc[...] = jnp.zeros_like(acc)
-
-            @pl.loop(0, tiles)
-            def _(t):
-                for copy in copies(t):
-                    copy.wait()
-                acc[:, :kv_width] += jnp.dot(x[t], k[t], preferred_element_type=jnp.float32)
-                acc[:, kv_width:] += jnp.dot(x[t], v[t], preferred_element_type=jnp.float32)
-
-            out_ref[...] = acc[...].astype(out_ref.dtype)
-
-    return pl.pallas_call(
-        body,
-        in_specs=[SMEM, ANY, ANY, ANY],
-        out_specs=VMEM,
-        out_shape=jax.ShapeDtypeStruct((span, 2 * kv_width), jnp.bfloat16),
-        scratch_shapes=[
-            pltpu.VMEM((tiles, span, depth), jnp.bfloat16),
-            pltpu.VMEM((tiles, depth, kv_width), jnp.bfloat16),
-            pltpu.VMEM((tiles, depth, kv_width), jnp.bfloat16),
-            pltpu.VMEM((span, 2 * kv_width), jnp.float32),
-            pltpu.SemaphoreType.DMA((3 * tiles,)),
-        ],
-        cost_estimate=cost(4 * span * width * kv_width, 3 << 20),
-        name="first_kv",
-    )(lengths, rows, wk, wv)
-
-
-def other_qkv(lengths, rows, wq, wk, wv, after):
+def project(lengths, rows, weights, first=0, shared=0, after=()):
     batch, span, width = rows.shape
-    kv_width = wk.shape[1]
-    q_width = wq.shape[1]
-
-    def body(len_ref, x_ref, q_ref, k_ref, v_ref, _, *rest):
-        q_outs, kv_outs = rest[:batch], rest[batch : 2 * batch - 1]
-        x, wqs, wks, wvs, q, kv, sem, out_sem = rest[2 * batch - 1 :]
+    sets = len(weights)
+    widths = [sum(w.shape[1] for w in part) for part in weights]
+    flat = [w for part in weights for w in part]
+    more = min(shared, 1)
+
+    def body(len_ref, x_ref, *refs):
+        given, refs = refs[: len(flat)], refs[len(flat) + len(after) :]
+        outs, refs = refs[: sets * batch], refs[sets * batch :]
+        again, refs = refs[:more], refs[more:]
+        x, refs = refs[0], refs[1:]
+        held, out, (sem, w_sem, out_sem) = refs[:sets], refs[sets : 2 * sets], refs[2 * sets :]
         here = lax.axis_index("kv")
         seqs = [nth_longest(len_ref, tier) for tier in range(batch)]
         alive = [here * span < len_ref[seq] for seq in seqs]
-        weights = [
-            pltpu.make_async_copy(ref, buf, sem.at[batch + i])
-            for i, (ref, buf) in enumerate(((q_ref, wqs), (k_ref, wks), (v_ref, wvs)))
-        ]
-        inbound = [
-            pltpu.make_async_copy(x_ref.at[seqs[tier]], x.at[tier], sem.at[tier])
-            for tier in range(batch)
-        ]
-        q_out = [
-            pltpu.make_async_copy(q.at[tier], q_outs[tier], out_sem.at[tier])
-            for tier in range(batch)
-        ]
-        kv_out = [
-            pltpu.make_async_copy(kv.at[tier], kv_outs[tier - 1], out_sem.at[batch + tier])
-            for tier in range(1, batch)
-        ]
-        tiers = [*range(1, batch), 0]
+        loads, at = [], 0
+        for i, part in enumerate(weights):
+            loads.append([])
+            base = 0
+            for w in part:
+                loads[i].append(
+                    pltpu.make_async_copy(
+                        given[at], held[i].at[:, pl.ds(base, w.shape[1])], w_sem.at[at]
+                    )
+                )
+                at += 1
+                base += w.shape[1]
+
+        def load(tier):
+            return pltpu.make_async_copy(x_ref.at[seqs[tier]], x.at[tier], sem.at[tier])
+
+        def stores(tier):
+            found = [
+                pltpu.make_async_copy(
+                    out[i].at[tier], outs[i * batch + tier], out_sem.at[i, tier]
+                )
+                for i in range(sets)
+            ]
+            if first <= tier < first + shared:
+                found.append(
+                    pltpu.make_async_copy(
+                        out[0].at[tier], again[0].at[tier - first], out_sem.at[sets, tier]
+                    )
+                )
+            return found
 
         @pl.when(alive[0])
         def _():
-            for copy in weights:
-                copy.start()
-            for tier in tiers:
-
-                @pl.when(alive[tier])
-                def _():
-                    inbound[tier].start()
-
-            for copy in weights:
-                copy.wait()
+            load(0).start()
+            for part in loads:
+                for one in part:
+                    one.start()
+
+        for tier in range(1, batch):
+
+            @pl.when(alive[tier])
+            def _():
+                load(tier).start()
 
         @pl.loop(0, batch)
-        def _(step):
-            tier = lax.rem(step + 1, batch)
-
+        def _(tier):
             @pl.when(here * span < len_ref[nth_longest(len_ref, tier)])
             def _():
                 pltpu.make_async_copy(x_ref.at[0], x.at[tier], sem.at[tier]).wait()
-                q[tier] = jnp.dot(
-                    x[tier], wqs[...], preferred_element_type=jnp.float32
-                ).astype(q.dtype)
-                kv[tier, :, :kv_width] = jnp.dot(
-                    x[tier], wks[...], preferred_element_type=jnp.float32
-                ).astype(kv.dtype)
-                kv[tier, :, kv_width:] = jnp.dot(
-                    x[tier], wvs[...], preferred_element_type=jnp.float32
-                ).astype(kv.dtype)
+                for i in range(sets):
+
+                    @pl.when(tier == 0)
+                    def _():
+                        for one in loads[i]:
+                            one.wait()
+
+                    out[i][tier] = jnp.dot(
+                        x[tier], held[i][...], preferred_element_type=jnp.float32
+                    ).astype(out[i].dtype)
                 for t in range(batch):
 
                     @pl.when(tier == t)
                     def _():
-                        q_out[t].start()
-                        if t > 0:
-                            kv_out[t - 1].start()
-
-        for tier in tiers:
+                        for store in stores(t):
+                            store.start()
+
+        for tier in range(batch):
 
             @pl.when(alive[tier])
             def _():
-                if tier > 0:
-                    kv_out[tier - 1].wait()
-                q_out[tier].wait()
-
-    outs = pl.pallas_call(
+                for store in stores(tier):
+                    store.wait()
+
+    found = pl.pallas_call(
         body,
-        in_specs=[SMEM, ANY, ANY, ANY, ANY, ANY],
-        out_specs=[ANY] * (2 * batch - 1),
-        out_shape=[jax.ShapeDtypeStruct((span, q_width), jnp.bfloat16)] * batch
-        + [jax.ShapeDtypeStruct((span, 2 * kv_width), jnp.bfloat16)] * (batch - 1),
-        scratch_shapes=[
-            pltpu.VMEM((batch, span, width), jnp.bfloat16),
-            pltpu.VMEM((width, q_width), jnp.bfloat16),
-            pltpu.VMEM((width, kv_width), jnp.bfloat16),
-            pltpu.VMEM((width, kv_width), jnp.bfloat16),
-            pltpu.VMEM((batch, span, q_width), jnp.bfloat16),
-            pltpu.VMEM((batch, span, 2 * kv_width), jnp.bfloat16),
-            pltpu.SemaphoreType.DMA((batch + 3,)),
-            pltpu.SemaphoreType.DMA((2 * batch,)),
+        in_specs=[SMEM] + [ANY] * (1 + len(flat) + len(after)),
+        out_specs=[ANY] * (sets * batch + more),
+        out_shape=[
+            jax.ShapeDtypeStruct((span, size), jnp.bfloat16) for size in widths for _ in range(batch)
+        ]
+        + [jax.ShapeDtypeStruct((shared, span, widths[0]), jnp.bfloat16)] * more,
+        scratch_shapes=[pltpu.VMEM((batch, span, width), jnp.bfloat16)]
+        + [pltpu.VMEM((width, size), jnp.bfloat16) for size in widths]
+        + [pltpu.VMEM((batch, span, size), jnp.bfloat16) for size in widths]
+        + [
+            pltpu.SemaphoreType.DMA((batch,)),
+            pltpu.SemaphoreType.DMA((len(flat),)),
+            pltpu.SemaphoreType.DMA((sets + 1, batch)),
         ],
-        cost_estimate=cost(2 * batch * span * width * (q_width + 2 * kv_width), 8 << 20),
-        name="other_qkv",
-    )(lengths, rows, wq, wk, wv, after)
-    return outs[:batch], outs[batch:]
-
-
-def attend(tiers, columns, lengths, chosen, queries, own_kv, slabs, wo, parts, after=()):
+        compiler_params=pltpu.CompilerParams(vmem_limit_bytes=ROOM),
+        cost_estimate=cost(2 * batch * span * width * sum(widths), 8 << 20),
+    )(lengths, rows, *flat, *after)
+    return [found[i * batch : (i + 1) * batch] for i in range(sets)], found[-1]
+
+
+def attend(tiers, columns, lengths, chosen, queries, own_kv, slabs, wo, parts):
     group = len(tiers)
     span, q_width = queries[0].shape
     blocks = span // KB
@@ -193,18 +158,17 @@
     width = wo.shape[1]
     piece = width // (parts * CORES)
     names = chosen.shape[2]
-    spread = jnp.repeat(jnp.swapaxes(chosen, 1, 2), KB, axis=2)
     devices = lax.axis_size("kv")
     most = max(len(part) for part in slabs)
     room = (most + 1) * blocks
-    arrays = [array for part in slabs for array, _, _ in part]
+    arrays = [array for part in slabs for array, _, _, _ in part]
 
     def body(len_ref, pick_ref, names_ref, *rest):
         q_hbm, kv_hbm = rest[:group], rest[group : 2 * group]
         rest = rest[2 * group :]
         slab_refs = rest[: len(arrays)]
         w_hbm = rest[len(arrays)]
-        rest = rest[len(arrays) + 1 + len(after) :]
+        rest = rest[len(arrays) + 1 :]
         keep_hbm, give_hbm, q_ref, w_ref, packed, top, low, acc, att, mask, out = rest[:11]
         marks, listed, count, q_sem, kv_sem, w_sem, slot_sem, out_sem = rest[11:]
         here = lax.axis_index("kv")
@@ -225,20 +189,25 @@
                 out_sem.at[g, side, far],
             )
 
+        def load(g):
+            for i in range(group):
+
+                @pl.when(g == i)
+                def _():
+                    pltpu.make_async_copy(q_hbm[i], q_ref, q_sem).start()
+                    pltpu.make_async_copy(kv_hbm[i], packed.at[pl.ds(0, span)], kv_sem).start()
+
         def one(g, tier):
             seq = nth_longest(len_ref, tier)
             length = len_ref[seq]
 
             @pl.when(here * span < length)
             def _():
-                for i in range(group):
-
-                    @pl.when(g == i)
-                    def _():
-                        pltpu.make_async_copy(q_hbm[i], q_ref, q_sem).start()
-                        pltpu.make_async_copy(
-                            kv_hbm[i], packed.at[pl.ds(0, span)], kv_sem
-                        ).start()
+                opening = (g == 0) | (here * span >= len_ref[nth_longest(len_ref, tier + 1)])
+
+                @pl.when(opening)
+                def _():
+                    load(g)
 
                 for c in range(blocks):
                     listed[c] = here * blocks + c
@@ -258,8 +227,8 @@
 
                     at = 0
                     for i in range(group):
-                        for _, back, turned in slabs[i]:
-                            ref = slab_refs[at]
+                        for _, place, back, turned in slabs[i]:
+                            ref = slab_refs[at] if place is None else slab_refs[at].at[place]
                             at += 1
                             source = (row - back) * columns + lax.rem(
                                 column - turned + columns, columns
@@ -280,7 +249,16 @@
                                             slot_sem.at[slot],
                                         ).start()
 
-                picked = names_ref[seq]
+                widen = lax.broadcasted_iota(jnp.int32, (blocks, span), 1) // KB
+                widen = widen == lax.broadcasted_iota(jnp.int32, (blocks, span), 0)
+                picked = lax.dot_general(
+                    names_ref[seq].astype(jnp.float32),
+                    widen.astype(jnp.float32),
+                    (((0,), (0,)), ((), ())),
+                    precision=lax.Precision.HIGHEST,
+                    preferred_element_type=jnp.float32,
+                )
+                picked = jnp.round(picked).astype(jnp.int32)
                 own_id = here * blocks + lax.broadcasted_iota(jnp.int32, (1, span), 1) // KB
                 times = jnp.sum((picked == own_id).astype(jnp.float32), axis=0, keepdims=True)
                 extra = jnp.log2(times) * (1.0 / SCALE)
@@ -347,6 +325,7 @@
                             preferred_element_type=jnp.float32,
                         )
 
+                load(g + 1)
                 living = here * span + lax.broadcasted_iota(jnp.int32, (span, 1), 0) < length
                 for head in range(kv_heads):
                     done = acc[head] * (1.0 / low[head])
@@ -356,7 +335,7 @@
                             living, done[:, k * span : (k + 1) * span].T, 0.0
                         ).astype(att.dtype)
 
-                @pl.when((g == 0) | (here * span >= len_ref[nth_longest(len_ref, tier + 1)]))
+                @pl.when(opening)
                 def _():
                     load_w.wait()
 
@@ -393,7 +372,7 @@
     result = jax.ShapeDtypeStruct((parts, group, span, piece), jnp.bfloat16)
     return pl.pallas_call(
         body,
-        in_specs=[SMEM, SMEM, VMEM, *[ANY] * (2 * group + len(arrays) + 1 + len(after))],
+        in_specs=[SMEM, SMEM, VMEM, *[ANY] * (2 * group + len(arrays) + 1)],
         out_specs=[ANY, ANY],
         out_shape=[result, result],
         scratch_shapes=[
@@ -415,57 +394,89 @@
             pltpu.SemaphoreType.DMA((room,)),
             pltpu.SemaphoreType.DMA((group, CORES, parts)),
         ],
+        compiler_params=pltpu.CompilerParams(vmem_limit_bytes=ROOM),
         cost_estimate=cost(group * 4 * span * q_width * width, group * (3 << 20)),
-    )(lengths, chosen, spread, *queries, *own_kv, *arrays, wo, *after)
-
-
-def finish(lengths, batch, groups):
-    _, _, span, piece = groups[0][1].shape
+    )(lengths, chosen, chosen, *queries, *own_kv, *arrays, wo)
+
+
+def finish(lengths, batch, groups, before=None):
+    parts, _, span, piece = groups[0][1].shape
+    every = [(tier, g, at) for at, group in enumerate(groups) for g, tier in enumerate(group[0])]
+    each = 1 + parts
 
     def body(len_ref, *refs):
-        out_ref = refs[-1]
-        at = 0
-        for tiers, _, _, coming in groups:
-            mine = refs[at : at + 2 + len(coming)]
-            at += 2 + len(coming)
-            for g, tier in enumerate(tiers):
-                seq = nth_longest(len_ref, tier)
-                alive = lax.axis_index("kv") * span < len_ref[seq]
-
-                @pl.when(alive)
-                def _():
-                    total = mine[0][0, g].astype(jnp.float32) + mine[1][0, g].astype(jnp.float32)
-                    for ref in mine[2:]:
-                        total = total + ref[g].astype(jnp.float32)
-                    out_ref[seq] = total.astype(out_ref.dtype)
-
-                @pl.when(jnp.logical_not(alive))
-                def _():
-                    out_ref[seq] = jnp.zeros((span, piece), out_ref.dtype)
-
-    specs, operands = [SMEM], [lengths]
-    for tiers, keep, got, coming in groups:
-        size = len(tiers)
-        near = pl.BlockSpec((1, size, span, piece), lambda i: (0, 0, 0, 0))
-        flat = pl.BlockSpec((size, span, piece), lambda i: (0, 0, 0))
-        specs += [near, near] + [flat] * len(coming)
-        operands += [keep, got, *coming]
+        given = refs[: each * len(groups)]
+        out_ref, terms, sums, in_sem, out_sem = refs[-5:]
+        here = lax.axis_index("kv")
+        seqs = [nth_longest(len_ref, tier) for tier, _, _ in every]
+
+        def loads(n):
+            _, g, at = every[n]
+            mine = given[at * each : (at + 1) * each]
+            sources = [mine[0].at[0, g], mine[1].at[0, g]] + [ref.at[g] for ref in mine[2:]]
+            return [
+                pltpu.make_async_copy(source, terms.at[n, i], in_sem.at[n, i])
+                for i, source in enumerate(sources)
+            ]
+
+        def store(n):
+            return pltpu.make_async_copy(sums.at[n], out_ref.at[seqs[n]], out_sem.at[n])
+
+        for n in range(len(every)):
+
+            @pl.when(here * span < len_ref[seqs[n]])
+            def _():
+                for load in loads(n):
+                    load.start()
+
+        for n in range(len(every)):
+            alive = here * span < len_ref[seqs[n]]
+
+            @pl.when(alive)
+            def _():
+                for load in loads(n):
+                    load.wait()
+                total = terms[n, 0].astype(jnp.float32)
+                for i in range(1, each):
+                    total = total + terms[n, i].astype(jnp.float32)
+                sums[n] = total.astype(sums.dtype)
+
+            @pl.when(jnp.logical_not(alive))
+            def _():
+                sums[n] = jnp.zeros((span, piece), sums.dtype)
+
+            store(n).start()
+        for n in range(len(every)):
+            store(n).wait()
+
+    operands = [part for _, keep, got, coming in groups for part in (keep, got, *coming)]
+    aliases = {}
+    if before is not None:
+        aliases = {1 + len(operands): 0}
+        operands.append(before)
     return pl.pallas_call(
         body,
-        grid=(1,),
-        in_specs=specs,
-        out_specs=pl.BlockSpec((batch, span, piece), lambda i: (0, 0, 0)),
+        in_specs=[SMEM] + [ANY] * len(operands),
+        out_specs=ANY,
         out_shape=jax.ShapeDtypeStruct((batch, span, piece), jnp.bfloat16),
-        cost_estimate=cost(batch * 4 * span * piece, batch * 8 * span * piece),
+        scratch_shapes=[
+            pltpu.VMEM((len(every), each, span, piece), jnp.bfloat16),
+            pltpu.VMEM((len(every), span, piece), jnp.bfloat16),
+            pltpu.SemaphoreType.DMA((len(every), each)),
+            pltpu.SemaphoreType.DMA((len(every),)),
+        ],
+        input_output_aliases=aliases,
+        compiler_params=pltpu.CompilerParams(vmem_limit_bytes=ROOM),
+        cost_estimate=cost(len(every) * 4 * span * piece, len(every) * 8 * span * piece),
         name="finish",
-    )(*operands)
-
-
-def gather_spans(slab, reach, columns):
-    rows = reach // columns
-    arrived = []
-
-    def turn(x, back):
+    )(lengths, *operands)
+
+
+def gather_spans(slabs, joined, first, reaches, columns):
+    arrived = [[] for _ in reaches]
+
+    def turn(x, back, rows):
+        found = []
         for d in range(1, columns):
             pairs = [
                 (r * columns + c, r * columns + (c + d) % columns)
@@ -473,19 +484,28 @@
                 for c in range(columns)
                 if r > 0 or c + d < columns
             ]
-            arrived.append((lax.ppermute(x, "kv", pairs), back, d))
-
-    turn(slab, 0)
-    passing = slab
-    for back in range(1, rows):
-        pairs = [
-            (r * columns + c, (r + 1) * columns + c)
-            for r in range(back - 1, rows - 1)
-            for c in range(columns)
-        ]
-        passing = lax.ppermute(passing, "kv", pairs)
-        arrived.append((passing, back, 0))
-        turn(passing, back)
+            found.append((lax.ppermute(x, "kv", pairs), d))
+        return found
+
+    for moved, d in turn(joined, 0, reaches[first] // columns):
+        for place in range(joined.shape[0]):
+            arrived[first + place].append((moved, place, 0, d))
+    for tier, reach in enumerate(reaches):
+        rows = reach // columns
+        if reach > 1 and not first <= tier < first + joined.shape[0]:
+            for moved, d in turn(slabs[tier], 0, rows):
+                arrived[tier].append((moved, None, 0, d))
+        passing = slabs[tier]
+        for back in range(1, rows):
+            pairs = [
+                (r * columns + c, (r + 1) * columns + c)
+                for r in range(back - 1, rows - 1)
+                for c in range(columns)
+            ]
+            passing = lax.ppermute(passing, "kv", pairs)
+            arrived[tier].append((passing, None, back, 0))
+            for moved, d in turn(passing, back, rows):
+                arrived[tier].append((moved, None, back, d))
     return arrived
 
 
@@ -494,13 +514,10 @@
     members = lax.axis_size("tp")
     parts = members // CORES
 
-    kv0 = first_kv(lengths, inputs, wk, wv)
-    queries, kv_rest = other_qkv(lengths, inputs, wq, wk, wv, kv0)
-    own = [kv0, *kv_rest]
-    gathered = [
-        gather_spans(own[tier], reaches[tier], columns) if reaches[tier] > 1 else []
-        for tier in range(batch)
-    ]
+    first = 1
+    shared = sum(reach > 1 for reach in reaches) - first
+    (own, queries), joined = project(lengths, inputs, ((wk, wv), (wq,)), first, shared)
+    gathered = gather_spans(own, joined, first, reaches, columns)
 
     groups = []
     for tiers in together:
@@ -536,7 +553,10 @@
                 )
             )
         groups.append((tiers, keep, got, coming))
-    return finish(lengths, batch, groups)
+    out = None
+    if len(groups) > 1:
+        out = finish(lengths, batch, groups[:-1])
+    return finish(lengths, batch, groups[-1:], out)
 
 
 def tier_reaches(devices, batch, columns):
@@ -567,7 +587,7 @@
         lengths = args[-1]
         common = tier_reaches(devices, batch, columns)
         backwards = range(batch - 1, -1, -1)
-        together = (tuple(backwards[:2]), *((tier,) for tier in backwards[2:]))
+        together = (tuple(backwards[:1]), tuple(backwards[1:-1]), tuple(backwards[-1:]))
         out = layer(common, together, columns, *args)
         reach = jnp.array(common, jnp.int32)
         longer = jnp.sum((lengths[None, :] > reach[:, None] * span).astype(jnp.int32), axis=1)

time: 95.7 us -> 91 us (0.951)
  the two profiles are of different devices: /device:TPU:0 before, /device:TPU:8 now
where the time goes in v2:
time: 91 us; the launch traced here: 90.6 us
  waiting for transfers between devices  41.3 us (45%)
  starting transfers between devices  23.5 us (26%)
  Pallas kernels  20.2 us (22%)
  other arithmetic  3.39 us (4%)
  local copies, waits for them, and re-layouts  1.03 us (1%)
    ppermute x6, waiting for transfers between devices, turn(): found.append((lax.ppermute(x, 'kv', pairs), d))  15.3 us
    ppermute x4, waiting for transfers between devices, gather_spans(): passing = lax.ppermute(passing, 'kv', pairs)  13.4 us
    ppermute x6, waiting for transfers between devices, swap(): return lax.ppermute(x, ('kv', 'tp'), pairs)  12.6 us
    ppermute x6, starting transfers between devices, turn(): found.append((lax.ppermute(x, 'kv', pairs), d))  11 us
    pallas_call x3, Pallas kernels, attend(): pl.pallas_call(body, in_specs=[SMEM, SMEM, VMEM, *[ANY] * (2 * group + le...  10.5 us
    ppermute x6, starting transfers between devices, swap(): return lax.ppermute(x, ('kv', 'tp'), pairs)  7.26 us
    pallas_call x1, Pallas kernels, project(): pl.pallas_call(body, in_specs=[SMEM] + [ANY] * (1 + len(flat) + len(after...  6.2 us
    ppermute x4, starting transfers between devices, gather_spans(): passing = lax.ppermute(passing, 'kv', pairs)  5.18 us
  transfers between devices with their start and end apart: 16, of which 7 were waited for; matrix products, arithmetic and copies ran while one was open for 4% of the time, Pallas kernels for 14%

profile of v2, /device:TPU:8, one launch (start us, length us, event | category | flops | bytes accessed | tf_op | source)
XLA Modules:
  0.0 90.6 jit_solution(6222744742423784034)
XLA Ops:
  0.0 6.2 %shard_map.84 = (bf16[256,512]{1,0:T(8,128)(2,1)S(1)}, bf16[256,512]{1,0:T(8,128)(2,1)S(1)}, bf16[256,512]{1,0:T(8,128)(2,1)S(1)}, bf16[256,512]{1,0:T(8,128)(2,...) custom-call(s32[4]{0:T(128)} %len_ref.11, ...), custom_call_target="tpu_custom_call" | custom-call | flops 4294967296 | bytes 8388608 | tf_op jit(solution)/shard_map/pallas_call | solution.py:129
  6.2 1.3 %collective-permute-start.40 = (bf16[256,512]{1,0:T(8,128)(2,1)S(1)}, bf16[256,512]{1,0:T(8,128)(2,1)S(1)}, u32[]{:S(2)}, u32[]{:S(2)}) collective-permute-start(bf16[256,512]{1,0:T(8,128)(2,1)S(1)} %get-tuple-element.67.rest_3_), channel_id=1, source_target_pairs={{0,8},{4,12},{1,9},{5,13},{2,10},{6,14},{3,11},{7,15}} | collective-permute-start | bytes 786440 | tf_op jit(solution)/shard_map/ppermute | solution.py:505
  7.5 1.9 %collective-permute-start.39 = (bf16[2,256,512]{2,1,0:T(8,128)(2,1)S(1)}, bf16[2,256,512]{2,1,0:T(8,128)(2,1)S(1)}, u32[]{:S(2)}, u32[]{:S(2)}) collective-permute-start(bf16[2,256,512]{2,1,0:T(8,128)(2,1)S(1)} %get-tuple-element.68), channel_id=1, source_target_pairs={{0,4},{8,12},{12,8},{1,5},{9,13},{13,9},{2,6},{10,14},{14,10},{3,7... | collective-permute-start | bytes 1572872 | tf_op jit(solution)/shard_map/ppermute | solution.py:487
  9.4 6.9 %collective-permute-done.40.rest_6_ = bf16[256,512]{1,0:T(8,128)(2,1)S(1)} collective-permute-done((bf16[256,512]{1,0:T(8,128)(2,1)S(1)}, bf16[256,512]{1,0:T(8,128)(2,1)S(1)}, u32[]{:S(2)}, u32[]{:S(2)}) %collective-permute-start.40) | collective-permute-done | bytes 262176 | tf_op jit(solution)/shard_map/ppermute | solution.py:505
  16.4 1.9 %collective-permute-start.41 = (bf16[256,512]{1,0:T(8,128)(2,1)S(1)}, bf16[256,512]{1,0:T(8,128)(2,1)S(1)}, u32[]{:S(2)}, u32[]{:S(2)}) collective-permute-start(bf16[256,512]{1,0:T(8,128)(2,1)S(1)} %collective-permute-done.40.rest_6_), channel_id=1, source_target_pairs={{8,12},{12,8},{9,13},{13,9},{10,14},{14,10},{11,15},{15,11}} | collective-permute-start | bytes 786440 | tf_op jit(solution)/shard_map/ppermute | solution.py:487
  18.3 1.9 %collective-permute-start.29 = (bf16[256,512]{1,0:T(8,128)(2,1)S(1)}, bf16[256,512]{1,0:T(8,128)(2,1)S(1)}, u32[]{:S(2)}, u32[]{:S(2)}) collective-permute-start(bf16[256,512]{1,0:T(8,128)(2,1)S(1)} %get-tuple-element.57.rest_1_), channel_id=1, source_target_pairs={{0,8},{4,12},{8,16},{12,20},{16,24},{20,28},{1,9},{5,13},{9,17},{1... | collective-permute-start | bytes 786440 | tf_op jit(solution)/shard_map/ppermute | solution.py:505
  20.2 8.5 %collective-permute-done.41.rest_7_ = bf16[256,512]{1,0:T(8,128)(2,1)S(1)} collective-permute-done((bf16[256,512]{1,0:T(8,128)(2,1)S(1)}, bf16[256,512]{1,0:T(8,128)(2,1)S(1)}, u32[]{:S(2)}, u32[]{:S(2)}) %collective-permute-start.41) | collective-permute-done | bytes 262176 | tf_op jit(solution)/shard_map/ppermute | solution.py:487
  28.7 4.3 %shard_map.87 = (bf16[2,2,256,512]{3,2,1,0:T(8,128)(2,1)S(1)}, bf16[2,2,256,512]{3,2,1,0:T(8,128)(2,1)S(1)}) custom-call(s32[4]{0:T(128)S(1)} %copy-done.8, s32[4,4,32]{2,1,0:T(4,128)S(1)} %copy-done.7, s32[4,4,32]{2,1,0:T(4,128)S(1)} %copy-done.7, bf16[256,512]{1,0:T(8,128)(2,1)S(1)} %get-tuple-element.64.rest_0_, ...), custom_call_target="tpu_custom_call" | custom-call | flops 2147483648 | bytes 6291456 | tf_op jit(solution)/shard_map/pallas_call | solution.py:373
  33.0 1.9 %collective-permute-start.42 = (bf16[2,2,256,512]{3,2,1,0:T(8,128)(2,1)S(1)}, bf16[2,2,256,512]{3,2,1,0:T(8,128)(2,1)S(1)}, u32[]{:S(2)}, u32[]{:S(2)}) collective-permute-start(bf16[2,2,256,512]{3,2,1,0:T(8,128)(2,1)S(1)} %get-tuple-element.70), channel_id=1, source_target_pairs={{0,1},{1,0},{2,3},{3,2},{4,5},{5,4},{6,7},{7,6},{8,9},{9,8},{10,11... | collective-permute-start | bytes 3145736 | tf_op jit(solution)/shard_map/ppermute | solution.py:543
  35.0 1.3 %collective-permute-start.31 = (bf16[256,512]{1,0:T(8,128)(2,1)S(1)}, bf16[256,512]{1,0:T(8,128)(2,1)S(1)}, u32[]{:S(2)}, u32[]{:S(2)}) collective-permute-start(bf16[256,512]{1,0:T(8,128)(2,1)S(1)} %collective-permute-done.29.rest_3_), channel_id=1, source_target_pairs={{8,16},{12,20},{16,24},{20,28},{9,17},{13,21},{17,25},{21,29},{10,... | collective-permute-start | bytes 786440 | tf_op jit(solution)/shard_map/ppermute | solution.py:505
  36.3 6.5 %collective-permute-done.31.rest_5_ = bf16[256,512]{1,0:T(8,128)(2,1)S(1)} collective-permute-done((bf16[256,512]{1,0:T(8,128)(2,1)S(1)}, bf16[256,512]{1,0:T(8,128)(2,1)S(1)}, u32[]{:S(2)}, u32[]{:S(2)}) %collective-permute-start.31) | collective-permute-done | bytes 262176 | tf_op jit(solution)/shard_map/ppermute | solution.py:505
  42.7 0.7 collective-permute-start.33
  43.4 1.9 %collective-permute-start.28 = (bf16[256,512]{1,0:T(8,128)(2,1)S(1)}, bf16[256,512]{1,0:T(8,128)(2,1)S(1)}, u32[]{:S(2)}, u32[]{:S(2)}) collective-permute-start(bf16[256,512]{1,0:T(8,128)(2,1)S(1)} %get-tuple-element.57.rest_1_), channel_id=1, source_target_pairs={{0,4},{8,12},{12,8},{16,20},{20,16},{24,28},{28,24},{1,5},{9,13},{... | collective-permute-start | bytes 786440 | tf_op jit(solution)/shard_map/ppermute | solution.py:487
  45.3 3.9 %collective-permute-start.30 = (bf16[256,512]{1,0:T(8,128)(2,1)S(1)}, bf16[256,512]{1,0:T(8,128)(2,1)S(1)}, u32[]{:S(2)}, u32[]{:S(2)}) collective-permute-start(bf16[256,512]{1,0:T(8,128)(2,1)S(1)} %collective-permute-done.29.rest_3_), channel_id=1, source_target_pairs={{8,12},{12,8},{16,20},{20,16},{24,28},{28,24},{9,13},{13,9},{17,21... | collective-permute-start | bytes 786440 | tf_op jit(solution)/shard_map/ppermute | solution.py:487
  49.3 0.7 collective-permute-start.32
  50.0 0.7 collective-permute-start.34
  50.7 0.8 shard_map.86
  51.5 3.0 %collective-permute-done.28.rest_2_ = bf16[256,512]{1,0:T(8,128)(2,1)S(1)} collective-permute-done((bf16[256,512]{1,0:T(8,128)(2,1)S(1)}, bf16[256,512]{1,0:T(8,128)(2,1)S(1)}, u32[]{:S(2)}, u32[]{:S(2)}) %collective-permute-start.28) | collective-permute-done | bytes 262176 | tf_op jit(solution)/shard_map/ppermute | solution.py:487
  54.5 0.7 collective-permute-start.37
  55.2 3.9 %collective-permute-done.30.rest_4_ = bf16[256,512]{1,0:T(8,128)(2,1)S(1)} collective-permute-done((bf16[256,512]{1,0:T(8,128)(2,1)S(1)}, bf16[256,512]{1,0:T(8,128)(2,1)S(1)}, u32[]{:S(2)}, u32[]{:S(2)}) %collective-permute-start.30) | collective-permute-done | bytes 262176 | tf_op jit(solution)/shard_map/ppermute | solution.py:487
  59.1 5.4 %shard_map.85 = (bf16[2,1,256,512]{3,2,1,0:T(8,128)(2,1)S(1)}, bf16[2,1,256,512]{3,2,1,0:T(8,128)(2,1)S(1)}) custom-call(s32[4]{0:T(128)S(1)} %copy-done.8, s32[4,4,32]{2,1,0:T(4,128)S(1)} %copy-done.7, s32[4,4,32]{2,1,0:T(4,128)S(1)} %copy-done.7, bf16[256,512]{1,0:T(8,128)(2,1)S(1)} %get-tuple-element.56.rest_0_, ...), custom_call_target="tpu_custom_call" | custom-call | flops 1073741824 | bytes 3145728 | tf_op jit(solution)/shard_map/pallas_call | solution.py:373
  64.6 0.9 %fusion.1 = bf16[2,256,512]{2,1,0:T(8,128)(2,1)} fusion(bf16[2,2,256,512]{3,2,1,0:T(8,128)(2,1)S(1)} %collective-permute-done.42.refs_4_, bf16[2,2,256,512]{3,2,1,0:T(8,128)(2,1)S(1)} %get-tuple-element.69.refs_3_), kind=kLoop, calls=%fused_computation.3 | loop fusion | flops 1048576 | bytes 1572864 | tf_op jit(solution)/shard_map/convert_element_type | solution.py:551
  65.5 3.4 %collective-permute-start.43 = (bf16[2,256,512]{2,1,0:T(8,128)(2,1)}, bf16[2,256,512]{2,1,0:T(8,128)(2,1)}, u32[]{:S(2)}, u32[]{:S(2)}) collective-permute-start(bf16[2,256,512]{2,1,0:T(8,128)(2,1)} %fusion.1), channel_id=1, source_target_pairs={{0,2},{1,3},{2,0},{3,1},{4,6},{5,7},{6,4},{7,5},{8,10},{9,11},{10,... | collective-permute-start | bytes 1572872 | tf_op jit(solution)/shard_map/ppermute | solution.py:543
  68.9 0.8 fusion.3
  69.7 0.7 collective-permute-start.38
  70.4 0.9 fusion.2
  72.0 0.6 compare_reduce_fusion
  73.2 9.3 %collective-permute-done.43.refs_5_ = bf16[2,256,512]{2,1,0:T(8,128)(2,1)} collective-permute-done((bf16[2,256,512]{2,1,0:T(8,128)(2,1)}, bf16[2,256,512]{2,1,0:T(8,128)(2,1)}, u32[]{:S(2)}, u32[]{:S(2)}) %collective-permute-start.43) | collective-permute-done | bytes 524320 | tf_op jit(solution)/shard_map/ppermute | solution.py:543
  82.5 1.8 %finish.4.refs_3_ = bf16[4,256,512]{2,1,0:T(8,128)(2,1)S(1)} custom-call(s32[4]{0:T(128)S(1)} %copy-done.8, bf16[2,1,256,512]{3,2,1,0:T(8,128)(2,1)S(1)} %get-tuple-element.62.refs_0_, bf16[2,1,256,512]{3,2,1,0:T(8,128)(2,1)S(1)} %collective-permute-done.37.refs_1_, bf16[1,256,512]{2,1,0:T(8,128)(2,1)S(1)} %collective-permute-done.38.refs_2_, ...), custom_call_target="tpu_custom_call" | custom-call | flops 1572864 | bytes 3145728 | tf_op jit(solution)/shard_map/finish/pallas_call | solution.py:457
  84.3 3.3 %collective-permute-done.36.refs_2_ = bf16[1,256,512]{2,1,0:T(8,128)(2,1)} collective-permute-done((bf16[1,256,512]{2,1,0:T(8,128)(2,1)}, bf16[1,256,512]{2,1,0:T(8,128)(2,1)}, u32[]{:S(2)}, u32[]{:S(2)}) %collective-permute-start.36) | collective-permute-done | bytes 262176 | tf_op jit(solution)/shard_map/ppermute | solution.py:543
  87.7 1.7 %finish.5 = bf16[4,256,512]{2,1,0:T(8,128)(2,1)S(1)} custom-call(s32[4]{0:T(128)S(1)} %copy-done.8, bf16[2,1,256,512]{3,2,1,0:T(8,128)(2,1)S(1)} %copy-done.1, bf16[2,1,256,512]{3,2,1,0:T(8,128)(2,1)S(1)} %copy-done.3, bf16[1,256,512]{2,1,0:T(8,128)(2,1)} %collective-permute-done.36.refs_2_, ...), custom_call_target="tpu_custom_call", output_to_operand_aliasing={{}: (4, {})} | custom-call | flops 524288 | bytes 1048576 | tf_op jit(solution)/shard_map/finish/pallas_call | solution.py:457
  89.6 1.0 %copy-done.4 = bf16[4,256,512]{2,1,0:T(8,128)(2,1)} copy-done((bf16[4,256,512]{2,1,0:T(8,128)(2,1)}, bf16[4,256,512]{2,1,0:T(8,128)(2,1)S(1)}, u32[]{:S(2)}) %copy-start.4) | copy-done | bytes 1048600
  (34 shorter events, 1.1 us)
Async XLA Ops:
  0.0 28.7 %copy-start.8 = (s32[4]{0:T(128)S(1)}, s32[4]{0:T(128)}, u32[]{:S(2)}) copy-start(s32[4]{0:T(128)} %len_ref.11) | copy-start | bytes 52
  0.0 28.7 %copy-start.7 = (s32[4,4,32]{2,1,0:T(4,128)S(1)}, s32[4,4,32]{2,1,0:T(4,128)}, u32[]{:S(2)}) copy-start(s32[4,4,32]{2,1,0:T(4,128)} %names_ref.5) | copy-start | bytes 6148
  0.0 28.7 %copy-start.5 = (bf16[512,2048]{1,0:T(8,128)(2,1)S(1)}, bf16[512,2048]{1,0:T(8,128)(2,1)}, u32[]{:S(2)}) copy-start(bf16[512,2048]{1,0:T(8,128)(2,1)} %rest_8_.1) | copy-start | bytes 6291460
  6.2 10.1 %collective-permute-start.40 = (bf16[256,512]{1,0:T(8,128)(2,1)S(1)}, bf16[256,512]{1,0:T(8,128)(2,1)S(1)}, u32[]{:S(2)}, u32[]{:S(2)}) collective-permute-start(bf16[256,512]{1,0:T(8,128)(2,1)S(1)} %get-tuple-element.67.rest_3_), channel_id=1, source_target_pairs={{0,8},{4,12},{1,9},{5,13},{2,10},{6,14},{3,11},{7,15}} | collective-permute-start | bytes 786440 | tf_op jit(solution)/shard_map/ppermute | solution.py:505
  7.5 21.2 %collective-permute-start.39 = (bf16[2,256,512]{2,1,0:T(8,128)(2,1)S(1)}, bf16[2,256,512]{2,1,0:T(8,128)(2,1)S(1)}, u32[]{:S(2)}, u32[]{:S(2)}) collective-permute-start(bf16[2,256,512]{2,1,0:T(8,128)(2,1)S(1)} %get-tuple-element.68), channel_id=1, source_target_pairs={{0,4},{8,12},{12,8},{1,5},{9,13},{13,9},{2,6},{10,14},{14,10},{3,7... | collective-permute-start | bytes 1572872 | tf_op jit(solution)/shard_map/ppermute | solution.py:487
  16.4 12.3 %collective-permute-start.41 = (bf16[256,512]{1,0:T(8,128)(2,1)S(1)}, bf16[256,512]{1,0:T(8,128)(2,1)S(1)}, u32[]{:S(2)}, u32[]{:S(2)}) collective-permute-start(bf16[256,512]{1,0:T(8,128)(2,1)S(1)} %collective-permute-done.40.rest_6_), channel_id=1, source_target_pairs={{8,12},{12,8},{9,13},{13,9},{10,14},{14,10},{11,15},{15,11}} | collective-permute-start | bytes 786440 | tf_op jit(solution)/shard_map/ppermute | solution.py:487
  18.3 16.7 %collective-permute-start.29 = (bf16[256,512]{1,0:T(8,128)(2,1)S(1)}, bf16[256,512]{1,0:T(8,128)(2,1)S(1)}, u32[]{:S(2)}, u32[]{:S(2)}) collective-permute-start(bf16[256,512]{1,0:T(8,128)(2,1)S(1)} %get-tuple-element.57.rest_1_), channel_id=1, source_target_pairs={{0,8},{4,12},{8,16},{12,20},{16,24},{20,28},{1,9},{5,13},{9,17},{1... | collective-permute-start | bytes 786440 | tf_op jit(solution)/shard_map/ppermute | solution.py:505
  33.0 31.5 %collective-permute-start.42 = (bf16[2,2,256,512]{3,2,1,0:T(8,128)(2,1)S(1)}, bf16[2,2,256,512]{3,2,1,0:T(8,128)(2,1)S(1)}, u32[]{:S(2)}, u32[]{:S(2)}) collective-permute-start(bf16[2,2,256,512]{3,2,1,0:T(8,128)(2,1)S(1)} %get-tuple-element.70), channel_id=1, source_target_pairs={{0,1},{1,0},{2,3},{3,2},{4,5},{5,4},{6,7},{7,6},{8,9},{9,8},{10,11... | collective-permute-start | bytes 3145736 | tf_op jit(solution)/shard_map/ppermute | solution.py:543
  35.0 7.8 %collective-permute-start.31 = (bf16[256,512]{1,0:T(8,128)(2,1)S(1)}, bf16[256,512]{1,0:T(8,128)(2,1)S(1)}, u32[]{:S(2)}, u32[]{:S(2)}) collective-permute-start(bf16[256,512]{1,0:T(8,128)(2,1)S(1)} %collective-permute-done.29.rest_3_), channel_id=1, source_target_pairs={{8,16},{12,20},{16,24},{20,28},{9,17},{13,21},{17,25},{21,29},{10,... | collective-permute-start | bytes 786440 | tf_op jit(solution)/shard_map/ppermute | solution.py:505
  42.7 7.2 %collective-permute-start.33 = (bf16[256,512]{1,0:T(8,128)(2,1)S(1)}, bf16[256,512]{1,0:T(8,128)(2,1)S(1)}, u32[]{:S(2)}, u32[]{:S(2)}) collective-permute-start(bf16[256,512]{1,0:T(8,128)(2,1)S(1)} %collective-permute-done.31.rest_5_), channel_id=1, source_target_pairs={{16,24},{20,28},{17,25},{21,29},{18,26},{22,30},{19,27},{23,31}} | collective-permute-start | bytes 786440 | tf_op jit(solution)/shard_map/ppermute | solution.py:505
  43.4 11.1 %collective-permute-start.28 = (bf16[256,512]{1,0:T(8,128)(2,1)S(1)}, bf16[256,512]{1,0:T(8,128)(2,1)S(1)}, u32[]{:S(2)}, u32[]{:S(2)}) collective-permute-start(bf16[256,512]{1,0:T(8,128)(2,1)S(1)} %get-tuple-element.57.rest_1_), channel_id=1, source_target_pairs={{0,4},{8,12},{12,8},{16,20},{20,16},{24,28},{28,24},{1,5},{9,13},{... | collective-permute-start | bytes 786440 | tf_op jit(solution)/shard_map/ppermute | solution.py:487
  45.3 13.7 %collective-permute-start.30 = (bf16[256,512]{1,0:T(8,128)(2,1)S(1)}, bf16[256,512]{1,0:T(8,128)(2,1)S(1)}, u32[]{:S(2)}, u32[]{:S(2)}) collective-permute-start(bf16[256,512]{1,0:T(8,128)(2,1)S(1)} %collective-permute-done.29.rest_3_), channel_id=1, source_target_pairs={{8,12},{12,8},{16,20},{20,16},{24,28},{28,24},{9,13},{13,9},{17,21... | collective-permute-start | bytes 786440 | tf_op jit(solution)/shard_map/ppermute | solution.py:487
  49.3 9.8 %collective-permute-start.32 = (bf16[256,512]{1,0:T(8,128)(2,1)S(1)}, bf16[256,512]{1,0:T(8,128)(2,1)S(1)}, u32[]{:S(2)}, u32[]{:S(2)}) collective-permute-start(bf16[256,512]{1,0:T(8,128)(2,1)S(1)} %collective-permute-done.31.rest_5_), channel_id=1, source_target_pairs={{16,20},{20,16},{24,28},{28,24},{17,21},{21,17},{25,29},{29,25},{1... | collective-permute-start | bytes 786440 | tf_op jit(solution)/shard_map/ppermute | solution.py:487
  50.0 9.1 %collective-permute-start.34 = (bf16[256,512]{1,0:T(8,128)(2,1)S(1)}, bf16[256,512]{1,0:T(8,128)(2,1)S(1)}, u32[]{:S(2)}, u32[]{:S(2)}) collective-permute-start(bf16[256,512]{1,0:T(8,128)(2,1)S(1)} %collective-permute-done.33.rest_7_), channel_id=1, source_target_pairs={{24,28},{28,24},{25,29},{29,25},{26,30},{30,26},{27,31},{31,27}} | collective-permute-start | bytes 786440 | tf_op jit(solution)/shard_map/ppermute | solution.py:487
  54.5 14.4 %collective-permute-start.37 = (bf16[2,1,256,512]{3,2,1,0:T(8,128)(2,1)S(1)}, bf16[2,1,256,512]{3,2,1,0:T(8,128)(2,1)S(1)}, u32[]{:S(2)}, u32[]{:S(2)}) collective-permute-start(bf16[2,1,256,512]{3,2,1,0:T(8,128)(2,1)S(1)} %get-tuple-element.63), channel_id=1, source_target_pairs={{0,1},{1,0},{2,3},{3,2}} | collective-permute-start | bytes 1572872 | tf_op jit(solution)/shard_map/ppermute | solution.py:543
  64.4 6.0 %copy-start = (bf16[2,1,256,512]{3,2,1,0:T(8,128)(2,1)}, bf16[2,1,256,512]{3,2,1,0:T(8,128)(2,1)S(1)}, u32[]{:S(2)}) copy-start(bf16[2,1,256,512]{3,2,1,0:T(8,128)(2,1)S(1)} %get-tuple-element.58.refs_0_) | copy-start | bytes 1572868
  64.5 7.3 %copy-start.10 = (s32[4]{0:T(128)S(1)}, s32[4]{0:T(128)}, u32[]{:S(2)}) copy-start(s32[4]{0:T(128)} %constant.10) | copy-start | bytes 52
  64.5 5.9 %collective-permute-start.35 = (bf16[2,1,256,512]{3,2,1,0:T(8,128)(2,1)S(1)}, bf16[2,1,256,512]{3,2,1,0:T(8,128)(2,1)S(1)}, u32[]{:S(2)}, u32[]{:S(2)}) collective-permute-start(bf16[2,1,256,512]{3,2,1,0:T(8,128)(2,1)S(1)} %get-tuple-element.59), channel_id=1, source_target_pairs={{0,1},{1,0},{2,3},{3,2},{4,5},{5,4},{6,7},{7,6},{8,9},{9,8},{10,11... | collective-permute-start | bytes 1572872 | tf_op jit(solution)/shard_map/ppermute | solution.py:543
  65.5 17.0 %collective-permute-start.43 = (bf16[2,256,512]{2,1,0:T(8,128)(2,1)}, bf16[2,256,512]{2,1,0:T(8,128)(2,1)}, u32[]{:S(2)}, u32[]{:S(2)}) collective-permute-start(bf16[2,256,512]{2,1,0:T(8,128)(2,1)} %fusion.1), channel_id=1, source_target_pairs={{0,2},{1,3},{2,0},{3,1},{4,6},{5,7},{6,4},{7,5},{8,10},{9,11},{10,... | collective-permute-start | bytes 1572872 | tf_op jit(solution)/shard_map/ppermute | solution.py:543
  69.7 3.5 %collective-permute-start.38 = (bf16[1,256,512]{2,1,0:T(8,128)(2,1)}, bf16[1,256,512]{2,1,0:T(8,128)(2,1)S(1)}, u32[]{:S(2)}, u32[]{:S(2)}) collective-permute-start(bf16[1,256,512]{2,1,0:T(8,128)(2,1)} %fusion.3), channel_id=1, source_target_pairs={{0,2},{1,3},{2,0},{3,1}} | collective-permute-start | bytes 786440 | tf_op jit(solution)/shard_map/ppermute | solution.py:543
  70.4 0.9 copy-start.2
  71.3 16.3 %collective-permute-start.36 = (bf16[1,256,512]{2,1,0:T(8,128)(2,1)}, bf16[1,256,512]{2,1,0:T(8,128)(2,1)}, u32[]{:S(2)}, u32[]{:S(2)}) collective-permute-start(bf16[1,256,512]{2,1,0:T(8,128)(2,1)} %fusion.2), channel_id=1, source_target_pairs={{0,2},{1,3},{2,0},{3,1},{4,6},{5,7},{6,4},{7,5},{8,10},{9,11},{10,... | collective-permute-start | bytes 786440 | tf_op jit(solution)/shard_map/ppermute | solution.py:543
  73.2 14.5 %copy-start.1 = (bf16[2,1,256,512]{3,2,1,0:T(8,128)(2,1)S(1)}, bf16[2,1,256,512]{3,2,1,0:T(8,128)(2,1)}, u32[]{:S(2)}) copy-start(bf16[2,1,256,512]{3,2,1,0:T(8,128)(2,1)} %copy-done) | copy-start | bytes 1572868
  73.2 14.4 %copy-start.3 = (bf16[2,1,256,512]{3,2,1,0:T(8,128)(2,1)S(1)}, bf16[2,1,256,512]{3,2,1,0:T(8,128)(2,1)}, u32[]{:S(2)}) copy-start(bf16[2,1,256,512]{3,2,1,0:T(8,128)(2,1)} %copy-done.2) | copy-start | bytes 1572868
  73.2 14.4 %copy-start.6 = (bf16[512,2048]{1,0:T(8,128)(2,1)S(1)}, bf16[512,2048]{1,0:T(8,128)(2,1)}, u32[]{:S(2)}) copy-start(bf16[512,2048]{1,0:T(8,128)(2,1)} %rest_8_.1) | copy-start | bytes 6291460
  73.2 14.4 %copy-start.9 = (bf16[2048,256]{1,0:T(8,128)(2,1)S(1)}, bf16[2048,256]{1,0:T(8,128)(2,1)}, u32[]{:S(2)}) copy-start(bf16[2048,256]{1,0:T(8,128)(2,1)} %refs_0_.1) | copy-start | bytes 3145732
  89.6 1.0 %copy-start.4 = (bf16[4,256,512]{2,1,0:T(8,128)(2,1)}, bf16[4,256,512]{2,1,0:T(8,128)(2,1)S(1)}, u32[]{:S(2)}) copy-start(bf16[4,256,512]{2,1,0:T(8,128)(2,1)S(1)} %get-tuple-element.156) | copy-start | bytes 3145732

commit v3 on v2

--- a/solution.py
+++ b/solution.py
@@ -400,23 +400,23 @@
 
 
 def finish(lengths, batch, groups, before=None):
-    parts, _, span, piece = groups[0][1].shape
+    _, span, piece = groups[0][1].shape
+    parts = 1 + len(groups[0][2])
     every = [(tier, g, at) for at, group in enumerate(groups) for g, tier in enumerate(group[0])]
-    each = 1 + parts
+    each = parts
 
     def body(len_ref, *refs):
         given = refs[: each * len(groups)]
-        out_ref, terms, sums, in_sem, out_sem = refs[-5:]
+        out_ref, nears, terms, sums, in_sem, out_sem = refs[-6:]
         here = lax.axis_index("kv")
         seqs = [nth_longest(len_ref, tier) for tier, _, _ in every]
 
         def loads(n):
             _, g, at = every[n]
             mine = given[at * each : (at + 1) * each]
-            sources = [mine[0].at[0, g], mine[1].at[0, g]] + [ref.at[g] for ref in mine[2:]]
-            return [
-                pltpu.make_async_copy(source, terms.at[n, i], in_sem.at[n, i])
-                for i, source in enumerate(sources)
+            return [pltpu.make_async_copy(mine[0].at[g], nears.at[n], in_sem.at[n, 0])] + [
+                pltpu.make_async_copy(ref.at[g], terms.at[n, i], in_sem.at[n, 1 + i])
+                for i, ref in enumerate(mine[1:])
             ]
 
         def store(n):
@@ -436,8 +436,8 @@
             def _():
                 for load in loads(n):
                     load.wait()
-                total = terms[n, 0].astype(jnp.float32)
-                for i in range(1, each):
+                total = nears[n]
+                for i in range(each - 1):
                     total = total + terms[n, i].astype(jnp.float32)
                 sums[n] = total.astype(sums.dtype)
 
@@ -449,7 +449,7 @@
         for n in range(len(every)):
             store(n).wait()
 
-    operands = [part for _, keep, got, coming in groups for part in (keep, got, *coming)]
+    operands = [part for _, near, coming in groups for part in (near, *coming)]
     aliases = {}
     if before is not None:
         aliases = {1 + len(operands): 0}
@@ -460,6 +460,7 @@
         out_specs=ANY,
         out_shape=jax.ShapeDtypeStruct((batch, span, piece), jnp.bfloat16),
         scratch_shapes=[
+            pltpu.VMEM((len(every), span, piece), jnp.float32),
             pltpu.VMEM((len(every), each, span, piece), jnp.bfloat16),
             pltpu.VMEM((len(every), span, piece), jnp.bfloat16),
             pltpu.SemaphoreType.DMA((len(every), each)),
@@ -552,7 +553,8 @@
                     lambda t, far=far: ((t // CORES + far) % parts) * CORES + t % CORES,
                 )
             )
-        groups.append((tiers, keep, got, coming))
+        near = keep[0].astype(jnp.float32) + got[0].astype(jnp.float32)
+        groups.append((tiers, near, coming))
     out = None
     if len(groups) > 1:
         out = finish(lengths, batch, groups[:-1])

time: 91 us -> 90.1 us (level)
  Pallas kernels: 20.2 us -> 18.3 us
  waiting for transfers between devices: 41.3 us -> 42.7 us
    pallas_call x2, Pallas kernels: 3.51 us -> 1.62 us  [finish(): pl.pallas_call(body, in_specs=[SMEM] + [ANY] * len(operands), out_specs=A...]
    ppermute x6, waiting for transfers between devices: 12.6 us -> 14 us  [swap(): return lax.ppermute(x, ('kv', 'tp'), pairs)]
  transfers between devices with their start and end apart: 16 -> 16, of which waited for: 7 -> 7; matrix products, arithmetic and copies ran while one was open for 4% -> 3% of each run, Pallas kernels for 14% -> 13%
where the time goes in v3:
time: 90.1 us; the launch traced here: 89.7 us
  waiting for transfers between devices  42.7 us (47%)
  starting transfers between devices  23.7 us (26%)
  Pallas kernels  18.3 us (20%)
  other arithmetic  2.89 us (3%)
  local copies, waits for them, and re-layouts  0.99 us (1%)
  between operations  0.92 us (1%)
    ppermute x6, waiting for transfers between devices, turn(): found.append((lax.ppermute(x, 'kv', pairs), d))  15.3 us
    ppermute x6, waiting for transfers between devices, swap(): return lax.ppermute(x, ('kv', 'tp'), pairs)  14 us
    ppermute x4, waiting for transfers between devices, gather_spans(): passing = lax.ppermute(passing, 'kv', pairs)  13.4 us
    ppermute x6, starting transfers between devices, turn(): found.append((lax.ppermute(x, 'kv', pairs), d))  11 us
    pallas_call x3, Pallas kernels, attend(): pl.pallas_call(body, in_specs=[SMEM, SMEM, VMEM, *[ANY] * (2 * group + le...  10.5 us
    ppermute x6, starting transfers between devices, swap(): return lax.ppermute(x, ('kv', 'tp'), pairs)  7.46 us
    pallas_call x1, Pallas kernels, project(): pl.pallas_call(body, in_specs=[SMEM] + [ANY] * (1 + len(flat) + len(after...  6.2 us
    ppermute x4, starting transfers between devices, gather_spans(): passing = lax.ppermute(passing, 'kv', pairs)  5.18 us
  transfers between devices with their start and end apart: 16, of which 7 were waited for; matrix products, arithmetic and copies ran while one was open for 3% of the time, Pallas kernels for 13%

profile of v3, /device:TPU:8, one launch (start us, length us, event | category | flops | bytes accessed | tf_op | source)
XLA Modules:
  0.0 89.7 jit_solution(12645641952833481204)
XLA Ops:
  0.0 6.2 %shard_map.84 = (bf16[256,512]{1,0:T(8,128)(2,1)S(1)}, bf16[256,512]{1,0:T(8,128)(2,1)S(1)}, bf16[256,512]{1,0:T(8,128)(2,1)S(1)}, bf16[256,512]{1,0:T(8,128)(2,...) custom-call(s32[4]{0:T(128)} %len_ref.11, ...), custom_call_target="tpu_custom_call" | custom-call | flops 4294967296 | bytes 8388608 | tf_op jit(solution)/shard_map/pallas_call | solution.py:129
  6.2 1.3 %collective-permute-start.40 = (bf16[256,512]{1,0:T(8,128)(2,1)S(1)}, bf16[256,512]{1,0:T(8,128)(2,1)S(1)}, u32[]{:S(2)}, u32[]{:S(2)}) collective-permute-start(bf16[256,512]{1,0:T(8,128)(2,1)S(1)} %get-tuple-element.67.rest_3_), channel_id=1, source_target_pairs={{0,8},{4,12},{1,9},{5,13},{2,10},{6,14},{3,11},{7,15}} | collective-permute-start | bytes 786440 | tf_op jit(solution)/shard_map/ppermute | solution.py:506
  7.5 1.9 %collective-permute-start.39 = (bf16[2,256,512]{2,1,0:T(8,128)(2,1)S(1)}, bf16[2,256,512]{2,1,0:T(8,128)(2,1)S(1)}, u32[]{:S(2)}, u32[]{:S(2)}) collective-permute-start(bf16[2,256,512]{2,1,0:T(8,128)(2,1)S(1)} %get-tuple-element.68), channel_id=1, source_target_pairs={{0,4},{8,12},{12,8},{1,5},{9,13},{13,9},{2,6},{10,14},{14,10},{3,7... | collective-permute-start | bytes 1572872 | tf_op jit(solution)/shard_map/ppermute | solution.py:488
  9.4 6.9 %collective-permute-done.40.rest_6_ = bf16[256,512]{1,0:T(8,128)(2,1)S(1)} collective-permute-done((bf16[256,512]{1,0:T(8,128)(2,1)S(1)}, bf16[256,512]{1,0:T(8,128)(2,1)S(1)}, u32[]{:S(2)}, u32[]{:S(2)}) %collective-permute-start.40) | collective-permute-done | bytes 262176 | tf_op jit(solution)/shard_map/ppermute | solution.py:506
  16.4 1.9 %collective-permute-start.41 = (bf16[256,512]{1,0:T(8,128)(2,1)S(1)}, bf16[256,512]{1,0:T(8,128)(2,1)S(1)}, u32[]{:S(2)}, u32[]{:S(2)}) collective-permute-start(bf16[256,512]{1,0:T(8,128)(2,1)S(1)} %collective-permute-done.40.rest_6_), channel_id=1, source_target_pairs={{8,12},{12,8},{9,13},{13,9},{10,14},{14,10},{11,15},{15,11}} | collective-permute-start | bytes 786440 | tf_op jit(solution)/shard_map/ppermute | solution.py:488
  18.3 1.9 %collective-permute-start.29 = (bf16[256,512]{1,0:T(8,128)(2,1)S(1)}, bf16[256,512]{1,0:T(8,128)(2,1)S(1)}, u32[]{:S(2)}, u32[]{:S(2)}) collective-permute-start(bf16[256,512]{1,0:T(8,128)(2,1)S(1)} %get-tuple-element.57.rest_1_), channel_id=1, source_target_pairs={{0,8},{4,12},{8,16},{12,20},{16,24},{20,28},{1,9},{5,13},{9,17},{1... | collective-permute-start | bytes 786440 | tf_op jit(solution)/shard_map/ppermute | solution.py:506
  20.2 8.5 %collective-permute-done.41.rest_7_ = bf16[256,512]{1,0:T(8,128)(2,1)S(1)} collective-permute-done((bf16[256,512]{1,0:T(8,128)(2,1)S(1)}, bf16[256,512]{1,0:T(8,128)(2,1)S(1)}, u32[]{:S(2)}, u32[]{:S(2)}) %collective-permute-start.41) | collective-permute-done | bytes 262176 | tf_op jit(solution)/shard_map/ppermute | solution.py:488
  28.7 4.3 %shard_map.87 = (bf16[2,2,256,512]{3,2,1,0:T(8,128)(2,1)S(1)}, bf16[2,2,256,512]{3,2,1,0:T(8,128)(2,1)S(1)}) custom-call(s32[4]{0:T(128)S(1)} %copy-done.4, s32[4,4,32]{2,1,0:T(4,128)S(1)} %copy-done.3, s32[4,4,32]{2,1,0:T(4,128)S(1)} %copy-done.3, bf16[256,512]{1,0:T(8,128)(2,1)S(1)} %get-tuple-element.64.rest_0_, ...), custom_call_target="tpu_custom_call" | custom-call | flops 2147483648 | bytes 6291456 | tf_op jit(solution)/shard_map/pallas_call | solution.py:373
  33.0 1.9 %collective-permute-start.42 = (bf16[2,2,256,512]{3,2,1,0:T(8,128)(2,1)S(1)}, bf16[2,2,256,512]{3,2,1,0:T(8,128)(2,1)S(1)}, u32[]{:S(2)}, u32[]{:S(2)}) collective-permute-start(bf16[2,2,256,512]{3,2,1,0:T(8,128)(2,1)S(1)} %get-tuple-element.70), channel_id=1, source_target_pairs={{0,1},{1,0},{2,3},{3,2},{4,5},{5,4},{6,7},{7,6},{8,9},{9,8},{10,11... | collective-permute-start | bytes 3145736 | tf_op jit(solution)/shard_map/ppermute | solution.py:544
  35.0 1.3 %collective-permute-start.31 = (bf16[256,512]{1,0:T(8,128)(2,1)S(1)}, bf16[256,512]{1,0:T(8,128)(2,1)S(1)}, u32[]{:S(2)}, u32[]{:S(2)}) collective-permute-start(bf16[256,512]{1,0:T(8,128)(2,1)S(1)} %collective-permute-done.29.rest_3_), channel_id=1, source_target_pairs={{8,16},{12,20},{16,24},{20,28},{9,17},{13,21},{17,25},{21,29},{10,... | collective-permute-start | bytes 786440 | tf_op jit(solution)/shard_map/ppermute | solution.py:506
  36.3 6.5 %collective-permute-done.31.rest_5_ = bf16[256,512]{1,0:T(8,128)(2,1)S(1)} collective-permute-done((bf16[256,512]{1,0:T(8,128)(2,1)S(1)}, bf16[256,512]{1,0:T(8,128)(2,1)S(1)}, u32[]{:S(2)}, u32[]{:S(2)}) %collective-permute-start.31) | collective-permute-done | bytes 262176 | tf_op jit(solution)/shard_map/ppermute | solution.py:506
  42.7 0.7 collective-permute-start.33
  43.4 1.9 %collective-permute-start.28 = (bf16[256,512]{1,0:T(8,128)(2,1)S(1)}, bf16[256,512]{1,0:T(8,128)(2,1)S(1)}, u32[]{:S(2)}, u32[]{:S(2)}) collective-permute-start(bf16[256,512]{1,0:T(8,128)(2,1)S(1)} %get-tuple-element.57.rest_1_), channel_id=1, source_target_pairs={{0,4},{8,12},{12,8},{16,20},{20,16},{24,28},{28,24},{1,5},{9,13},{... | collective-permute-start | bytes 786440 | tf_op jit(solution)/shard_map/ppermute | solution.py:488
  45.3 3.9 %collective-permute-start.30 = (bf16[256,512]{1,0:T(8,128)(2,1)S(1)}, bf16[256,512]{1,0:T(8,128)(2,1)S(1)}, u32[]{:S(2)}, u32[]{:S(2)}) collective-permute-start(bf16[256,512]{1,0:T(8,128)(2,1)S(1)} %collective-permute-done.29.rest_3_), channel_id=1, source_target_pairs={{8,12},{12,8},{16,20},{20,16},{24,28},{28,24},{9,13},{13,9},{17,21... | collective-permute-start | bytes 786440 | tf_op jit(solution)/shard_map/ppermute | solution.py:488
  49.3 0.7 collective-permute-start.32
  50.0 0.7 collective-permute-start.34
  50.7 0.8 shard_map.86
  51.5 3.0 %collective-permute-done.28.rest_2_ = bf16[256,512]{1,0:T(8,128)(2,1)S(1)} collective-permute-done((bf16[256,512]{1,0:T(8,128)(2,1)S(1)}, bf16[256,512]{1,0:T(8,128)(2,1)S(1)}, u32[]{:S(2)}, u32[]{:S(2)}) %collective-permute-start.28) | collective-permute-done | bytes 262176 | tf_op jit(solution)/shard_map/ppermute | solution.py:488
  54.5 0.7 collective-permute-start.37
  55.2 3.9 %collective-permute-done.30.rest_4_ = bf16[256,512]{1,0:T(8,128)(2,1)S(1)} collective-permute-done((bf16[256,512]{1,0:T(8,128)(2,1)S(1)}, bf16[256,512]{1,0:T(8,128)(2,1)S(1)}, u32[]{:S(2)}, u32[]{:S(2)}) %collective-permute-start.30) | collective-permute-done | bytes 262176 | tf_op jit(solution)/shard_map/ppermute | solution.py:488
  59.1 5.4 %shard_map.85 = (bf16[2,1,256,512]{3,2,1,0:T(8,128)(2,1)S(1)}, bf16[2,1,256,512]{3,2,1,0:T(8,128)(2,1)S(1)}) custom-call(s32[4]{0:T(128)S(1)} %copy-done.4, s32[4,4,32]{2,1,0:T(4,128)S(1)} %copy-done.3, s32[4,4,32]{2,1,0:T(4,128)S(1)} %copy-done.3, bf16[256,512]{1,0:T(8,128)(2,1)S(1)} %get-tuple-element.56.rest_0_, ...), custom_call_target="tpu_custom_call" | custom-call | flops 1073741824 | bytes 3145728 | tf_op jit(solution)/shard_map/pallas_call | solution.py:373
  64.5 1.1 %fusion.1 = (bf16[2,256,512]{2,1,0:T(8,128)(2,1)}, f32[2,256,512]{2,1,0:T(8,128)S(1)}) fusion(bf16[2,2,256,512]{3,2,1,0:T(8,128)(2,1)S(1)} %collective-permute-done.42, bf16[2,2,256,512]{3,2,1,0:T(8,128)(2,1)S(1)} %get-tuple-element.69), kind=kLoop, calls=%fused_computation.5 | loop fusion | flops 1835008 | bytes 3670016 | tf_op jit(solution)/shard_map/convert_element_type | solution.py:552
  65.6 3.5 %collective-permute-start.43 = (bf16[2,256,512]{2,1,0:T(8,128)(2,1)}, bf16[2,256,512]{2,1,0:T(8,128)(2,1)S(1)}, u32[]{:S(2)}, u32[]{:S(2)}) collective-permute-start(bf16[2,256,512]{2,1,0:T(8,128)(2,1)} %get-tuple-element.74), channel_id=1, source_target_pairs={{0,2},{1,3},{2,0},{3,1},{4,6},{5,7},{6,4},{7,5},{8,10},{9,11},{10,... | collective-permute-start | bytes 1572872 | tf_op jit(solution)/shard_map/ppermute | solution.py:544
  69.2 0.8 fusion.3
  70.0 0.7 collective-permute-start.38
  70.8 0.6 collective-permute-start.36
  71.6 0.7 compare_reduce_fusion
  72.9 9.7 %collective-permute-done.43.refs_3_ = bf16[2,256,512]{2,1,0:T(8,128)(2,1)S(1)} collective-permute-done((bf16[2,256,512]{2,1,0:T(8,128)(2,1)}, bf16[2,256,512]{2,1,0:T(8,128)(2,1)S(1)}, u32[]{:S(2)}, u32[]{:S(2)}) %collective-permute-start.43) | collective-permute-done | bytes 524320 | tf_op jit(solution)/shard_map/ppermute | solution.py:544
  82.6 0.9 finish.4.refs_2_
  83.5 4.2 %collective-permute-done.36.refs_1_ = bf16[1,256,512]{2,1,0:T(8,128)(2,1)S(1)} collective-permute-done((bf16[1,256,512]{2,1,0:T(8,128)(2,1)S(1)}, bf16[1,256,512]{2,1,0:T(8,128)(2,1)S(1)}, u32[]{:S(2)}, u32[]{:S(2)}) %collective-permute-start.36) | collective-permute-done | bytes 262176 | tf_op jit(solution)/shard_map/ppermute | solution.py:544
  87.8 0.7 finish.5
  88.8 1.0 %copy-done = bf16[4,256,512]{2,1,0:T(8,128)(2,1)} copy-done((bf16[4,256,512]{2,1,0:T(8,128)(2,1)}, bf16[4,256,512]{2,1,0:T(8,128)(2,1)S(1)}, u32[]{:S(2)}) %copy-start) | copy-done | bytes 1048600
  (26 shorter events, 0.7 us)
Async XLA Ops:
  0.0 28.7 %copy-start.4 = (s32[4]{0:T(128)S(1)}, s32[4]{0:T(128)}, u32[]{:S(2)}) copy-start(s32[4]{0:T(128)} %len_ref.11) | copy-start | bytes 52
  0.0 28.7 %copy-start.3 = (s32[4,4,32]{2,1,0:T(4,128)S(1)}, s32[4,4,32]{2,1,0:T(4,128)}, u32[]{:S(2)}) copy-start(s32[4,4,32]{2,1,0:T(4,128)} %names_ref.5) | copy-start | bytes 6148
  0.0 28.7 %copy-start.1 = (bf16[512,2048]{1,0:T(8,128)(2,1)S(1)}, bf16[512,2048]{1,0:T(8,128)(2,1)}, u32[]{:S(2)}) copy-start(bf16[512,2048]{1,0:T(8,128)(2,1)} %rest_8_.1) | copy-start | bytes 6291460
  6.2 10.1 %collective-permute-start.40 = (bf16[256,512]{1,0:T(8,128)(2,1)S(1)}, bf16[256,512]{1,0:T(8,128)(2,1)S(1)}, u32[]{:S(2)}, u32[]{:S(2)}) collective-permute-start(bf16[256,512]{1,0:T(8,128)(2,1)S(1)} %get-tuple-element.67.rest_3_), channel_id=1, source_target_pairs={{0,8},{4,12},{1,9},{5,13},{2,10},{6,14},{3,11},{7,15}} | collective-permute-start | bytes 786440 | tf_op jit(solution)/shard_map/ppermute | solution.py:506
  7.5 21.2 %collective-permute-start.39 = (bf16[2,256,512]{2,1,0:T(8,128)(2,1)S(1)}, bf16[2,256,512]{2,1,0:T(8,128)(2,1)S(1)}, u32[]{:S(2)}, u32[]{:S(2)}) collective-permute-start(bf16[2,256,512]{2,1,0:T(8,128)(2,1)S(1)} %get-tuple-element.68), channel_id=1, source_target_pairs={{0,4},{8,12},{12,8},{1,5},{9,13},{13,9},{2,6},{10,14},{14,10},{3,7... | collective-permute-start | bytes 1572872 | tf_op jit(solution)/shard_map/ppermute | solution.py:488
  16.4 12.3 %collective-permute-start.41 = (bf16[256,512]{1,0:T(8,128)(2,1)S(1)}, bf16[256,512]{1,0:T(8,128)(2,1)S(1)}, u32[]{:S(2)}, u32[]{:S(2)}) collective-permute-start(bf16[256,512]{1,0:T(8,128)(2,1)S(1)} %collective-permute-done.40.rest_6_), channel_id=1, source_target_pairs={{8,12},{12,8},{9,13},{13,9},{10,14},{14,10},{11,15},{15,11}} | collective-permute-start | bytes 786440 | tf_op jit(solution)/shard_map/ppermute | solution.py:488
  18.3 16.7 %collective-permute-start.29 = (bf16[256,512]{1,0:T(8,128)(2,1)S(1)}, bf16[256,512]{1,0:T(8,128)(2,1)S(1)}, u32[]{:S(2)}, u32[]{:S(2)}) collective-permute-start(bf16[256,512]{1,0:T(8,128)(2,1)S(1)} %get-tuple-element.57.rest_1_), channel_id=1, source_target_pairs={{0,8},{4,12},{8,16},{12,20},{16,24},{20,28},{1,9},{5,13},{9,17},{1... | collective-permute-start | bytes 786440 | tf_op jit(solution)/shard_map/ppermute | solution.py:506
  33.0 31.5 %collective-permute-start.42 = (bf16[2,2,256,512]{3,2,1,0:T(8,128)(2,1)S(1)}, bf16[2,2,256,512]{3,2,1,0:T(8,128)(2,1)S(1)}, u32[]{:S(2)}, u32[]{:S(2)}) collective-permute-start(bf16[2,2,256,512]{3,2,1,0:T(8,128)(2,1)S(1)} %get-tuple-element.70), channel_id=1, source_target_pairs={{0,1},{1,0},{2,3},{3,2},{4,5},{5,4},{6,7},{7,6},{8,9},{9,8},{10,11... | collective-permute-start | bytes 3145736 | tf_op jit(solution)/shard_map/ppermute | solution.py:544
  35.0 7.8 %collective-permute-start.31 = (bf16[256,512]{1,0:T(8,128)(2,1)S(1)}, bf16[256,512]{1,0:T(8,128)(2,1)S(1)}, u32[]{:S(2)}, u32[]{:S(2)}) collective-permute-start(bf16[256,512]{1,0:T(8,128)(2,1)S(1)} %collective-permute-done.29.rest_3_), channel_id=1, source_target_pairs={{8,16},{12,20},{16,24},{20,28},{9,17},{13,21},{17,25},{21,29},{10,... | collective-permute-start | bytes 786440 | tf_op jit(solution)/shard_map/ppermute | solution.py:506
  42.7 7.2 %collective-permute-start.33 = (bf16[256,512]{1,0:T(8,128)(2,1)S(1)}, bf16[256,512]{1,0:T(8,128)(2,1)S(1)}, u32[]{:S(2)}, u32[]{:S(2)}) collective-permute-start(bf16[256,512]{1,0:T(8,128)(2,1)S(1)} %collective-permute-done.31.rest_5_), channel_id=1, source_target_pairs={{16,24},{20,28},{17,25},{21,29},{18,26},{22,30},{19,27},{23,31}} | collective-permute-start | bytes 786440 | tf_op jit(solution)/shard_map/ppermute | solution.py:506
  43.4 11.1 %collective-permute-start.28 = (bf16[256,512]{1,0:T(8,128)(2,1)S(1)}, bf16[256,512]{1,0:T(8,128)(2,1)S(1)}, u32[]{:S(2)}, u32[]{:S(2)}) collective-permute-start(bf16[256,512]{1,0:T(8,128)(2,1)S(1)} %get-tuple-element.57.rest_1_), channel_id=1, source_target_pairs={{0,4},{8,12},{12,8},{16,20},{20,16},{24,28},{28,24},{1,5},{9,13},{... | collective-permute-start | bytes 786440 | tf_op jit(solution)/shard_map/ppermute | solution.py:488
  45.3 13.7 %collective-permute-start.30 = (bf16[256,512]{1,0:T(8,128)(2,1)S(1)}, bf16[256,512]{1,0:T(8,128)(2,1)S(1)}, u32[]{:S(2)}, u32[]{:S(2)}) collective-permute-start(bf16[256,512]{1,0:T(8,128)(2,1)S(1)} %collective-permute-done.29.rest_3_), channel_id=1, source_target_pairs={{8,12},{12,8},{16,20},{20,16},{24,28},{28,24},{9,13},{13,9},{17,21... | collective-permute-start | bytes 786440 | tf_op jit(solution)/shard_map/ppermute | solution.py:488
  49.3 9.8 %collective-permute-start.32 = (bf16[256,512]{1,0:T(8,128)(2,1)S(1)}, bf16[256,512]{1,0:T(8,128)(2,1)S(1)}, u32[]{:S(2)}, u32[]{:S(2)}) collective-permute-start(bf16[256,512]{1,0:T(8,128)(2,1)S(1)} %collective-permute-done.31.rest_5_), channel_id=1, source_target_pairs={{16,20},{20,16},{24,28},{28,24},{17,21},{21,17},{25,29},{29,25},{1... | collective-permute-start | bytes 786440 | tf_op jit(solution)/shard_map/ppermute | solution.py:488
  50.0 9.1 %collective-permute-start.34 = (bf16[256,512]{1,0:T(8,128)(2,1)S(1)}, bf16[256,512]{1,0:T(8,128)(2,1)S(1)}, u32[]{:S(2)}, u32[]{:S(2)}) collective-permute-start(bf16[256,512]{1,0:T(8,128)(2,1)S(1)} %collective-permute-done.33.rest_7_), channel_id=1, source_target_pairs={{24,28},{28,24},{25,29},{29,25},{26,30},{30,26},{27,31},{31,27}} | collective-permute-start | bytes 786440 | tf_op jit(solution)/shard_map/ppermute | solution.py:488
  54.5 14.7 %collective-permute-start.37 = (bf16[2,1,256,512]{3,2,1,0:T(8,128)(2,1)S(1)}, bf16[2,1,256,512]{3,2,1,0:T(8,128)(2,1)S(1)}, u32[]{:S(2)}, u32[]{:S(2)}) collective-permute-start(bf16[2,1,256,512]{3,2,1,0:T(8,128)(2,1)S(1)} %get-tuple-element.63), channel_id=1, source_target_pairs={{0,1},{1,0},{2,3},{3,2}} | collective-permute-start | bytes 1572872 | tf_op jit(solution)/shard_map/ppermute | solution.py:544
  64.4 6.2 %collective-permute-start.35 = (bf16[2,1,256,512]{3,2,1,0:T(8,128)(2,1)S(1)}, bf16[2,1,256,512]{3,2,1,0:T(8,128)(2,1)S(1)}, u32[]{:S(2)}, u32[]{:S(2)}) collective-permute-start(bf16[2,1,256,512]{3,2,1,0:T(8,128)(2,1)S(1)} %get-tuple-element.59), channel_id=1, source_target_pairs={{0,1},{1,0},{2,3},{3,2},{4,5},{5,4},{6,7},{7,6},{8,9},{9,8},{10,11... | collective-permute-start | bytes 1572872 | tf_op jit(solution)/shard_map/ppermute | solution.py:544
  65.6 5.8 %copy-start.6 = (s32[4]{0:T(128)S(1)}, s32[4]{0:T(128)}, u32[]{:S(2)}) copy-start(s32[4]{0:T(128)} %constant.10) | copy-start | bytes 52
  65.6 17.0 %collective-permute-start.43 = (bf16[2,256,512]{2,1,0:T(8,128)(2,1)}, bf16[2,256,512]{2,1,0:T(8,128)(2,1)S(1)}, u32[]{:S(2)}, u32[]{:S(2)}) collective-permute-start(bf16[2,256,512]{2,1,0:T(8,128)(2,1)} %get-tuple-element.74), channel_id=1, source_target_pairs={{0,2},{1,3},{2,0},{3,1},{4,6},{5,7},{6,4},{7,5},{8,10},{9,11},{10,... | collective-permute-start | bytes 1572872 | tf_op jit(solution)/shard_map/ppermute | solution.py:544
  70.0 2.9 %collective-permute-start.38 = (bf16[1,256,512]{2,1,0:T(8,128)(2,1)}, bf16[1,256,512]{2,1,0:T(8,128)(2,1)S(1)}, u32[]{:S(2)}, u32[]{:S(2)}) collective-permute-start(bf16[1,256,512]{2,1,0:T(8,128)(2,1)} %get-tuple-element.76), channel_id=1, source_target_pairs={{0,2},{1,3},{2,0},{3,1}} | collective-permute-start | bytes 786440 | tf_op jit(solution)/shard_map/ppermute | solution.py:544
  70.8 17.0 %collective-permute-start.36 = (bf16[1,256,512]{2,1,0:T(8,128)(2,1)S(1)}, bf16[1,256,512]{2,1,0:T(8,128)(2,1)S(1)}, u32[]{:S(2)}, u32[]{:S(2)}) collective-permute-start(bf16[1,256,512]{2,1,0:T(8,128)(2,1)S(1)} %get-tuple-element.78), channel_id=1, source_target_pairs={{0,2},{1,3},{2,0},{3,1},{4,6},{5,7},{6,4},{7,5},{8,10},{9,11},{10,... | collective-permute-start | bytes 786440 | tf_op jit(solution)/shard_map/ppermute | solution.py:544
  72.9 14.9 %copy-start.2 = (bf16[512,2048]{1,0:T(8,128)(2,1)S(1)}, bf16[512,2048]{1,0:T(8,128)(2,1)}, u32[]{:S(2)}) copy-start(bf16[512,2048]{1,0:T(8,128)(2,1)} %rest_8_.1) | copy-start | bytes 6291460
  72.9 14.9 %copy-start.5 = (bf16[2048,256]{1,0:T(8,128)(2,1)S(1)}, bf16[2048,256]{1,0:T(8,128)(2,1)}, u32[]{:S(2)}) copy-start(bf16[2048,256]{1,0:T(8,128)(2,1)} %refs_0_.1) | copy-start | bytes 3145732
  88.8 1.0 %copy-start = (bf16[4,256,512]{2,1,0:T(8,128)(2,1)}, bf16[4,256,512]{2,1,0:T(8,128)(2,1)S(1)}, u32[]{:S(2)}) copy-start(bf16[4,256,512]{2,1,0:T(8,128)(2,1)S(1)} %get-tuple-element.162) | copy-start | bytes 3145732

commit v4 on v3

--- a/solution.py
+++ b/solution.py
@@ -86,8 +86,10 @@
 
         @pl.when(alive[0])
         def _():
+            for one in loads[0]:
+                one.start()
             load(0).start()
-            for part in loads:
+            for part in loads[1:]:
                 for one in part:
                     one.start()
 
@@ -458,7 +460,7 @@
         body,
         in_specs=[SMEM] + [ANY] * len(operands),
         out_specs=ANY,
-        out_shape=jax.ShapeDtypeStruct((batch, span, piece), jnp.bfloat16),
+        out_shape=pltpu.HBM((batch, span, piece), jnp.bfloat16),
         scratch_shapes=[
             pltpu.VMEM((len(every), span, piece), jnp.float32),
             pltpu.VMEM((len(every), each, span, piece), jnp.bfloat16),

time: 90.1 us -> 90 us (level)
  Pallas kernels: 18.3 us -> 19.7 us
  local copies, waits for them, and re-layouts: 0.99 us -> 0.03 us
    pallas_call x2, Pallas kernels: 1.62 us -> 3.03 us  [finish(): pl.pallas_call(body, in_specs=[SMEM] + [ANY] * len(operands), out_specs=A...]
    unnamed x14 -> x12, local copies, waits for them, and re-layouts: 0.99 us -> 0.03 us
  transfers between devices with their start and end apart: 16 -> 16, of which waited for: 7 -> 7; matrix products, arithmetic and copies ran while one was open for 3% -> 3% of each run, Pallas kernels for 13% -> 14%
where the time goes in v4:
time: 90 us; the launch traced here: 89.6 us
  waiting for transfers between devices  42 us (47%)
  starting transfers between devices  23.7 us (26%)
  Pallas kernels  19.7 us (22%)
  other arithmetic  2.88 us (3%)
  between operations  1.05 us (1%)
    ppermute x6, waiting for transfers between devices, turn(): found.append((lax.ppermute(x, 'kv', pairs), d))  15.3 us
    ppermute x4, waiting for transfers between devices, gather_spans(): passing = lax.ppermute(passing, 'kv', pairs)  13.4 us
    ppermute x6, waiting for transfers between devices, swap(): return lax.ppermute(x, ('kv', 'tp'), pairs)  13.3 us
    ppermute x6, starting transfers between devices, turn(): found.append((lax.ppermute(x, 'kv', pairs), d))  11 us
    pallas_call x3, Pallas kernels, attend(): pl.pallas_call(body, in_specs=[SMEM, SMEM, VMEM, *[ANY] * (2 * group + le...  10.5 us
    ppermute x6, starting transfers between devices, swap(): return lax.ppermute(x, ('kv', 'tp'), pairs)  7.46 us
    pallas_call x1, Pallas kernels, project(): pl.pallas_call(body, in_specs=[SMEM] + [ANY] * (1 + len(flat) + len(after...  6.2 us
    ppermute x4, starting transfers between devices, gather_spans(): passing = lax.ppermute(passing, 'kv', pairs)  5.18 us
  transfers between devices with their start and end apart: 16, of which 7 were waited for; matrix products, arithmetic and copies ran while one was open for 3% of the time, Pallas kernels for 14%

profile of v4, /device:TPU:8, one launch (start us, length us, event | category | flops | bytes accessed | tf_op | source)
XLA Modules:
  0.0 89.6 jit_solution(1532568482113242918)
XLA Ops:
  0.0 6.2 %shard_map.84 = (bf16[256,512]{1,0:T(8,128)(2,1)S(1)}, bf16[256,512]{1,0:T(8,128)(2,1)S(1)}, bf16[256,512]{1,0:T(8,128)(2,1)S(1)}, bf16[256,512]{1,0:T(8,128)(2,...) custom-call(s32[4]{0:T(128)} %len_ref.11, ...), custom_call_target="tpu_custom_call" | custom-call | flops 4294967296 | bytes 8388608 | tf_op jit(solution)/shard_map/pallas_call | solution.py:131
  6.2 1.3 %collective-permute-start.40 = (bf16[256,512]{1,0:T(8,128)(2,1)S(1)}, bf16[256,512]{1,0:T(8,128)(2,1)S(1)}, u32[]{:S(2)}, u32[]{:S(2)}) collective-permute-start(bf16[256,512]{1,0:T(8,128)(2,1)S(1)} %get-tuple-element.67.rest_3_), channel_id=1, source_target_pairs={{0,8},{4,12},{1,9},{5,13},{2,10},{6,14},{3,11},{7,15}} | collective-permute-start | bytes 786440 | tf_op jit(solution)/shard_map/ppermute | solution.py:508
  7.5 1.9 %collective-permute-start.39 = (bf16[2,256,512]{2,1,0:T(8,128)(2,1)S(1)}, bf16[2,256,512]{2,1,0:T(8,128)(2,1)S(1)}, u32[]{:S(2)}, u32[]{:S(2)}) collective-permute-start(bf16[2,256,512]{2,1,0:T(8,128)(2,1)S(1)} %get-tuple-element.68), channel_id=1, source_target_pairs={{0,4},{8,12},{12,8},{1,5},{9,13},{13,9},{2,6},{10,14},{14,10},{3,7... | collective-permute-start | bytes 1572872 | tf_op jit(solution)/shard_map/ppermute | solution.py:490
  9.4 6.9 %collective-permute-done.40.rest_6_ = bf16[256,512]{1,0:T(8,128)(2,1)S(1)} collective-permute-done((bf16[256,512]{1,0:T(8,128)(2,1)S(1)}, bf16[256,512]{1,0:T(8,128)(2,1)S(1)}, u32[]{:S(2)}, u32[]{:S(2)}) %collective-permute-start.40) | collective-permute-done | bytes 262176 | tf_op jit(solution)/shard_map/ppermute | solution.py:508
  16.4 1.9 %collective-permute-start.41 = (bf16[256,512]{1,0:T(8,128)(2,1)S(1)}, bf16[256,512]{1,0:T(8,128)(2,1)S(1)}, u32[]{:S(2)}, u32[]{:S(2)}) collective-permute-start(bf16[256,512]{1,0:T(8,128)(2,1)S(1)} %collective-permute-done.40.rest_6_), channel_id=1, source_target_pairs={{8,12},{12,8},{9,13},{13,9},{10,14},{14,10},{11,15},{15,11}} | collective-permute-start | bytes 786440 | tf_op jit(solution)/shard_map/ppermute | solution.py:490
  18.3 1.9 %collective-permute-start.29 = (bf16[256,512]{1,0:T(8,128)(2,1)S(1)}, bf16[256,512]{1,0:T(8,128)(2,1)S(1)}, u32[]{:S(2)}, u32[]{:S(2)}) collective-permute-start(bf16[256,512]{1,0:T(8,128)(2,1)S(1)} %get-tuple-element.57.rest_1_), channel_id=1, source_target_pairs={{0,8},{4,12},{8,16},{12,20},{16,24},{20,28},{1,9},{5,13},{9,17},{1... | collective-permute-start | bytes 786440 | tf_op jit(solution)/shard_map/ppermute | solution.py:508
  20.2 8.5 %collective-permute-done.41.rest_7_ = bf16[256,512]{1,0:T(8,128)(2,1)S(1)} collective-permute-done((bf16[256,512]{1,0:T(8,128)(2,1)S(1)}, bf16[256,512]{1,0:T(8,128)(2,1)S(1)}, u32[]{:S(2)}, u32[]{:S(2)}) %collective-permute-start.41) | collective-permute-done | bytes 262176 | tf_op jit(solution)/shard_map/ppermute | solution.py:490
  28.7 4.3 %shard_map.87 = (bf16[2,2,256,512]{3,2,1,0:T(8,128)(2,1)S(1)}, bf16[2,2,256,512]{3,2,1,0:T(8,128)(2,1)S(1)}) custom-call(s32[4]{0:T(128)S(1)} %copy-done.3, s32[4,4,32]{2,1,0:T(4,128)S(1)} %copy-done.2, s32[4,4,32]{2,1,0:T(4,128)S(1)} %copy-done.2, bf16[256,512]{1,0:T(8,128)(2,1)S(1)} %get-tuple-element.64.rest_0_, ...), custom_call_target="tpu_custom_call" | custom-call | flops 2147483648 | bytes 6291456 | tf_op jit(solution)/shard_map/pallas_call | solution.py:375
  33.0 1.9 %collective-permute-start.42 = (bf16[2,2,256,512]{3,2,1,0:T(8,128)(2,1)S(1)}, bf16[2,2,256,512]{3,2,1,0:T(8,128)(2,1)S(1)}, u32[]{:S(2)}, u32[]{:S(2)}) collective-permute-start(bf16[2,2,256,512]{3,2,1,0:T(8,128)(2,1)S(1)} %get-tuple-element.70), channel_id=1, source_target_pairs={{0,1},{1,0},{2,3},{3,2},{4,5},{5,4},{6,7},{7,6},{8,9},{9,8},{10,11... | collective-permute-start | bytes 3145736 | tf_op jit(solution)/shard_map/ppermute | solution.py:546
  35.0 1.3 %collective-permute-start.31 = (bf16[256,512]{1,0:T(8,128)(2,1)S(1)}, bf16[256,512]{1,0:T(8,128)(2,1)S(1)}, u32[]{:S(2)}, u32[]{:S(2)}) collective-permute-start(bf16[256,512]{1,0:T(8,128)(2,1)S(1)} %collective-permute-done.29.rest_3_), channel_id=1, source_target_pairs={{8,16},{12,20},{16,24},{20,28},{9,17},{13,21},{17,25},{21,29},{10,... | collective-permute-start | bytes 786440 | tf_op jit(solution)/shard_map/ppermute | solution.py:508
  36.3 6.5 %collective-permute-done.31.rest_5_ = bf16[256,512]{1,0:T(8,128)(2,1)S(1)} collective-permute-done((bf16[256,512]{1,0:T(8,128)(2,1)S(1)}, bf16[256,512]{1,0:T(8,128)(2,1)S(1)}, u32[]{:S(2)}, u32[]{:S(2)}) %collective-permute-start.31) | collective-permute-done | bytes 262176 | tf_op jit(solution)/shard_map/ppermute | solution.py:508
  42.7 0.7 collective-permute-start.33
  43.4 1.9 %collective-permute-start.28 = (bf16[256,512]{1,0:T(8,128)(2,1)S(1)}, bf16[256,512]{1,0:T(8,128)(2,1)S(1)}, u32[]{:S(2)}, u32[]{:S(2)}) collective-permute-start(bf16[256,512]{1,0:T(8,128)(2,1)S(1)} %get-tuple-element.57.rest_1_), channel_id=1, source_target_pairs={{0,4},{8,12},{12,8},{16,20},{20,16},{24,28},{28,24},{1,5},{9,13},{... | collective-permute-start | bytes 786440 | tf_op jit(solution)/shard_map/ppermute | solution.py:490
  45.3 3.9 %collective-permute-start.30 = (bf16[256,512]{1,0:T(8,128)(2,1)S(1)}, bf16[256,512]{1,0:T(8,128)(2,1)S(1)}, u32[]{:S(2)}, u32[]{:S(2)}) collective-permute-start(bf16[256,512]{1,0:T(8,128)(2,1)S(1)} %collective-permute-done.29.rest_3_), channel_id=1, source_target_pairs={{8,12},{12,8},{16,20},{20,16},{24,28},{28,24},{9,13},{13,9},{17,21... | collective-permute-start | bytes 786440 | tf_op jit(solution)/shard_map/ppermute | solution.py:490
  49.3 0.7 collective-permute-start.32
  50.0 0.7 collective-permute-start.34
  50.7 0.8 shard_map.86
  51.5 3.0 %collective-permute-done.28.rest_2_ = bf16[256,512]{1,0:T(8,128)(2,1)S(1)} collective-permute-done((bf16[256,512]{1,0:T(8,128)(2,1)S(1)}, bf16[256,512]{1,0:T(8,128)(2,1)S(1)}, u32[]{:S(2)}, u32[]{:S(2)}) %collective-permute-start.28) | collective-permute-done | bytes 262176 | tf_op jit(solution)/shard_map/ppermute | solution.py:490
  54.5 0.7 collective-permute-start.37
  55.2 3.9 %collective-permute-done.30.rest_4_ = bf16[256,512]{1,0:T(8,128)(2,1)S(1)} collective-permute-done((bf16[256,512]{1,0:T(8,128)(2,1)S(1)}, bf16[256,512]{1,0:T(8,128)(2,1)S(1)}, u32[]{:S(2)}, u32[]{:S(2)}) %collective-permute-start.30) | collective-permute-done | bytes 262176 | tf_op jit(solution)/shard_map/ppermute | solution.py:490
  59.1 5.4 %shard_map.85 = (bf16[2,1,256,512]{3,2,1,0:T(8,128)(2,1)S(1)}, bf16[2,1,256,512]{3,2,1,0:T(8,128)(2,1)S(1)}) custom-call(s32[4]{0:T(128)S(1)} %copy-done.3, s32[4,4,32]{2,1,0:T(4,128)S(1)} %copy-done.2, s32[4,4,32]{2,1,0:T(4,128)S(1)} %copy-done.2, bf16[256,512]{1,0:T(8,128)(2,1)S(1)} %get-tuple-element.56.rest_0_, ...), custom_call_target="tpu_custom_call" | custom-call | flops 1073741824 | bytes 3145728 | tf_op jit(solution)/shard_map/pallas_call | solution.py:375
  64.5 1.1 %fusion.1 = (bf16[2,256,512]{2,1,0:T(8,128)(2,1)}, f32[2,256,512]{2,1,0:T(8,128)S(1)}) fusion(bf16[2,2,256,512]{3,2,1,0:T(8,128)(2,1)S(1)} %collective-permute-done.42, bf16[2,2,256,512]{3,2,1,0:T(8,128)(2,1)S(1)} %get-tuple-element.69), kind=kLoop, calls=%fused_computation.5 | loop fusion | flops 1835008 | bytes 3670016 | tf_op jit(solution)/shard_map/convert_element_type | solution.py:554
  65.6 3.5 %collective-permute-start.43 = (bf16[2,256,512]{2,1,0:T(8,128)(2,1)}, bf16[2,256,512]{2,1,0:T(8,128)(2,1)S(1)}, u32[]{:S(2)}, u32[]{:S(2)}) collective-permute-start(bf16[2,256,512]{2,1,0:T(8,128)(2,1)} %get-tuple-element.74), channel_id=1, source_target_pairs={{0,2},{1,3},{2,0},{3,1},{4,6},{5,7},{6,4},{7,5},{8,10},{9,11},{10,... | collective-permute-start | bytes 1572872 | tf_op jit(solution)/shard_map/ppermute | solution.py:546
  69.2 0.8 fusion.3
  70.0 0.7 collective-permute-start.38
  70.8 0.6 collective-permute-start.36
  71.6 0.7 compare_reduce_fusion
  72.9 9.7 %collective-permute-done.43.refs_3_ = bf16[2,256,512]{2,1,0:T(8,128)(2,1)S(1)} collective-permute-done((bf16[2,256,512]{2,1,0:T(8,128)(2,1)}, bf16[2,256,512]{2,1,0:T(8,128)(2,1)S(1)}, u32[]{:S(2)}, u32[]{:S(2)}) %collective-permute-start.43) | collective-permute-done | bytes 524320 | tf_op jit(solution)/shard_map/ppermute | solution.py:546
  82.6 1.6 %finish.4.refs_2_ = bf16[4,256,512]{2,1,0:T(8,128)(2,1)} custom-call(s32[4]{0:T(128)S(1)} %copy-done.3, f32[1,256,512]{2,1,0:T(8,128)S(1)} %get-tuple-element.77.refs_0_, bf16[1,256,512]{2,1,0:T(8,128)(2,1)S(1)} %collective-permute-done.38.refs_1_, f32[2,256,512]{2,1,0:T(8,128)S(1)} %get-tuple-element.75.refs_2_, ...), custom_call_target="tpu_custom_call" | custom-call | flops 1572864 | bytes 3145728 | tf_op jit(solution)/shard_map/finish/pallas_call | solution.py:459
  84.2 3.5 %collective-permute-done.36.refs_1_ = bf16[1,256,512]{2,1,0:T(8,128)(2,1)S(1)} collective-permute-done((bf16[1,256,512]{2,1,0:T(8,128)(2,1)S(1)}, bf16[1,256,512]{2,1,0:T(8,128)(2,1)S(1)}, u32[]{:S(2)}, u32[]{:S(2)}) %collective-permute-start.36) | collective-permute-done | bytes 262176 | tf_op jit(solution)/shard_map/ppermute | solution.py:546
  87.8 1.4 %finish.5 = bf16[4,256,512]{2,1,0:T(8,128)(2,1)} custom-call(s32[4]{0:T(128)S(1)} %copy-done.3, f32[1,256,512]{2,1,0:T(8,128)S(1)} %get-tuple-element.79.refs_0_, bf16[1,256,512]{2,1,0:T(8,128)(2,1)S(1)} %collective-permute-done.36.refs_1_, bf16[4,256,512]{2,1,0:T(8,128)(2,1)} %finish.4.refs_2_), custom_call_target="tpu_custom_call", output_to_operand_aliasing={{}: (3, {})} | custom-call | flops 524288 | bytes 1048576 | tf_op jit(solution)/shard_map/finish/pallas_call | solution.py:459
  89.2 0.2 conditional.1
  (24 shorter events, 0.4 us)
Async XLA Ops:
  0.0 28.7 %copy-start.3 = (s32[4]{0:T(128)S(1)}, s32[4]{0:T(128)}, u32[]{:S(2)}) copy-start(s32[4]{0:T(128)} %len_ref.11) | copy-start | bytes 52
  0.0 28.7 %copy-start.2 = (s32[4,4,32]{2,1,0:T(4,128)S(1)}, s32[4,4,32]{2,1,0:T(4,128)}, u32[]{:S(2)}) copy-start(s32[4,4,32]{2,1,0:T(4,128)} %names_ref.5) | copy-start | bytes 6148
  0.0 28.7 %copy-start = (bf16[512,2048]{1,0:T(8,128)(2,1)S(1)}, bf16[512,2048]{1,0:T(8,128)(2,1)}, u32[]{:S(2)}) copy-start(bf16[512,2048]{1,0:T(8,128)(2,1)} %rest_8_.1) | copy-start | bytes 6291460
  6.2 10.1 %collective-permute-start.40 = (bf16[256,512]{1,0:T(8,128)(2,1)S(1)}, bf16[256,512]{1,0:T(8,128)(2,1)S(1)}, u32[]{:S(2)}, u32[]{:S(2)}) collective-permute-start(bf16[256,512]{1,0:T(8,128)(2,1)S(1)} %get-tuple-element.67.rest_3_), channel_id=1, source_target_pairs={{0,8},{4,12},{1,9},{5,13},{2,10},{6,14},{3,11},{7,15}} | collective-permute-start | bytes 786440 | tf_op jit(solution)/shard_map/ppermute | solution.py:508
  7.5 21.2 %collective-permute-start.39 = (bf16[2,256,512]{2,1,0:T(8,128)(2,1)S(1)}, bf16[2,256,512]{2,1,0:T(8,128)(2,1)S(1)}, u32[]{:S(2)}, u32[]{:S(2)}) collective-permute-start(bf16[2,256,512]{2,1,0:T(8,128)(2,1)S(1)} %get-tuple-element.68), channel_id=1, source_target_pairs={{0,4},{8,12},{12,8},{1,5},{9,13},{13,9},{2,6},{10,14},{14,10},{3,7... | collective-permute-start | bytes 1572872 | tf_op jit(solution)/shard_map/ppermute | solution.py:490
  16.4 12.3 %collective-permute-start.41 = (bf16[256,512]{1,0:T(8,128)(2,1)S(1)}, bf16[256,512]{1,0:T(8,128)(2,1)S(1)}, u32[]{:S(2)}, u32[]{:S(2)}) collective-permute-start(bf16[256,512]{1,0:T(8,128)(2,1)S(1)} %collective-permute-done.40.rest_6_), channel_id=1, source_target_pairs={{8,12},{12,8},{9,13},{13,9},{10,14},{14,10},{11,15},{15,11}} | collective-permute-start | bytes 786440 | tf_op jit(solution)/shard_map/ppermute | solution.py:490
  18.3 16.7 %collective-permute-start.29 = (bf16[256,512]{1,0:T(8,128)(2,1)S(1)}, bf16[256,512]{1,0:T(8,128)(2,1)S(1)}, u32[]{:S(2)}, u32[]{:S(2)}) collective-permute-start(bf16[256,512]{1,0:T(8,128)(2,1)S(1)} %get-tuple-element.57.rest_1_), channel_id=1, source_target_pairs={{0,8},{4,12},{8,16},{12,20},{16,24},{20,28},{1,9},{5,13},{9,17},{1... | collective-permute-start | bytes 786440 | tf_op jit(solution)/shard_map/ppermute | solution.py:508
  33.0 31.5 %collective-permute-start.42 = (bf16[2,2,256,512]{3,2,1,0:T(8,128)(2,1)S(1)}, bf16[2,2,256,512]{3,2,1,0:T(8,128)(2,1)S(1)}, u32[]{:S(2)}, u32[]{:S(2)}) collective-permute-start(bf16[2,2,256,512]{3,2,1,0:T(8,128)(2,1)S(1)} %get-tuple-element.70), channel_id=1, source_target_pairs={{0,1},{1,0},{2,3},{3,2},{4,5},{5,4},{6,7},{7,6},{8,9},{9,8},{10,11... | collective-permute-start | bytes 3145736 | tf_op jit(solution)/shard_map/ppermute | solution.py:546
  35.0 7.8 %collective-permute-start.31 = (bf16[256,512]{1,0:T(8,128)(2,1)S(1)}, bf16[256,512]{1,0:T(8,128)(2,1)S(1)}, u32[]{:S(2)}, u32[]{:S(2)}) collective-permute-start(bf16[256,512]{1,0:T(8,128)(2,1)S(1)} %collective-permute-done.29.rest_3_), channel_id=1, source_target_pairs={{8,16},{12,20},{16,24},{20,28},{9,17},{13,21},{17,25},{21,29},{10,... | collective-permute-start | bytes 786440 | tf_op jit(solution)/shard_map/ppermute | solution.py:508
  42.7 7.2 %collective-permute-start.33 = (bf16[256,512]{1,0:T(8,128)(2,1)S(1)}, bf16[256,512]{1,0:T(8,128)(2,1)S(1)}, u32[]{:S(2)}, u32[]{:S(2)}) collective-permute-start(bf16[256,512]{1,0:T(8,128)(2,1)S(1)} %collective-permute-done.31.rest_5_), channel_id=1, source_target_pairs={{16,24},{20,28},{17,25},{21,29},{18,26},{22,30},{19,27},{23,31}} | collective-permute-start | bytes 786440 | tf_op jit(solution)/shard_map/ppermute | solution.py:508
  43.4 11.1 %collective-permute-start.28 = (bf16[256,512]{1,0:T(8,128)(2,1)S(1)}, bf16[256,512]{1,0:T(8,128)(2,1)S(1)}, u32[]{:S(2)}, u32[]{:S(2)}) collective-permute-start(bf16[256,512]{1,0:T(8,128)(2,1)S(1)} %get-tuple-element.57.rest_1_), channel_id=1, source_target_pairs={{0,4},{8,12},{12,8},{16,20},{20,16},{24,28},{28,24},{1,5},{9,13},{... | collective-permute-start | bytes 786440 | tf_op jit(solution)/shard_map/ppermute | solution.py:490
  45.3 13.7 %collective-permute-start.30 = (bf16[256,512]{1,0:T(8,128)(2,1)S(1)}, bf16[256,512]{1,0:T(8,128)(2,1)S(1)}, u32[]{:S(2)}, u32[]{:S(2)}) collective-permute-start(bf16[256,512]{1,0:T(8,128)(2,1)S(1)} %collective-permute-done.29.rest_3_), channel_id=1, source_target_pairs={{8,12},{12,8},{16,20},{20,16},{24,28},{28,24},{9,13},{13,9},{17,21... | collective-permute-start | bytes 786440 | tf_op jit(solution)/shard_map/ppermute | solution.py:490
  49.3 9.8 %collective-permute-start.32 = (bf16[256,512]{1,0:T(8,128)(2,1)S(1)}, bf16[256,512]{1,0:T(8,128)(2,1)S(1)}, u32[]{:S(2)}, u32[]{:S(2)}) collective-permute-start(bf16[256,512]{1,0:T(8,128)(2,1)S(1)} %collective-permute-done.31.rest_5_), channel_id=1, source_target_pairs={{16,20},{20,16},{24,28},{28,24},{17,21},{21,17},{25,29},{29,25},{1... | collective-permute-start | bytes 786440 | tf_op jit(solution)/shard_map/ppermute | solution.py:490
  50.0 9.1 %collective-permute-start.34 = (bf16[256,512]{1,0:T(8,128)(2,1)S(1)}, bf16[256,512]{1,0:T(8,128)(2,1)S(1)}, u32[]{:S(2)}, u32[]{:S(2)}) collective-permute-start(bf16[256,512]{1,0:T(8,128)(2,1)S(1)} %collective-permute-done.33.rest_7_), channel_id=1, source_target_pairs={{24,28},{28,24},{25,29},{29,25},{26,30},{30,26},{27,31},{31,27}} | collective-permute-start | bytes 786440 | tf_op jit(solution)/shard_map/ppermute | solution.py:490
  54.5 14.7 %collective-permute-start.37 = (bf16[2,1,256,512]{3,2,1,0:T(8,128)(2,1)S(1)}, bf16[2,1,256,512]{3,2,1,0:T(8,128)(2,1)S(1)}, u32[]{:S(2)}, u32[]{:S(2)}) collective-permute-start(bf16[2,1,256,512]{3,2,1,0:T(8,128)(2,1)S(1)} %get-tuple-element.63), channel_id=1, source_target_pairs={{0,1},{1,0},{2,3},{3,2}} | collective-permute-start | bytes 1572872 | tf_op jit(solution)/shard_map/ppermute | solution.py:546
  64.4 6.2 %collective-permute-start.35 = (bf16[2,1,256,512]{3,2,1,0:T(8,128)(2,1)S(1)}, bf16[2,1,256,512]{3,2,1,0:T(8,128)(2,1)S(1)}, u32[]{:S(2)}, u32[]{:S(2)}) collective-permute-start(bf16[2,1,256,512]{3,2,1,0:T(8,128)(2,1)S(1)} %get-tuple-element.59), channel_id=1, source_target_pairs={{0,1},{1,0},{2,3},{3,2},{4,5},{5,4},{6,7},{7,6},{8,9},{9,8},{10,11... | collective-permute-start | bytes 1572872 | tf_op jit(solution)/shard_map/ppermute | solution.py:546
  65.6 5.8 %copy-start.5 = (s32[4]{0:T(128)S(1)}, s32[4]{0:T(128)}, u32[]{:S(2)}) copy-start(s32[4]{0:T(128)} %constant.10) | copy-start | bytes 52
  65.6 17.0 %collective-permute-start.43 = (bf16[2,256,512]{2,1,0:T(8,128)(2,1)}, bf16[2,256,512]{2,1,0:T(8,128)(2,1)S(1)}, u32[]{:S(2)}, u32[]{:S(2)}) collective-permute-start(bf16[2,256,512]{2,1,0:T(8,128)(2,1)} %get-tuple-element.74), channel_id=1, source_target_pairs={{0,2},{1,3},{2,0},{3,1},{4,6},{5,7},{6,4},{7,5},{8,10},{9,11},{10,... | collective-permute-start | bytes 1572872 | tf_op jit(solution)/shard_map/ppermute | solution.py:546
  70.0 2.9 %collective-permute-start.38 = (bf16[1,256,512]{2,1,0:T(8,128)(2,1)}, bf16[1,256,512]{2,1,0:T(8,128)(2,1)S(1)}, u32[]{:S(2)}, u32[]{:S(2)}) collective-permute-start(bf16[1,256,512]{2,1,0:T(8,128)(2,1)} %get-tuple-element.76), channel_id=1, source_target_pairs={{0,2},{1,3},{2,0},{3,1}} | collective-permute-start | bytes 786440 | tf_op jit(solution)/shard_map/ppermute | solution.py:546
  70.8 16.9 %collective-permute-start.36 = (bf16[1,256,512]{2,1,0:T(8,128)(2,1)S(1)}, bf16[1,256,512]{2,1,0:T(8,128)(2,1)S(1)}, u32[]{:S(2)}, u32[]{:S(2)}) collective-permute-start(bf16[1,256,512]{2,1,0:T(8,128)(2,1)S(1)} %get-tuple-element.78), channel_id=1, source_target_pairs={{0,2},{1,3},{2,0},{3,1},{4,6},{5,7},{6,4},{7,5},{8,10},{9,11},{10,... | collective-permute-start | bytes 786440 | tf_op jit(solution)/shard_map/ppermute | solution.py:546
  72.9 14.9 %copy-start.1 = (bf16[512,2048]{1,0:T(8,128)(2,1)S(1)}, bf16[512,2048]{1,0:T(8,128)(2,1)}, u32[]{:S(2)}) copy-start(bf16[512,2048]{1,0:T(8,128)(2,1)} %rest_8_.1) | copy-start | bytes 6291460
  72.9 14.9 %copy-start.4 = (bf16[2048,256]{1,0:T(8,128)(2,1)S(1)}, bf16[2048,256]{1,0:T(8,128)(2,1)}, u32[]{:S(2)}) copy-start(bf16[2048,256]{1,0:T(8,128)(2,1)} %refs_0_.1) | copy-start | bytes 3145732
